TPU v7x, 768 devices: a whole 4x8x12 slice. The times are simulated.
768 devices in a mesh: fs: 96 (over z, y), tp: 8 (over x, core).
Axes of the slice: x: 4, y: 8, z: 12, core: 2. Of those that a mesh axis runs over, the one named last changes fastest.
Arguments:
- tokens: bfloat16 [24576, 1344], P('fs'), may hold values from -6 to 6
- cotangent: bfloat16 [24576, 1344], P('fs'), may hold values from -20 to 20
- gate_weight: bfloat16 [1344, 3072], P('fs', 'tp'), may hold values from -0.15625 to 0.15625
- up_weight: bfloat16 [1344, 3072], P('fs', 'tp'), may hold values from -0.15625 to 0.15625
- down_weight: bfloat16 [3072, 1344], P('tp', 'fs'), may hold values from -0.109375 to 0.109375
Outputs:
- input_grad: bfloat16 [24576, 1344], P('fs')
- down_grad: float32 [3072, 1344], P('tp', 'fs')
All inputs are finite; a program needn't handle non-finite values.
Results may differ from a plain program's by a relative error of at most 0.013.
Values may be sent and summed in bfloat16 or wider, within the bound.
No kernel may reach another device: no remote copies, remote signals or barrier semaphores. Data moves between devices by JAX's collectives and lax.ppermute only.
A program may use at most 64 MiB of HBM per device.

v0:
```python
import jax
import jax.numpy as jnp
import numpy as np
from jax import lax
from jax.sharding import Mesh
from jax.sharding import PartitionSpec as P


FS = ("fs_0", "fs_1")


def shifted(array, axis, step):
    peers = lax.axis_size(axis)
    return lax.ppermute(array, axis, [(k, (k + step) % peers) for k in range(peers)])


def sent_to_all(array, axis):
    peers = lax.axis_size(axis)
    return lax.all_to_all(
        jnp.broadcast_to(array[None], (peers, *array.shape)), axis, 0, 0, tiled=True
    )


def exchanged(parts, axis):
    got = lax.all_to_all(parts, axis, 0, 0, tiled=True)
    return got.astype(jnp.float32).sum(axis=0)


def contract_rows(left, right):
    return lax.dot_general(
        left, right, (((0,), (0,)), ((), ())), preferred_element_type=jnp.float32
    )


def contract_cols(left, right):
    return lax.dot_general(
        left, right, (((1,), (1,)), ((), ())), preferred_element_type=jnp.float32
    )


def inner_first(width, outer, inner):
    rows = width // (outer * inner)
    return np.arange(width).reshape(outer, inner, rows).transpose(1, 0, 2).reshape(-1)


def picked(source):
    source = jnp.asarray(source, jnp.int32)
    spot = lax.broadcasted_iota(jnp.int32, (source.size, source.size), 1)
    return (source[:, None] == spot).astype(jnp.bfloat16)


def around(blocks, axis):
    peers = lax.axis_size(axis)
    split = blocks[0].shape[0] // 16 * 8
    ups = downs = blocks
    parts, order = [[b] for b in blocks], [0]
    for step in range(1, peers // 2):
        moved = [(shifted(u, axis, 1), shifted(d, axis, -1)) for u, d in zip(ups, downs)]
        ups, downs = zip(*moved)
        for held, pair in zip(parts, moved):
            held += pair
        order += [-step % peers, step]
    for held, u, d in zip(parts, ups, downs):
        held += [shifted(u[:split], axis, 1), shifted(d[split:], axis, -1)]
    return [jnp.concatenate(held) for held in parts], order + [peers // 2]


def summed_over_tp(partial, after):
    half = partial.shape[0] // 2
    core = lax.axis_index("core")
    kept = lax.dynamic_slice_in_dim(partial, core * half, half)
    given = lax.dynamic_slice_in_dim(partial, (1 - core) * half, half)
    kept = kept.astype(jnp.float32) + shifted(given, "core", 1).astype(jnp.float32)
    kept = kept.astype(jnp.bfloat16)
    chips = lax.axis_size("chip")
    others = [shifted(kept, "chip", s) for s in range(1, chips)]
    *others, _ = lax.optimization_barrier((*others, after))
    total = kept.astype(jnp.float32)
    for other in others:
        total = total + other.astype(jnp.float32)
    total = total.astype(jnp.bfloat16)
    other = shifted(total, "core", 1)
    first = jnp.where(core == 0, total, other)
    second = jnp.where(core == 0, other, total)
    return jnp.concatenate([first, second])


def gradients(tokens, cotangent, gate_weight, up_weight, down_weight):
    outer, inner = (lax.axis_size(a) for a in FS)
    rows, units = gate_weight.shape
    width = tokens.shape[1]
    place = lax.axis_index("fs_1")

    weights = jnp.concatenate([gate_weight, up_weight, down_weight.T], axis=1)
    weights = sent_to_all(weights, "fs_0").reshape(outer * rows, 3 * units)
    (gate_up, down), order = around((weights[:, : 2 * units], weights[:, 2 * units :]), "fs_1")

    spot = inner_first(width, outer, inner)
    block = (jnp.asarray(order, jnp.int32) + place) % inner
    near = (block[:, None] * rows + spot[: outer * rows][None, :]).reshape(-1)
    here = picked(near)
    near_tokens = contract_cols(here, tokens).astype(jnp.bfloat16)
    near_cotangent = contract_cols(here, cotangent).astype(jnp.bfloat16)
    turned_cotangent = contract_cols(picked(spot), cotangent).astype(jnp.bfloat16)
    near_tokens, near_cotangent, turned_cotangent = lax.optimization_barrier(
        (near_tokens, near_cotangent, turned_cotangent)
    )

    both = contract_rows(near_tokens, gate_up)
    gate_pre, up_pre = both[:, :units], both[:, units:]
    sigmoid_gate = jax.nn.sigmoid(gate_pre)
    activated = gate_pre * sigmoid_gate
    hidden = (activated * up_pre).astype(jnp.bfloat16)

    terms = jnp.dot(turned_cotangent, hidden, preferred_element_type=jnp.float32)
    terms = terms.astype(jnp.bfloat16).reshape(inner, outer * rows, units)
    terms = exchanged(terms, "fs_1").astype(jnp.bfloat16).reshape(outer, rows, units)

    hidden_grad = contract_rows(near_cotangent, down)
    gate_pre_grad = (
        hidden_grad * up_pre * sigmoid_gate * (1.0 + gate_pre * (1.0 - sigmoid_gate))
    ).astype(jnp.bfloat16)
    up_pre_grad = (hidden_grad * activated).astype(jnp.bfloat16)
    partial = contract_cols(gate_up, jnp.concatenate([gate_pre_grad, up_pre_grad], axis=1))
    total = summed_over_tp(partial.astype(jnp.bfloat16), terms)
    down_grad = exchanged(terms, "fs_0").T
    input_grad = contract_rows(total, here).astype(jnp.bfloat16)
    return (input_grad, down_grad)


def solution(mesh):
    torus = Mesh(
        mesh.devices.reshape(12, 8, mesh.shape["tp"] // 2, 2), ("fs_0", "fs_1", "chip", "core")
    )
    tp = ("chip", "core")
    in_specs = (P(FS, None), P(FS, None), P(FS, tp), P(FS, tp), P(tp, FS))
    out_specs = (P(FS, None), P(tp, FS))
    return jax.shard_map(
        gradients, mesh=torus, in_specs=in_specs, out_specs=out_specs, check_vma=False
    )
```

profile of v0, /device:TPU:10, one launch (start us, length us, event | category | flops | bytes accessed | tf_op | source)
XLA Modules:
  0.0 171.2 jit_solution(14593959677710843784)
XLA Ops:
  0.6 0.0 copy-start
  0.6 0.8 pad_maximum_fusion
  1.5 0.8 broadcast_in_dim.2
  2.3 15.2 %all-to-all-start = ((bf16[12,14,1152]{2,1,0:T(8,128)(2,1)}), bf16[12,14,1152]{2,1,0:T(8,128)(2,1)S(1)}, u32[]{:S(2)}, u32[]{:S(2)}) async-start(bf16[12,14,1152]{2,1,0:T(8,128)(2,1)} %broadcast_in_dim.2), calls=%async_computation | async-start | bytes 884736 | tf_op jit(solution)/shard_map/all_to_all | solution.py:19
  17.4 0.7 fusion.21
  18.1 0.7 broadcast_add_fusion
  18.9 0.1 add.65
  19.0 2.4 %fusion.10 = bf16[1344,256]{1,0:T(8,128)(2,1)} fusion(bf16[256,1344]{0,1:T(8,128)(2,1)S(1)} %copy-done, s32[1344]{0:T(1024)S(1)} %add.65), kind=kOutput, calls=%fused_computation.14 | convolution fusion | flops 926994432 | bytes 1381632 | tf_op jit(solution)/shard_map/dot_general | solution.py:36
  21.3 2.3 %fusion.9 = bf16[1344,256]{1,0:T(8,128)(2,1)} fusion(bf16[256,1344]{0,1:T(8,128)(2,1)S(1)} %copy-done.2, s32[1344]{0:T(1024)S(1)} %add.65), kind=kOutput, calls=%fused_computation.13 | convolution fusion | flops 926994432 | bytes 1381632 | tf_op jit(solution)/shard_map/dot_general | solution.py:36
  23.7 14.8 %all-to-all-done = bf16[12,14,1152]{2,1,0:T(8,128)(2,1)S(1)} async-done(((bf16[12,14,1152]{2,1,0:T(8,128)(2,1)}), bf16[12,14,1152]{2,1,0:T(8,128)(2,1)S(1)}, u32[]{:S(2)}, u32[]{:S(2)}) %all-to-all-start) | async-done | bytes 387104 | tf_op jit(solution)/shard_map/all_to_all | solution.py:19
  38.5 0.1 reshape.31
  38.6 0.7 fusion.26
  39.3 3.5 %collective-permute-start = (bf16[168,768]{1,0:T(8,128)(2,1)S(1)}, bf16[168,768]{1,0:T(8,128)(2,1)S(1)}, u32[]{:S(2)}, u32[]{:S(2)}) collective-permute-start(bf16[168,768]{1,0:T(8,128)(2,1)S(1)} %get-tuple-element.20), channel_id=1, source_target_pairs={{0,8},{8,16},{16,24},{24,32},{32,40},{40,48},{48,56},{56,0},{1,9},... | collective-permute-start | bytes 774152 | tf_op jit(solution)/shard_map/ppermute | solution.py:14
  42.8 2.4 %collective-permute-start.1 = (bf16[168,768]{1,0:T(8,128)(2,1)S(1)}, bf16[168,768]{1,0:T(8,128)(2,1)S(1)}, u32[]{:S(2)}, u32[]{:S(2)}) collective-permute-start(bf16[168,768]{1,0:T(8,128)(2,1)S(1)} %get-tuple-element.20), channel_id=1, source_target_pairs={{0,56},{8,0},{16,8},{24,16},{32,24},{40,32},{48,40},{56,48},{1,57}... | collective-permute-start | bytes 774152 | tf_op jit(solution)/shard_map/ppermute | solution.py:14
  45.2 3.5 %collective-permute-start.8 = (bf16[168,384]{1,0:T(8,128)(2,1)S(1)}, bf16[168,384]{1,0:T(8,128)(2,1)S(1)}, u32[]{:S(2)}, u32[]{:S(2)}) collective-permute-start(bf16[168,384]{1,0:T(8,128)(2,1)S(1)} %get-tuple-element.18), channel_id=1, source_target_pairs={{0,8},{8,16},{16,24},{24,32},{32,40},{40,48},{48,56},{56,0},{1,9},... | collective-permute-start | bytes 387080 | tf_op jit(solution)/shard_map/ppermute | solution.py:14
  48.7 2.4 %collective-permute-start.9 = (bf16[168,384]{1,0:T(8,128)(2,1)S(1)}, bf16[168,384]{1,0:T(8,128)(2,1)S(1)}, u32[]{:S(2)}, u32[]{:S(2)}) collective-permute-start(bf16[168,384]{1,0:T(8,128)(2,1)S(1)} %get-tuple-element.18), channel_id=1, source_target_pairs={{0,56},{8,0},{16,8},{24,16},{32,24},{40,32},{48,40},{56,48},{1,57}... | collective-permute-start | bytes 387080 | tf_op jit(solution)/shard_map/ppermute | solution.py:14
  51.1 2.3 %fusion.8 = bf16[1344,256]{1,0:T(8,128)(2,1)} fusion(bf16[256,1344]{0,1:T(8,128)(2,1)S(1)} %copy-done, s32[1344]{0:T(1024)S(1)} %copy-done.3), kind=kOutput, calls=%fused_computation.12 | convolution fusion | flops 926994432 | bytes 1381632 | tf_op jit(solution)/shard_map/dot_general | solution.py:36
  53.4 3.8 %collective-permute-start.10 = (bf16[168,384]{1,0:T(8,128)(2,1)S(1)}, bf16[168,384]{1,0:T(8,128)(2,1)S(1)}, u32[]{:S(2)}, u32[]{:S(2)}) collective-permute-start(bf16[168,384]{1,0:T(8,128)(2,1)S(1)} %collective-permute-done.8), channel_id=1, source_target_pairs={{0,8},{8,16},{16,24},{24,32},{32,40},{40,48},{48,56},{56,0},{1,9},... | collective-permute-start | bytes 387080 | tf_op jit(solution)/shard_map/ppermute | solution.py:14
  57.3 3.1 %collective-permute-start.11 = (bf16[168,384]{1,0:T(8,128)(2,1)S(1)}, bf16[168,384]{1,0:T(8,128)(2,1)S(1)}, u32[]{:S(2)}, u32[]{:S(2)}) collective-permute-start(bf16[168,384]{1,0:T(8,128)(2,1)S(1)} %collective-permute-done.9), channel_id=1, source_target_pairs={{0,56},{8,0},{16,8},{24,16},{32,24},{40,32},{48,40},{56,48},{1,57}... | collective-permute-start | bytes 387080 | tf_op jit(solution)/shard_map/ppermute | solution.py:14
  60.5 3.9 %collective-permute-start.2 = (bf16[168,768]{1,0:T(8,128)(2,1)S(1)}, bf16[168,768]{1,0:T(8,128)(2,1)S(1)}, u32[]{:S(2)}, u32[]{:S(2)}) collective-permute-start(bf16[168,768]{1,0:T(8,128)(2,1)S(1)} %collective-permute-done), channel_id=1, source_target_pairs={{0,8},{8,16},{16,24},{24,32},{32,40},{40,48},{48,56},{56,0},{1,9},... | collective-permute-start | bytes 774152 | tf_op jit(solution)/shard_map/ppermute | solution.py:14
  64.4 3.1 %collective-permute-start.3 = (bf16[168,768]{1,0:T(8,128)(2,1)S(1)}, bf16[168,768]{1,0:T(8,128)(2,1)S(1)}, u32[]{:S(2)}, u32[]{:S(2)}) collective-permute-start(bf16[168,768]{1,0:T(8,128)(2,1)S(1)} %collective-permute-done.1), channel_id=1, source_target_pairs={{0,56},{8,0},{16,8},{24,16},{32,24},{40,32},{48,40},{56,48},{1,57}... | collective-permute-start | bytes 774152 | tf_op jit(solution)/shard_map/ppermute | solution.py:14
  67.6 3.9 %collective-permute-start.12 = (bf16[168,384]{1,0:T(8,128)(2,1)S(1)}, bf16[168,384]{1,0:T(8,128)(2,1)S(1)}, u32[]{:S(2)}, u32[]{:S(2)}) collective-permute-start(bf16[168,384]{1,0:T(8,128)(2,1)S(1)} %collective-permute-done.10), channel_id=1, source_target_pairs={{0,8},{8,16},{16,24},{24,32},{32,40},{40,48},{48,56},{56,0},{1,9},... | collective-permute-start | bytes 387080 | tf_op jit(solution)/shard_map/ppermute | solution.py:14
  71.5 0.7 constant_dynamic-update-slice_fusion.7
  72.3 3.1 %collective-permute-start.13 = (bf16[168,384]{1,0:T(8,128)(2,1)S(1)}, bf16[168,384]{1,0:T(8,128)(2,1)S(1)}, u32[]{:S(2)}, u32[]{:S(2)}) collective-permute-start(bf16[168,384]{1,0:T(8,128)(2,1)S(1)} %collective-permute-done.11), channel_id=1, source_target_pairs={{0,56},{8,0},{16,8},{24,16},{32,24},{40,32},{48,40},{56,48},{1,57}... | collective-permute-start | bytes 387080 | tf_op jit(solution)/shard_map/ppermute | solution.py:14
  75.4 0.7 constant_dynamic-update-slice_fusion.6
  76.2 3.9 %collective-permute-start.14 = (bf16[80,384]{1,0:T(8,128)(2,1)S(1)}, bf16[80,384]{1,0:T(8,128)(2,1)S(1)}, u32[]{:S(2)}, u32[]{:S(2)}) collective-permute-start(bf16[80,384]{1,0:T(8,128)(2,1)S(1)} %slice.36), channel_id=1, source_target_pairs={{0,8},{8,16},{16,24},{24,32},{32,40},{40,48},{48,56},{56,0},{1,9},... | collective-permute-start | bytes 184328 | tf_op jit(solution)/shard_map/ppermute | solution.py:14
  80.1 0.2 collective-permute-done.13
  80.3 2.9 %collective-permute-start.15 = (bf16[88,384]{1,0:T(8,128)(2,1)S(1)}, bf16[88,384]{1,0:T(8,128)(2,1)S(1)}, u32[]{:S(2)}, u32[]{:S(2)}) collective-permute-start(bf16[88,384]{1,0:T(8,128)(2,1)S(1)} %slice.37), channel_id=1, source_target_pairs={{0,56},{8,0},{16,8},{24,16},{32,24},{40,32},{48,40},{56,48},{1,57}... | collective-permute-start | bytes 202760 | tf_op jit(solution)/shard_map/ppermute | solution.py:14
  83.3 4.1 %collective-permute-start.4 = (bf16[168,768]{1,0:T(8,128)(2,1)S(1)}, bf16[168,768]{1,0:T(8,128)(2,1)S(1)}, u32[]{:S(2)}, u32[]{:S(2)}) collective-permute-start(bf16[168,768]{1,0:T(8,128)(2,1)S(1)} %collective-permute-done.2), channel_id=1, source_target_pairs={{0,8},{8,16},{16,24},{24,32},{32,40},{40,48},{48,56},{56,0},{1,9},... | collective-permute-start | bytes 774152 | tf_op jit(solution)/shard_map/ppermute | solution.py:14
  87.4 3.1 %collective-permute-start.5 = (bf16[168,768]{1,0:T(8,128)(2,1)S(1)}, bf16[168,768]{1,0:T(8,128)(2,1)S(1)}, u32[]{:S(2)}, u32[]{:S(2)}) collective-permute-start(bf16[168,768]{1,0:T(8,128)(2,1)S(1)} %collective-permute-done.3), channel_id=1, source_target_pairs={{0,56},{8,0},{16,8},{24,16},{32,24},{40,32},{48,40},{56,48},{1,57}... | collective-permute-start | bytes 774152 | tf_op jit(solution)/shard_map/ppermute | solution.py:14
  90.6 0.7 constant_dynamic-update-slice_fusion.5
  91.3 0.7 constant_dynamic-update-slice_fusion.4
  92.0 0.9 collective-permute-done.4
  93.0 4.0 %collective-permute-start.6 = (bf16[80,768]{1,0:T(8,128)(2,1)S(1)}, bf16[80,768]{1,0:T(8,128)(2,1)S(1)}, u32[]{:S(2)}, u32[]{:S(2)}) collective-permute-start(bf16[80,768]{1,0:T(8,128)(2,1)S(1)} %slice.33), channel_id=1, source_target_pairs={{0,8},{8,16},{16,24},{24,32},{32,40},{40,48},{48,56},{56,0},{1,9},... | collective-permute-start | bytes 368648 | tf_op jit(solution)/shard_map/ppermute | solution.py:14
  97.1 3.3 %collective-permute-start.7 = (bf16[88,768]{1,0:T(8,128)(2,1)S(1)}, bf16[88,768]{1,0:T(8,128)(2,1)S(1)}, u32[]{:S(2)}, u32[]{:S(2)}) collective-permute-start(bf16[88,768]{1,0:T(8,128)(2,1)S(1)} %slice.34), channel_id=1, source_target_pairs={{0,56},{8,0},{16,8},{24,16},{32,24},{40,32},{48,40},{56,48},{1,57}... | collective-permute-start | bytes 405512 | tf_op jit(solution)/shard_map/ppermute | solution.py:14
  100.4 0.7 constant_dynamic-update-slice_fusion.3
  101.1 0.7 constant_dynamic-update-slice_fusion.2
  101.9 0.7 constant_dynamic-update-slice_fusion.1
  102.5 3.1 %collective-permute-done.7 = bf16[88,768]{1,0:T(8,128)(2,1)S(1)} collective-permute-done((bf16[88,768]{1,0:T(8,128)(2,1)S(1)}, bf16[88,768]{1,0:T(8,128)(2,1)S(1)}, u32[]{:S(2)}, u32[]{:S(2)}) %collective-permute-start.7) | collective-permute-done | bytes 135200 | tf_op jit(solution)/shard_map/ppermute | solution.py:14
  105.6 0.7 constant_dynamic-update-slice_fusion
  106.2 2.4 %fusion.27 = f32[256,768]{1,0:T(8,128)S(1)} fusion(bf16[1344,256]{1,0:T(8,128)(2,1)S(1)} %copy-done.5, bf16[1344,768]{1,0:T(8,128)(2,1)} %constant_dynamic-update-slice_fusion), kind=kOutput, calls=%fused_computation.63 | convolution fusion | flops 528482304 | bytes 3538944 | tf_op jit(solution)/shard_map/dot_general | solution.py:30
  108.6 0.9 copy-done.4
  109.5 1.6 convolution_convert_fusion
  111.1 8.9 %all-to-all-start.1 = ((bf16[8,168,384]{2,1,0:T(8,128)(2,1)}), bf16[8,168,384]{2,1,0:T(8,128)(2,1)S(1)}, u32[]{:S(2)}, u32[]{:S(2)}) async-start(bf16[8,168,384]{2,1,0:T(8,128)(2,1)} %bitcast.1), calls=%async_computation.1 | async-start | bytes 2064384 | tf_op jit(solution)/shard_map/all_to_all | solution.py:25
  120.1 2.1 %multiply_convert_fusion.2 = (bf16[256,384]{1,0:T(8,128)(2,1)S(1)}, bf16[256,384]{1,0:T(8,128)(2,1)S(1)}) fusion(f32[256,768]{1,0:T(8,128)} %copy-done.4, bf16[1344,256]{1,0:T(8,128)(2,1)} %fusion.10, bf16[1344,384]{1,0:T(8,128)(2,1)S(1)} %constant_dynamic-update-slice_fusion.9), kind=kOutput, calls=%fused_computation.26 | convolution fusion | flops 265519104 | bytes 2899968 | tf_op jit(solution)/shard_map/dot_general | solution.py:30
  122.2 0.7 convolution_convert_fusion.1
  123.0 1.9 %collective-permute-start.16 = (bf16[672,256]{1,0:T(8,128)(2,1)S(1)}, bf16[672,256]{1,0:T(8,128)(2,1)S(1)}, u32[]{:S(2)}, u32[]{:S(2)}) collective-permute-start(bf16[672,256]{1,0:T(8,128)(2,1)S(1)} %constant_dynamic-slice_fusion), channel_id=1, source_target_pairs={{0,1},{1,0},{2,3},{3,2},{4,5},{5,4},{6,7},{7,6},{8,9},{9,8},{10,11... | collective-permute-start | bytes 1032200 | tf_op jit(solution)/shard_map/ppermute | solution.py:14
  124.9 1.6 collective-permute-done.16
  126.6 0.1 add_convert_fusion.1
  126.7 3.4 %collective-permute-start.17 = (bf16[672,256]{1,0:T(8,128)(2,1)S(1)}, bf16[672,256]{1,0:T(8,128)(2,1)S(1)}, u32[]{:S(2)}, u32[]{:S(2)}) collective-permute-start(bf16[672,256]{1,0:T(8,128)(2,1)S(1)} %add_convert_fusion.1), channel_id=1, source_target_pairs={{0,2},{2,4},{4,6},{6,0},{1,3},{3,5},{5,7},{7,1},{8,10},{10,12},{12... | collective-permute-start | bytes 1032200 | tf_op jit(solution)/shard_map/ppermute | solution.py:14
  130.1 3.0 %collective-permute-start.18 = (bf16[672,256]{1,0:T(8,128)(2,1)S(1)}, bf16[672,256]{1,0:T(8,128)(2,1)S(1)}, u32[]{:S(2)}, u32[]{:S(2)}) collective-permute-start(bf16[672,256]{1,0:T(8,128)(2,1)S(1)} %add_convert_fusion.1), channel_id=1, source_target_pairs={{0,4},{2,6},{4,0},{6,2},{1,5},{3,7},{5,1},{7,3},{8,12},{10,14},{12... | collective-permute-start | bytes 1032200 | tf_op jit(solution)/shard_map/ppermute | solution.py:14
  133.1 4.1 %collective-permute-start.19 = (bf16[672,256]{1,0:T(8,128)(2,1)S(1)}, bf16[672,256]{1,0:T(8,128)(2,1)S(1)}, u32[]{:S(2)}, u32[]{:S(2)}) collective-permute-start(bf16[672,256]{1,0:T(8,128)(2,1)S(1)} %add_convert_fusion.1), channel_id=1, source_target_pairs={{0,6},{2,0},{4,2},{6,4},{1,7},{3,1},{5,3},{7,5},{8,14},{10,8},{12,... | collective-permute-start | bytes 1032200 | tf_op jit(solution)/shard_map/ppermute | solution.py:14
  137.2 2.3 %all-to-all-done.1 = bf16[8,168,384]{2,1,0:T(8,128)(2,1)S(1)} async-done(((bf16[8,168,384]{2,1,0:T(8,128)(2,1)}), bf16[8,168,384]{2,1,0:T(8,128)(2,1)S(1)}, u32[]{:S(2)}, u32[]{:S(2)}) %all-to-all-start.1) | async-done | bytes 1032224 | tf_op jit(solution)/shard_map/all_to_all | solution.py:25
  139.4 0.1 reduce_sum.21
  139.6 0.7 reshape.33
  140.3 4.2 %collective-permute-done.18 = bf16[672,256]{1,0:T(8,128)(2,1)S(1)} collective-permute-done((bf16[672,256]{1,0:T(8,128)(2,1)S(1)}, bf16[672,256]{1,0:T(8,128)(2,1)S(1)}, u32[]{:S(2)}, u32[]{:S(2)}) %collective-permute-start.18) | collective-permute-done | bytes 344096 | tf_op jit(solution)/shard_map/ppermute | solution.py:14
  144.4 6.2 %collective-permute-done.19 = bf16[672,256]{1,0:T(8,128)(2,1)S(1)} collective-permute-done((bf16[672,256]{1,0:T(8,128)(2,1)S(1)}, bf16[672,256]{1,0:T(8,128)(2,1)S(1)}, u32[]{:S(2)}, u32[]{:S(2)}) %collective-permute-start.19) | collective-permute-done | bytes 344096 | tf_op jit(solution)/shard_map/ppermute | solution.py:14
  150.7 0.2 add_convert_fusion
  150.8 1.9 %collective-permute-start.20 = (bf16[672,256]{1,0:T(8,128)(2,1)S(1)}, bf16[672,256]{1,0:T(8,128)(2,1)S(1)}, u32[]{:S(2)}, u32[]{:S(2)}) collective-permute-start(bf16[672,256]{1,0:T(8,128)(2,1)S(1)} %add_convert_fusion), channel_id=1, source_target_pairs={{0,1},{1,0},{2,3},{3,2},{4,5},{5,4},{6,7},{7,6},{8,9},{9,8},{10,11... | collective-permute-start | bytes 1032200 | tf_op jit(solution)/shard_map/ppermute | solution.py:14
  152.8 4.5 %all-to-all-start.2 = ((bf16[12,14,384]{2,1,0:T(8,128)(2,1)}), bf16[12,14,384]{2,1,0:T(8,128)(2,1)S(1)}, u32[]{:S(2)}, u32[]{:S(2)}) async-start(bf16[12,14,384]{2,1,0:T(8,128)(2,1)} %reshape.33), calls=%async_computation.2 | async-start | bytes 294912 | tf_op jit(solution)/shard_map/all_to_all | solution.py:25
  157.3 0.1 broadcast_select_fusion.1
  157.4 3.3 %fusion.11 = bf16[256,1344]{0,1:T(8,128)(2,1)} fusion(s32[1344]{0:T(1024)S(1)} %add.65, bf16[672,256]{1,0:T(8,128)(2,1)S(1)} %get-tuple-element.17, bf16[672,256]{1,0:T(8,128)(2,1)S(1)} %get-tuple-element.16), kind=kOutput, calls=%fused_computation.15 | convolution fusion | flops 928370688 | bytes 1381632 | tf_op jit(solution)/shard_map/dot_general | solution.py:30
  160.7 9.9 %all-to-all-done.2 = bf16[12,14,384]{2,1,0:T(8,128)(2,1)S(1)} async-done(((bf16[12,14,384]{2,1,0:T(8,128)(2,1)}), bf16[12,14,384]{2,1,0:T(8,128)(2,1)S(1)}, u32[]{:S(2)}, u32[]{:S(2)}) %all-to-all-start.2) | async-done | bytes 129056 | tf_op jit(solution)/shard_map/all_to_all | solution.py:25
  170.6 0.6 convert_reduce_fusion
  (41 shorter events, 0.3 us)
Async XLA Ops:
  0.6 18.3 %copy-start = (bf16[256,1344]{0,1:T(8,128)(2,1)S(1)}, bf16[256,1344]{0,1:T(8,128)(2,1)}, u32[]{:S(2)}) copy-start(bf16[256,1344]{0,1:T(8,128)(2,1)} %param.9) | copy-start | bytes 2064388
  2.3 36.2 %all-to-all-start = ((bf16[12,14,1152]{2,1,0:T(8,128)(2,1)}), bf16[12,14,1152]{2,1,0:T(8,128)(2,1)S(1)}, u32[]{:S(2)}, u32[]{:S(2)}) async-start(bf16[12,14,1152]{2,1,0:T(8,128)(2,1)} %broadcast_in_dim.2), calls=%async_computation | async-start | bytes 884736 | tf_op jit(solution)/shard_map/all_to_all | solution.py:19
  19.0 2.4 %copy-start.2 = (bf16[256,1344]{0,1:T(8,128)(2,1)S(1)}, bf16[256,1344]{0,1:T(8,128)(2,1)}, u32[]{:S(2)}) copy-start(bf16[256,1344]{0,1:T(8,128)(2,1)} %param.8) | copy-start | bytes 2064388
  21.3 29.8 %copy-start.3 = (s32[1344]{0:T(1024)S(1)}, s32[1344]{0:T(1024)}, u32[]{:S(2)}) copy-start(s32[1344]{0:T(1024)} %constant.47.clone) | copy-start | bytes 16132
  39.3 21.1 %collective-permute-start = (bf16[168,768]{1,0:T(8,128)(2,1)S(1)}, bf16[168,768]{1,0:T(8,128)(2,1)S(1)}, u32[]{:S(2)}, u32[]{:S(2)}) collective-permute-start(bf16[168,768]{1,0:T(8,128)(2,1)S(1)} %get-tuple-element.20), channel_id=1, source_target_pairs={{0,8},{8,16},{16,24},{24,32},{32,40},{40,48},{48,56},{56,0},{1,9},... | collective-permute-start | bytes 774152 | tf_op jit(solution)/shard_map/ppermute | solution.py:14
  42.8 21.6 %collective-permute-start.1 = (bf16[168,768]{1,0:T(8,128)(2,1)S(1)}, bf16[168,768]{1,0:T(8,128)(2,1)S(1)}, u32[]{:S(2)}, u32[]{:S(2)}) collective-permute-start(bf16[168,768]{1,0:T(8,128)(2,1)S(1)} %get-tuple-element.20), channel_id=1, source_target_pairs={{0,56},{8,0},{16,8},{24,16},{32,24},{40,32},{48,40},{56,48},{1,57}... | collective-permute-start | bytes 774152 | tf_op jit(solution)/shard_map/ppermute | solution.py:14
  45.2 8.2 %collective-permute-start.8 = (bf16[168,384]{1,0:T(8,128)(2,1)S(1)}, bf16[168,384]{1,0:T(8,128)(2,1)S(1)}, u32[]{:S(2)}, u32[]{:S(2)}) collective-permute-start(bf16[168,384]{1,0:T(8,128)(2,1)S(1)} %get-tuple-element.18), channel_id=1, source_target_pairs={{0,8},{8,16},{16,24},{24,32},{32,40},{40,48},{48,56},{56,0},{1,9},... | collective-permute-start | bytes 387080 | tf_op jit(solution)/shard_map/ppermute | solution.py:14
  48.7 8.6 %collective-permute-start.9 = (bf16[168,384]{1,0:T(8,128)(2,1)S(1)}, bf16[168,384]{1,0:T(8,128)(2,1)S(1)}, u32[]{:S(2)}, u32[]{:S(2)}) collective-permute-start(bf16[168,384]{1,0:T(8,128)(2,1)S(1)} %get-tuple-element.18), channel_id=1, source_target_pairs={{0,56},{8,0},{16,8},{24,16},{32,24},{40,32},{48,40},{56,48},{1,57}... | collective-permute-start | bytes 387080 | tf_op jit(solution)/shard_map/ppermute | solution.py:14
  53.4 14.1 %collective-permute-start.10 = (bf16[168,384]{1,0:T(8,128)(2,1)S(1)}, bf16[168,384]{1,0:T(8,128)(2,1)S(1)}, u32[]{:S(2)}, u32[]{:S(2)}) collective-permute-start(bf16[168,384]{1,0:T(8,128)(2,1)S(1)} %collective-permute-done.8), channel_id=1, source_target_pairs={{0,8},{8,16},{16,24},{24,32},{32,40},{40,48},{48,56},{56,0},{1,9},... | collective-permute-start | bytes 387080 | tf_op jit(solution)/shard_map/ppermute | solution.py:14
  57.3 15.0 %collective-permute-start.11 = (bf16[168,384]{1,0:T(8,128)(2,1)S(1)}, bf16[168,384]{1,0:T(8,128)(2,1)S(1)}, u32[]{:S(2)}, u32[]{:S(2)}) collective-permute-start(bf16[168,384]{1,0:T(8,128)(2,1)S(1)} %collective-permute-done.9), channel_id=1, source_target_pairs={{0,56},{8,0},{16,8},{24,16},{32,24},{40,32},{48,40},{56,48},{1,57}... | collective-permute-start | bytes 387080 | tf_op jit(solution)/shard_map/ppermute | solution.py:14
  60.5 22.8 %collective-permute-start.2 = (bf16[168,768]{1,0:T(8,128)(2,1)S(1)}, bf16[168,768]{1,0:T(8,128)(2,1)S(1)}, u32[]{:S(2)}, u32[]{:S(2)}) collective-permute-start(bf16[168,768]{1,0:T(8,128)(2,1)S(1)} %collective-permute-done), channel_id=1, source_target_pairs={{0,8},{8,16},{16,24},{24,32},{32,40},{40,48},{48,56},{56,0},{1,9},... | collective-permute-start | bytes 774152 | tf_op jit(solution)/shard_map/ppermute | solution.py:14
  64.4 23.0 %collective-permute-start.3 = (bf16[168,768]{1,0:T(8,128)(2,1)S(1)}, bf16[168,768]{1,0:T(8,128)(2,1)S(1)}, u32[]{:S(2)}, u32[]{:S(2)}) collective-permute-start(bf16[168,768]{1,0:T(8,128)(2,1)S(1)} %collective-permute-done.1), channel_id=1, source_target_pairs={{0,56},{8,0},{16,8},{24,16},{32,24},{40,32},{48,40},{56,48},{1,57}... | collective-permute-start | bytes 774152 | tf_op jit(solution)/shard_map/ppermute | solution.py:14
  67.6 8.6 %collective-permute-start.12 = (bf16[168,384]{1,0:T(8,128)(2,1)S(1)}, bf16[168,384]{1,0:T(8,128)(2,1)S(1)}, u32[]{:S(2)}, u32[]{:S(2)}) collective-permute-start(bf16[168,384]{1,0:T(8,128)(2,1)S(1)} %collective-permute-done.10), channel_id=1, source_target_pairs={{0,8},{8,16},{16,24},{24,32},{32,40},{40,48},{48,56},{56,0},{1,9},... | collective-permute-start | bytes 387080 | tf_op jit(solution)/shard_map/ppermute | solution.py:14
  72.3 8.0 %collective-permute-start.13 = (bf16[168,384]{1,0:T(8,128)(2,1)S(1)}, bf16[168,384]{1,0:T(8,128)(2,1)S(1)}, u32[]{:S(2)}, u32[]{:S(2)}) collective-permute-start(bf16[168,384]{1,0:T(8,128)(2,1)S(1)} %collective-permute-done.11), channel_id=1, source_target_pairs={{0,56},{8,0},{16,8},{24,16},{32,24},{40,32},{48,40},{56,48},{1,57}... | collective-permute-start | bytes 387080 | tf_op jit(solution)/shard_map/ppermute | solution.py:14
  75.4 30.8 %copy-start.5 = (bf16[1344,256]{1,0:T(8,128)(2,1)S(1)}, bf16[1344,256]{1,0:T(8,128)(2,1)}, u32[]{:S(2)}) copy-start(bf16[1344,256]{1,0:T(8,128)(2,1)} %fusion.9) | copy-start | bytes 2064388
  76.2 43.9 %collective-permute-start.14 = (bf16[80,384]{1,0:T(8,128)(2,1)S(1)}, bf16[80,384]{1,0:T(8,128)(2,1)S(1)}, u32[]{:S(2)}, u32[]{:S(2)}) collective-permute-start(bf16[80,384]{1,0:T(8,128)(2,1)S(1)} %slice.36), channel_id=1, source_target_pairs={{0,8},{8,16},{16,24},{24,32},{32,40},{40,48},{48,56},{56,0},{1,9},... | collective-permute-start | bytes 184328 | tf_op jit(solution)/shard_map/ppermute | solution.py:14
  80.3 39.7 %collective-permute-start.15 = (bf16[88,384]{1,0:T(8,128)(2,1)S(1)}, bf16[88,384]{1,0:T(8,128)(2,1)S(1)}, u32[]{:S(2)}, u32[]{:S(2)}) collective-permute-start(bf16[88,384]{1,0:T(8,128)(2,1)S(1)} %slice.37), channel_id=1, source_target_pairs={{0,56},{8,0},{16,8},{24,16},{32,24},{40,32},{48,40},{56,48},{1,57}... | collective-permute-start | bytes 202760 | tf_op jit(solution)/shard_map/ppermute | solution.py:14
  83.3 9.7 %collective-permute-start.4 = (bf16[168,768]{1,0:T(8,128)(2,1)S(1)}, bf16[168,768]{1,0:T(8,128)(2,1)S(1)}, u32[]{:S(2)}, u32[]{:S(2)}) collective-permute-start(bf16[168,768]{1,0:T(8,128)(2,1)S(1)} %collective-permute-done.2), channel_id=1, source_target_pairs={{0,8},{8,16},{16,24},{24,32},{32,40},{40,48},{48,56},{56,0},{1,9},... | collective-permute-start | bytes 774152 | tf_op jit(solution)/shard_map/ppermute | solution.py:14
  87.4 9.6 %collective-permute-start.5 = (bf16[168,768]{1,0:T(8,128)(2,1)S(1)}, bf16[168,768]{1,0:T(8,128)(2,1)S(1)}, u32[]{:S(2)}, u32[]{:S(2)}) collective-permute-start(bf16[168,768]{1,0:T(8,128)(2,1)S(1)} %collective-permute-done.3), channel_id=1, source_target_pairs={{0,56},{8,0},{16,8},{24,16},{32,24},{40,32},{48,40},{56,48},{1,57}... | collective-permute-start | bytes 774152 | tf_op jit(solution)/shard_map/ppermute | solution.py:14
  93.0 8.9 %collective-permute-start.6 = (bf16[80,768]{1,0:T(8,128)(2,1)S(1)}, bf16[80,768]{1,0:T(8,128)(2,1)S(1)}, u32[]{:S(2)}, u32[]{:S(2)}) collective-permute-start(bf16[80,768]{1,0:T(8,128)(2,1)S(1)} %slice.33), channel_id=1, source_target_pairs={{0,8},{8,16},{16,24},{24,32},{32,40},{40,48},{48,56},{56,0},{1,9},... | collective-permute-start | bytes 368648 | tf_op jit(solution)/shard_map/ppermute | solution.py:14
  97.1 8.5 %collective-permute-start.7 = (bf16[88,768]{1,0:T(8,128)(2,1)S(1)}, bf16[88,768]{1,0:T(8,128)(2,1)S(1)}, u32[]{:S(2)}, u32[]{:S(2)}) collective-permute-start(bf16[88,768]{1,0:T(8,128)(2,1)S(1)} %slice.34), channel_id=1, source_target_pairs={{0,56},{8,0},{16,8},{24,16},{32,24},{40,32},{48,40},{56,48},{1,57}... | collective-permute-start | bytes 405512 | tf_op jit(solution)/shard_map/ppermute | solution.py:14
  101.9 7.7 %copy-start.6 = (bf16[1344,256]{1,0:T(8,128)(2,1)S(1)}, bf16[1344,256]{1,0:T(8,128)(2,1)}, u32[]{:S(2)}) copy-start(bf16[1344,256]{1,0:T(8,128)(2,1)} %fusion.8) | copy-start | bytes 2064388
  108.6 0.9 copy-start.4
  111.1 28.3 %all-to-all-start.1 = ((bf16[8,168,384]{2,1,0:T(8,128)(2,1)}), bf16[8,168,384]{2,1,0:T(8,128)(2,1)S(1)}, u32[]{:S(2)}, u32[]{:S(2)}) async-start(bf16[8,168,384]{2,1,0:T(8,128)(2,1)} %bitcast.1), calls=%async_computation.1 | async-start | bytes 2064384 | tf_op jit(solution)/shard_map/all_to_all | solution.py:25
  120.1 2.2 %copy-start.1 = (bf16[1344,768]{1,0:T(8,128)(2,1)S(1)}, bf16[1344,768]{1,0:T(8,128)(2,1)}, u32[]{:S(2)}) copy-start(bf16[1344,768]{1,0:T(8,128)(2,1)} %constant_dynamic-update-slice_fusion) | copy-start | bytes 6193156
  123.0 3.5 %collective-permute-start.16 = (bf16[672,256]{1,0:T(8,128)(2,1)S(1)}, bf16[672,256]{1,0:T(8,128)(2,1)S(1)}, u32[]{:S(2)}, u32[]{:S(2)}) collective-permute-start(bf16[672,256]{1,0:T(8,128)(2,1)S(1)} %constant_dynamic-slice_fusion), channel_id=1, source_target_pairs={{0,1},{1,0},{2,3},{3,2},{4,5},{5,4},{6,7},{7,6},{8,9},{9,8},{10,11... | collective-permute-start | bytes 1032200 | tf_op jit(solution)/shard_map/ppermute | solution.py:14
  126.7 13.6 %collective-permute-start.17 = (bf16[672,256]{1,0:T(8,128)(2,1)S(1)}, bf16[672,256]{1,0:T(8,128)(2,1)S(1)}, u32[]{:S(2)}, u32[]{:S(2)}) collective-permute-start(bf16[672,256]{1,0:T(8,128)(2,1)S(1)} %add_convert_fusion.1), channel_id=1, source_target_pairs={{0,2},{2,4},{4,6},{6,0},{1,3},{3,5},{5,7},{7,1},{8,10},{10,12},{12... | collective-permute-start | bytes 1032200 | tf_op jit(solution)/shard_map/ppermute | solution.py:14
  130.1 14.4 %collective-permute-start.18 = (bf16[672,256]{1,0:T(8,128)(2,1)S(1)}, bf16[672,256]{1,0:T(8,128)(2,1)S(1)}, u32[]{:S(2)}, u32[]{:S(2)}) collective-permute-start(bf16[672,256]{1,0:T(8,128)(2,1)S(1)} %add_convert_fusion.1), channel_id=1, source_target_pairs={{0,4},{2,6},{4,0},{6,2},{1,5},{3,7},{5,1},{7,3},{8,12},{10,14},{12... | collective-permute-start | bytes 1032200 | tf_op jit(solution)/shard_map/ppermute | solution.py:14
  133.1 17.6 %collective-permute-start.19 = (bf16[672,256]{1,0:T(8,128)(2,1)S(1)}, bf16[672,256]{1,0:T(8,128)(2,1)S(1)}, u32[]{:S(2)}, u32[]{:S(2)}) collective-permute-start(bf16[672,256]{1,0:T(8,128)(2,1)S(1)} %add_convert_fusion.1), channel_id=1, source_target_pairs={{0,6},{2,0},{4,2},{6,4},{1,7},{3,1},{5,3},{7,5},{8,14},{10,8},{12,... | collective-permute-start | bytes 1032200 | tf_op jit(solution)/shard_map/ppermute | solution.py:14
  150.8 6.5 %collective-permute-start.20 = (bf16[672,256]{1,0:T(8,128)(2,1)S(1)}, bf16[672,256]{1,0:T(8,128)(2,1)S(1)}, u32[]{:S(2)}, u32[]{:S(2)}) collective-permute-start(bf16[672,256]{1,0:T(8,128)(2,1)S(1)} %add_convert_fusion), channel_id=1, source_target_pairs={{0,1},{1,0},{2,3},{3,2},{4,5},{5,4},{6,7},{7,6},{8,9},{9,8},{10,11... | collective-permute-start | bytes 1032200 | tf_op jit(solution)/shard_map/ppermute | solution.py:14
  152.8 17.8 %all-to-all-start.2 = ((bf16[12,14,384]{2,1,0:T(8,128)(2,1)}), bf16[12,14,384]{2,1,0:T(8,128)(2,1)S(1)}, u32[]{:S(2)}, u32[]{:S(2)}) async-start(bf16[12,14,384]{2,1,0:T(8,128)(2,1)} %reshape.33), calls=%async_computation.2 | async-start | bytes 294912 | tf_op jit(solution)/shard_map/all_to_all | solution.py:25
where the time goes:
time: 172 us; the launch traced here: 171 us
  starting transfers between devices  97.1 us (56%)
  waiting for transfers between devices  43.2 us (25%)
  matrix products  17.2 us (10%)
  local copies, waits for them, and re-layouts  9.3 us (5%)
  other arithmetic  3.34 us (2%)
    ppermute x21, starting transfers between devices, shifted(): lax.ppermute(array, axis, [(k, (k + step) % peers) for k in range(peers)])  68.5 us
    ppermute x21, waiting for transfers between devices, shifted(): lax.ppermute(array, axis, [(k, (k + step) % peers) for k in range(peers)])  16.2 us
    all_to_all x1, starting transfers between devices, sent_to_all(): lax.all_to_all(jnp.broadcast_to(array[None], (peers, *array.shape)), axis...  15.2 us
    all_to_all x1, waiting for transfers between devices, sent_to_all(): lax.all_to_all(jnp.broadcast_to(array[None], (peers, *array.shape)), axis...  14.8 us
    all_to_all x2, starting transfers between devices, exchanged(): got = lax.all_to_all(parts, axis, 0, 0, tiled=True)  13.4 us
    all_to_all x2, waiting for transfers between devices, exchanged(): got = lax.all_to_all(parts, axis, 0, 0, tiled=True)  12.2 us
    dot_general x3, matrix products, contract_rows(): lax.dot_general(left, right, (((0,), (0,)), ((), ())), preferred_element_...  7.83 us
    dot_general x4, matrix products, contract_cols(): lax.dot_general(left, right, (((1,), (1,)), ((), ())), preferred_element_...  7.78 us
  transfers between devices with their start and end apart: 24, of which 9 were waited for; matrix products, arithmetic and copies ran while one was open for 15% of the time, Pallas kernels for 0%

commit v1 on v0

--- a/solution.py
+++ b/solution.py
@@ -49,20 +49,39 @@
     return (source[:, None] == spot).astype(jnp.bfloat16)
 
 
-def around(blocks, axis):
+def swung(array, axis, step):
     peers = lax.axis_size(axis)
-    split = blocks[0].shape[0] // 16 * 8
-    ups = downs = blocks
-    parts, order = [[b] for b in blocks], [0]
+    ways = [(core, step if core == 0 else -step) for core in range(2)]
+    pairs = [
+        (2 * k + core, 2 * ((k + way) % peers) + core) for k in range(peers) for core, way in ways
+    ]
+    return lax.ppermute(array, (axis, "core"), pairs)
+
+
+def around(block, axis, widths):
+    peers = lax.axis_size(axis)
+    rows = block.shape[0]
+    split = rows // 16 * 8
+    place = lax.axis_index(axis)
+    way = 1 - 2 * lax.axis_index("core")
+    ends = np.cumsum(widths)
+    wholes = [jnp.zeros((peers, rows, w), block.dtype) for w in widths]
+
+    def put(part, owner, start):
+        owner = (owner + peers) % peers
+        for k, (end, w) in enumerate(zip(ends, widths)):
+            piece = part[None, :, end - w : end]
+            wholes[k] = lax.dynamic_update_slice(wholes[k], piece, (owner, start, 0))
+
+    put(block, place, 0)
+    up = down = block
     for step in range(1, peers // 2):
-        moved = [(shifted(u, axis, 1), shifted(d, axis, -1)) for u, d in zip(ups, downs)]
-        ups, downs = zip(*moved)
-        for held, pair in zip(parts, moved):
-            held += pair
-        order += [-step % peers, step]
-    for held, u, d in zip(parts, ups, downs):
-        held += [shifted(u[:split], axis, 1), shifted(d[split:], axis, -1)]
-    return [jnp.concatenate(held) for held in parts], order + [peers // 2]
+        up, down = swung(up, axis, 1), swung(down, axis, -1)
+        put(up, place - step * way, 0)
+        put(down, place + step * way, 0)
+    put(swung(up[:split], axis, 1), place + peers // 2, 0)
+    put(swung(down[split:], axis, -1), place + peers // 2, split)
+    return [w.reshape(peers * rows, -1) for w in wholes]
 
 
 def summed_over_tp(partial, after):
@@ -89,24 +108,16 @@
     outer, inner = (lax.axis_size(a) for a in FS)
     rows, units = gate_weight.shape
     width = tokens.shape[1]
-    place = lax.axis_index("fs_1")
-
     weights = jnp.concatenate([gate_weight, up_weight, down_weight.T], axis=1)
     weights = sent_to_all(weights, "fs_0").reshape(outer * rows, 3 * units)
-    (gate_up, down), order = around((weights[:, : 2 * units], weights[:, 2 * units :]), "fs_1")
+    gate_up, down = around(weights, "fs_1", (2 * units, units))
 
-    spot = inner_first(width, outer, inner)
-    block = (jnp.asarray(order, jnp.int32) + place) % inner
-    near = (block[:, None] * rows + spot[: outer * rows][None, :]).reshape(-1)
-    here = picked(near)
-    near_tokens = contract_cols(here, tokens).astype(jnp.bfloat16)
-    near_cotangent = contract_cols(here, cotangent).astype(jnp.bfloat16)
-    turned_cotangent = contract_cols(picked(spot), cotangent).astype(jnp.bfloat16)
-    near_tokens, near_cotangent, turned_cotangent = lax.optimization_barrier(
-        (near_tokens, near_cotangent, turned_cotangent)
-    )
+    turn = lax.optimization_barrier(picked(inner_first(width, outer, inner)))
+    turned_tokens = contract_cols(turn, tokens).astype(jnp.bfloat16)
+    turned_cotangent = contract_cols(turn, cotangent).astype(jnp.bfloat16)
+    turned_tokens, turned_cotangent = lax.optimization_barrier((turned_tokens, turned_cotangent))
 
-    both = contract_rows(near_tokens, gate_up)
+    both = contract_rows(turned_tokens, gate_up)
     gate_pre, up_pre = both[:, :units], both[:, units:]
     sigmoid_gate = jax.nn.sigmoid(gate_pre)
     activated = gate_pre * sigmoid_gate
@@ -116,7 +127,7 @@
     terms = terms.astype(jnp.bfloat16).reshape(inner, outer * rows, units)
     terms = exchanged(terms, "fs_1").astype(jnp.bfloat16).reshape(outer, rows, units)
 
-    hidden_grad = contract_rows(near_cotangent, down)
+    hidden_grad = contract_rows(turned_cotangent, down)
     gate_pre_grad = (
         hidden_grad * up_pre * sigmoid_gate * (1.0 + gate_pre * (1.0 - sigmoid_gate))
     ).astype(jnp.bfloat16)
@@ -124,7 +135,7 @@
     partial = contract_cols(gate_up, jnp.concatenate([gate_pre_grad, up_pre_grad], axis=1))
     total = summed_over_tp(partial.astype(jnp.bfloat16), terms)
     down_grad = exchanged(terms, "fs_0").T
-    input_grad = contract_rows(total, here).astype(jnp.bfloat16)
+    input_grad = contract_rows(total, turn).astype(jnp.bfloat16)
     return (input_grad, down_grad)
 
 

time: 172 us -> 155 us (0.901)
  the two profiles are of different devices: /device:TPU:10 before, /device:TPU:8 now
where the time goes in v1:
time: 155 us; the launch traced here: 154 us
  waiting for transfers between devices  65.1 us (42%)
  starting transfers between devices  64.2 us (41%)
  matrix products  15.4 us (10%)
  other arithmetic  5.11 us (3%)
  local copies, waits for them, and re-layouts  3.25 us (2%)
    ppermute x8, waiting for transfers between devices, swung(): return lax.ppermute(array, (axis, 'core'), pairs)  28.4 us
    ppermute x8, starting transfers between devices, swung(): return lax.ppermute(array, (axis, 'core'), pairs)  22.5 us
    all_to_all x1, starting transfers between devices, sent_to_all(): lax.all_to_all(jnp.broadcast_to(array[None], (peers, *array.shape)), axis...  15.2 us
    ppermute x5, starting transfers between devices, shifted(): lax.ppermute(array, axis, [(k, (k + step) % peers) for k in range(peers)])  14 us
    all_to_all x2, waiting for transfers between devices, exchanged(): got = lax.all_to_all(parts, axis, 0, 0, tiled=True)  13.6 us
    all_to_all x2, starting transfers between devices, exchanged(): got = lax.all_to_all(parts, axis, 0, 0, tiled=True)  12.5 us
    all_to_all x1, waiting for transfers between devices, sent_to_all(): lax.all_to_all(jnp.broadcast_to(array[None], (peers, *array.shape)), axis...  12.2 us
    ppermute x5, waiting for transfers between devices, shifted(): lax.ppermute(array, axis, [(k, (k + step) % peers) for k in range(peers)])  10.7 us
  transfers between devices with their start and end apart: 16, of which 12 were waited for; matrix products, arithmetic and copies ran while one was open for 12% of the time, Pallas kernels for 0%

profile of v1, /device:TPU:8, one launch (start us, length us, event | category | flops | bytes accessed | tf_op | source)
XLA Modules:
  0.0 154.1 jit_solution(15198842999616815602)
XLA Ops:
  0.6 0.0 copy-start
  0.6 0.8 pad_maximum_fusion
  1.5 0.8 broadcast_in_dim.68
  2.3 15.2 %all-to-all-start = ((bf16[12,14,1152]{2,1,0:T(8,128)(2,1)}), bf16[12,14,1152]{2,1,0:T(8,128)(2,1)S(1)}, u32[]{:S(2)}, u32[]{:S(2)}) async-start(bf16[12,14,1152]{2,1,0:T(8,128)(2,1)} %broadcast_in_dim.68), calls=%async_computation | async-start | bytes 884736 | tf_op jit(solution)/shard_map/all_to_all | solution.py:19
  17.4 3.2 %fusion = bf16[1344,1344]{1,0:T(8,128)(2,1)} fusion(s32[1344]{0:T(1024)} %constant.78.clone), kind=kLoop, calls=%fused_computation.1 | loop fusion | flops 3612672 | bytes 3618048 | tf_op jit(solution)/shard_map/convert_element_type | solution.py:49
  20.6 0.0 copy-done
  20.6 0.0 copy-start.1
  20.6 4.3 %convolution_convert_fusion.3 = bf16[1344,256]{1,0:T(8,128)(2,1)} fusion(bf16[1344,1344]{1,0:T(8,128)(2,1)} %fusion, bf16[256,1344]{0,1:T(8,128)(2,1)S(1)} %copy-done), kind=kOutput, calls=%fused_computation.5 | convolution fusion | flops 925188096 | bytes 4988928 | tf_op jit(solution)/shard_map/dot_general | solution.py:36
  24.9 0.0 copy-done.1
  24.9 0.0 copy-done.4
  24.9 1.2 convolution_convert_fusion.4
  26.2 12.2 %all-to-all-done = bf16[12,14,1152]{2,1,0:T(8,128)(2,1)S(1)} async-done(((bf16[12,14,1152]{2,1,0:T(8,128)(2,1)}), bf16[12,14,1152]{2,1,0:T(8,128)(2,1)S(1)}, u32[]{:S(2)}, u32[]{:S(2)}) %all-to-all-start) | async-done | bytes 387104 | tf_op jit(solution)/shard_map/all_to_all | solution.py:19
  38.5 0.1 reshape.21
  38.6 2.4 %collective-permute-start.1 = (bf16[168,1152]{1,0:T(8,128)(2,1)S(1)}, bf16[168,1152]{1,0:T(8,128)(2,1)S(1)}, u32[]{:S(2)}, u32[]{:S(2)}) collective-permute-start(bf16[168,1152]{1,0:T(8,128)(2,1)S(1)} %reshape.21), channel_id=1, source_target_pairs={{0,56},{1,9},{8,0},{9,17},{16,8},{17,25},{24,16},{25,33},{32,24},{... | collective-permute-start | bytes 1161224 | tf_op jit(solution)/shard_map/ppermute | solution.py:58
  41.0 3.5 %collective-permute-start = (bf16[168,1152]{1,0:T(8,128)(2,1)S(1)}, bf16[168,1152]{1,0:T(8,128)(2,1)S(1)}, u32[]{:S(2)}, u32[]{:S(2)}) collective-permute-start(bf16[168,1152]{1,0:T(8,128)(2,1)S(1)} %reshape.21), channel_id=1, source_target_pairs={{0,8},{1,57},{8,16},{9,1},{16,24},{17,9},{24,32},{25,17},{32,40},{... | collective-permute-start | bytes 1161224 | tf_op jit(solution)/shard_map/ppermute | solution.py:58
  44.5 0.1 broadcast_in_dim.78
  44.6 0.1 broadcast_in_dim.67
  44.8 7.0 %collective-permute-done.1 = bf16[168,1152]{1,0:T(8,128)(2,1)S(1)} collective-permute-done((bf16[168,1152]{1,0:T(8,128)(2,1)S(1)}, bf16[168,1152]{1,0:T(8,128)(2,1)S(1)}, u32[]{:S(2)}, u32[]{:S(2)}) %collective-permute-start.1) | collective-permute-done | bytes 387104 | tf_op jit(solution)/shard_map/ppermute | solution.py:58
  51.8 3.2 %collective-permute-start.3 = (bf16[168,1152]{1,0:T(8,128)(2,1)S(1)}, bf16[168,1152]{1,0:T(8,128)(2,1)S(1)}, u32[]{:S(2)}, u32[]{:S(2)}) collective-permute-start(bf16[168,1152]{1,0:T(8,128)(2,1)S(1)} %collective-permute-done.1), channel_id=1, source_target_pairs={{0,56},{1,9},{8,0},{9,17},{16,8},{17,25},{24,16},{25,33},{32,24},{... | collective-permute-start | bytes 1161224 | tf_op jit(solution)/shard_map/ppermute | solution.py:58
  55.0 0.0 collective-permute-done
  55.0 2.6 %collective-permute-start.2 = (bf16[168,1152]{1,0:T(8,128)(2,1)S(1)}, bf16[168,1152]{1,0:T(8,128)(2,1)S(1)}, u32[]{:S(2)}, u32[]{:S(2)}) collective-permute-start(bf16[168,1152]{1,0:T(8,128)(2,1)S(1)} %collective-permute-done), channel_id=1, source_target_pairs={{0,8},{1,57},{8,16},{9,1},{16,24},{17,9},{24,32},{25,17},{32,40},{... | collective-permute-start | bytes 1161224 | tf_op jit(solution)/shard_map/ppermute | solution.py:58
  57.8 7.5 %collective-permute-done.3 = bf16[168,1152]{1,0:T(8,128)(2,1)S(1)} collective-permute-done((bf16[168,1152]{1,0:T(8,128)(2,1)S(1)}, bf16[168,1152]{1,0:T(8,128)(2,1)S(1)}, u32[]{:S(2)}, u32[]{:S(2)}) %collective-permute-start.3) | collective-permute-done | bytes 387104 | tf_op jit(solution)/shard_map/ppermute | solution.py:58
  65.2 3.1 %collective-permute-start.5 = (bf16[168,1152]{1,0:T(8,128)(2,1)S(1)}, bf16[168,1152]{1,0:T(8,128)(2,1)S(1)}, u32[]{:S(2)}, u32[]{:S(2)}) collective-permute-start(bf16[168,1152]{1,0:T(8,128)(2,1)S(1)} %collective-permute-done.3), channel_id=1, source_target_pairs={{0,56},{1,9},{8,0},{9,17},{16,8},{17,25},{24,16},{25,33},{32,24},{... | collective-permute-start | bytes 1161224 | tf_op jit(solution)/shard_map/ppermute | solution.py:58
  68.4 1.9 %collective-permute-done.2 = bf16[168,1152]{1,0:T(8,128)(2,1)S(1)} collective-permute-done((bf16[168,1152]{1,0:T(8,128)(2,1)S(1)}, bf16[168,1152]{1,0:T(8,128)(2,1)S(1)}, u32[]{:S(2)}, u32[]{:S(2)}) %collective-permute-start.2) | collective-permute-done | bytes 387104 | tf_op jit(solution)/shard_map/ppermute | solution.py:58
  70.3 1.9 %collective-permute-start.4 = (bf16[168,1152]{1,0:T(8,128)(2,1)S(1)}, bf16[168,1152]{1,0:T(8,128)(2,1)S(1)}, u32[]{:S(2)}, u32[]{:S(2)}) collective-permute-start(bf16[168,1152]{1,0:T(8,128)(2,1)S(1)} %collective-permute-done.2), channel_id=1, source_target_pairs={{0,8},{1,57},{8,16},{9,1},{16,24},{17,9},{24,32},{25,17},{32,40},{... | collective-permute-start | bytes 1161224 | tf_op jit(solution)/shard_map/ppermute | solution.py:58
  72.3 5.6 %collective-permute-done.5 = bf16[168,1152]{1,0:T(8,128)(2,1)S(1)} collective-permute-done((bf16[168,1152]{1,0:T(8,128)(2,1)S(1)}, bf16[168,1152]{1,0:T(8,128)(2,1)S(1)}, u32[]{:S(2)}, u32[]{:S(2)}) %collective-permute-start.5) | collective-permute-done | bytes 387104 | tf_op jit(solution)/shard_map/ppermute | solution.py:58
  77.9 3.1 %collective-permute-start.7 = (bf16[88,1152]{1,0:T(8,128)(2,1)S(1)}, bf16[88,1152]{1,0:T(8,128)(2,1)S(1)}, u32[]{:S(2)}, u32[]{:S(2)}) collective-permute-start(bf16[88,1152]{1,0:T(8,128)(2,1)S(1)} %slice.97), channel_id=1, source_target_pairs={{0,56},{1,9},{8,0},{9,17},{16,8},{17,25},{24,16},{25,33},{32,24},{... | collective-permute-start | bytes 608264 | tf_op jit(solution)/shard_map/ppermute | solution.py:58
  81.0 1.0 collective-permute-done.4
  82.0 2.7 %collective-permute-start.6 = (bf16[80,1152]{1,0:T(8,128)(2,1)S(1)}, bf16[80,1152]{1,0:T(8,128)(2,1)S(1)}, u32[]{:S(2)}, u32[]{:S(2)}) collective-permute-start(bf16[80,1152]{1,0:T(8,128)(2,1)S(1)} %slice.95), channel_id=1, source_target_pairs={{0,8},{1,57},{8,16},{9,1},{16,24},{17,9},{24,32},{25,17},{32,40},{... | collective-permute-start | bytes 552968 | tf_op jit(solution)/shard_map/ppermute | solution.py:58
  84.8 5.6 %collective-permute-done.6 = bf16[80,1152]{1,0:T(8,128)(2,1)S(1)} collective-permute-done((bf16[80,1152]{1,0:T(8,128)(2,1)S(1)}, bf16[80,1152]{1,0:T(8,128)(2,1)S(1)}, u32[]{:S(2)}, u32[]{:S(2)}) %collective-permute-start.6) | collective-permute-done | bytes 184352 | tf_op jit(solution)/shard_map/ppermute | solution.py:58
  90.3 0.0 copy-start.6
  90.4 0.0 collective-permute-done.7
  90.4 0.0 copy-start.2
  90.4 0.8 fusion.30
  91.2 0.0 copy-start.5
  91.3 0.9 copy-done.5
  92.1 0.0 copy-done.6
  92.1 1.6 %convolution_convert_fusion = bf16[1344,384]{1,0:T(8,128)(2,1)} fusion(bf16[1344,256]{1,0:T(8,128)(2,1)S(1)} %copy-done.6, f32[256,768]{1,0:T(8,128)S(1)} %fusion.30), kind=kOutput, calls=%fused_computation.2 | convolution fusion | flops 265347072 | bytes 2506752 | tf_op jit(solution)/shard_map/dot_general | solution.py:126
  93.7 0.0 copy-done.2
  93.7 8.8 %all-to-all-start.1 = ((bf16[8,168,384]{2,1,0:T(8,128)(2,1)}), bf16[8,168,384]{2,1,0:T(8,128)(2,1)S(1)}, u32[]{:S(2)}, u32[]{:S(2)}) async-start(bf16[8,168,384]{2,1,0:T(8,128)(2,1)} %bitcast.91), calls=%async_computation.1 | async-start | bytes 2064384 | tf_op jit(solution)/shard_map/all_to_all | solution.py:25
  102.6 0.0 copy-start.3
  102.6 2.1 %multiply_convert_fusion.2 = (bf16[256,384]{1,0:T(8,128)(2,1)S(1)}, bf16[256,384]{1,0:T(8,128)(2,1)S(1)}) fusion(f32[256,768]{1,0:T(8,128)} %copy-done.5, bf16[1344,256]{1,0:T(8,128)(2,1)} %convolution_convert_fusion.3, bf16[1344,384]{1,0:T(8,128)(2,1)S(1)} %bitcast.90), kind=kOutput, calls=%fused_computation.17 | convolution fusion | flops 265519104 | bytes 2899968 | tf_op jit(solution)/shard_map/dot_general | solution.py:30
  104.7 0.0 copy-done.3
  104.7 0.7 convolution_convert_fusion.2
  105.5 1.9 %collective-permute-start.8 = (bf16[672,256]{1,0:T(8,128)(2,1)S(1)}, bf16[672,256]{1,0:T(8,128)(2,1)S(1)}, u32[]{:S(2)}, u32[]{:S(2)}) collective-permute-start(bf16[672,256]{1,0:T(8,128)(2,1)S(1)} %constant_dynamic-slice_fusion), channel_id=1, source_target_pairs={{0,1},{1,0},{2,3},{3,2},{4,5},{5,4},{6,7},{7,6},{8,9},{9,8},{10,11... | collective-permute-start | bytes 1032200 | tf_op jit(solution)/shard_map/ppermute | solution.py:14
  107.4 1.6 %collective-permute-done.8 = bf16[672,256]{1,0:T(8,128)(2,1)S(1)} collective-permute-done((bf16[672,256]{1,0:T(8,128)(2,1)S(1)}, bf16[672,256]{1,0:T(8,128)(2,1)S(1)}, u32[]{:S(2)}, u32[]{:S(2)}) %collective-permute-start.8) | collective-permute-done | bytes 344096 | tf_op jit(solution)/shard_map/ppermute | solution.py:14
  109.0 0.1 add_convert_fusion.1
  109.1 4.7 %collective-permute-start.11 = (bf16[672,256]{1,0:T(8,128)(2,1)S(1)}, bf16[672,256]{1,0:T(8,128)(2,1)S(1)}, u32[]{:S(2)}, u32[]{:S(2)}) collective-permute-start(bf16[672,256]{1,0:T(8,128)(2,1)S(1)} %add_convert_fusion.1), channel_id=1, source_target_pairs={{0,6},{2,0},{4,2},{6,4},{1,7},{3,1},{5,3},{7,5},{8,14},{10,8},{12,... | collective-permute-start | bytes 1032200 | tf_op jit(solution)/shard_map/ppermute | solution.py:14
  113.8 2.7 %collective-permute-start.10 = (bf16[672,256]{1,0:T(8,128)(2,1)S(1)}, bf16[672,256]{1,0:T(8,128)(2,1)S(1)}, u32[]{:S(2)}, u32[]{:S(2)}) collective-permute-start(bf16[672,256]{1,0:T(8,128)(2,1)S(1)} %add_convert_fusion.1), channel_id=1, source_target_pairs={{0,4},{2,6},{4,0},{6,2},{1,5},{3,7},{5,1},{7,3},{8,12},{10,14},{12... | collective-permute-start | bytes 1032200 | tf_op jit(solution)/shard_map/ppermute | solution.py:14
  116.5 2.8 %collective-permute-start.9 = (bf16[672,256]{1,0:T(8,128)(2,1)S(1)}, bf16[672,256]{1,0:T(8,128)(2,1)S(1)}, u32[]{:S(2)}, u32[]{:S(2)}) collective-permute-start(bf16[672,256]{1,0:T(8,128)(2,1)S(1)} %add_convert_fusion.1), channel_id=1, source_target_pairs={{0,2},{2,4},{4,6},{6,0},{1,3},{3,5},{5,7},{7,1},{8,10},{10,12},{12... | collective-permute-start | bytes 1032200 | tf_op jit(solution)/shard_map/ppermute | solution.py:14
  119.3 5.1 %all-to-all-done.1 = bf16[8,168,384]{2,1,0:T(8,128)(2,1)S(1)} async-done(((bf16[8,168,384]{2,1,0:T(8,128)(2,1)}), bf16[8,168,384]{2,1,0:T(8,128)(2,1)S(1)}, u32[]{:S(2)}, u32[]{:S(2)}) %all-to-all-start.1) | async-done | bytes 1032224 | tf_op jit(solution)/shard_map/all_to_all | solution.py:25
  124.4 0.1 reduce_sum.21
  124.6 0.7 reshape.25
  125.3 3.5 %collective-permute-done.11 = bf16[672,256]{1,0:T(8,128)(2,1)S(1)} collective-permute-done((bf16[672,256]{1,0:T(8,128)(2,1)S(1)}, bf16[672,256]{1,0:T(8,128)(2,1)S(1)}, u32[]{:S(2)}, u32[]{:S(2)}) %collective-permute-start.11) | collective-permute-done | bytes 344096 | tf_op jit(solution)/shard_map/ppermute | solution.py:14
  128.8 0.0 collective-permute-done.10
  128.8 5.6 %collective-permute-done.9 = bf16[672,256]{1,0:T(8,128)(2,1)S(1)} collective-permute-done((bf16[672,256]{1,0:T(8,128)(2,1)S(1)}, bf16[672,256]{1,0:T(8,128)(2,1)S(1)}, u32[]{:S(2)}, u32[]{:S(2)}) %collective-permute-start.9) | collective-permute-done | bytes 344096 | tf_op jit(solution)/shard_map/ppermute | solution.py:14
  134.4 0.2 add_convert_fusion
  134.6 1.9 %collective-permute-start.12 = (bf16[672,256]{1,0:T(8,128)(2,1)S(1)}, bf16[672,256]{1,0:T(8,128)(2,1)S(1)}, u32[]{:S(2)}, u32[]{:S(2)}) collective-permute-start(bf16[672,256]{1,0:T(8,128)(2,1)S(1)} %add_convert_fusion), channel_id=1, source_target_pairs={{0,1},{1,0},{2,3},{3,2},{4,5},{5,4},{6,7},{7,6},{8,9},{9,8},{10,11... | collective-permute-start | bytes 1032200 | tf_op jit(solution)/shard_map/ppermute | solution.py:14
  136.5 3.7 %all-to-all-start.2 = ((bf16[12,14,384]{2,1,0:T(8,128)(2,1)}), bf16[12,14,384]{2,1,0:T(8,128)(2,1)S(1)}, u32[]{:S(2)}, u32[]{:S(2)}) async-start(bf16[12,14,384]{2,1,0:T(8,128)(2,1)} %reshape.25), calls=%async_computation.2 | async-start | bytes 294912 | tf_op jit(solution)/shard_map/all_to_all | solution.py:25
  140.2 0.0 collective-permute-done.12
  140.2 0.1 broadcast_select_fusion.1
  140.3 4.6 %convolution_convert_fusion.1 = bf16[256,1344]{0,1:T(8,128)(2,1)} fusion(bf16[1344,1344]{1,0:T(8,128)(2,1)} %fusion, bf16[672,256]{1,0:T(8,128)(2,1)S(1)} %get-tuple-element.15, bf16[672,256]{1,0:T(8,128)(2,1)S(1)} %get-tuple-element.14), kind=kOutput, calls=%fused_computation.3 | convolution fusion | flops 926564352 | bytes 4988928 | tf_op jit(solution)/shard_map/dot_general | solution.py:30
  144.9 8.5 %all-to-all-done.2 = bf16[12,14,384]{2,1,0:T(8,128)(2,1)S(1)} async-done(((bf16[12,14,384]{2,1,0:T(8,128)(2,1)}), bf16[12,14,384]{2,1,0:T(8,128)(2,1)S(1)}, u32[]{:S(2)}, u32[]{:S(2)}) %all-to-all-start.2) | async-done | bytes 129056 | tf_op jit(solution)/shard_map/all_to_all | solution.py:25
  153.4 0.6 convert_reduce_fusion
  (22 shorter events, 0.5 us)
Async XLA Ops:
  0.6 20.0 %copy-start = (bf16[256,1344]{0,1:T(8,128)(2,1)S(1)}, bf16[256,1344]{0,1:T(8,128)(2,1)}, u32[]{:S(2)}) copy-start(bf16[256,1344]{0,1:T(8,128)(2,1)} %param.7) | copy-start | bytes 2064388
  2.3 36.2 %all-to-all-start = ((bf16[12,14,1152]{2,1,0:T(8,128)(2,1)}), bf16[12,14,1152]{2,1,0:T(8,128)(2,1)S(1)}, u32[]{:S(2)}, u32[]{:S(2)}) async-start(bf16[12,14,1152]{2,1,0:T(8,128)(2,1)} %broadcast_in_dim.68), calls=%async_computation | async-start | bytes 884736 | tf_op jit(solution)/shard_map/all_to_all | solution.py:19
  20.6 4.3 %copy-start.1 = (bf16[1344,1344]{1,0:T(8,128)(2,1)S(1)}, bf16[1344,1344]{1,0:T(8,128)(2,1)}, u32[]{:S(2)}) copy-start(bf16[1344,1344]{1,0:T(8,128)(2,1)} %fusion) | copy-start | bytes 10838020
  20.6 4.3 %copy-start.4 = (bf16[256,1344]{0,1:T(8,128)(2,1)S(1)}, bf16[256,1344]{0,1:T(8,128)(2,1)}, u32[]{:S(2)}) copy-start(bf16[256,1344]{0,1:T(8,128)(2,1)} %param.6) | copy-start | bytes 2064388
  38.6 13.2 %collective-permute-start.1 = (bf16[168,1152]{1,0:T(8,128)(2,1)S(1)}, bf16[168,1152]{1,0:T(8,128)(2,1)S(1)}, u32[]{:S(2)}, u32[]{:S(2)}) collective-permute-start(bf16[168,1152]{1,0:T(8,128)(2,1)S(1)} %reshape.21), channel_id=1, source_target_pairs={{0,56},{1,9},{8,0},{9,17},{16,8},{17,25},{24,16},{25,33},{32,24},{... | collective-permute-start | bytes 1161224 | tf_op jit(solution)/shard_map/ppermute | solution.py:58
  41.0 14.0 %collective-permute-start = (bf16[168,1152]{1,0:T(8,128)(2,1)S(1)}, bf16[168,1152]{1,0:T(8,128)(2,1)S(1)}, u32[]{:S(2)}, u32[]{:S(2)}) collective-permute-start(bf16[168,1152]{1,0:T(8,128)(2,1)S(1)} %reshape.21), channel_id=1, source_target_pairs={{0,8},{1,57},{8,16},{9,1},{16,24},{17,9},{24,32},{25,17},{32,40},{... | collective-permute-start | bytes 1161224 | tf_op jit(solution)/shard_map/ppermute | solution.py:58
  51.8 13.5 %collective-permute-start.3 = (bf16[168,1152]{1,0:T(8,128)(2,1)S(1)}, bf16[168,1152]{1,0:T(8,128)(2,1)S(1)}, u32[]{:S(2)}, u32[]{:S(2)}) collective-permute-start(bf16[168,1152]{1,0:T(8,128)(2,1)S(1)} %collective-permute-done.1), channel_id=1, source_target_pairs={{0,56},{1,9},{8,0},{9,17},{16,8},{17,25},{24,16},{25,33},{32,24},{... | collective-permute-start | bytes 1161224 | tf_op jit(solution)/shard_map/ppermute | solution.py:58
  55.0 15.2 %collective-permute-start.2 = (bf16[168,1152]{1,0:T(8,128)(2,1)S(1)}, bf16[168,1152]{1,0:T(8,128)(2,1)S(1)}, u32[]{:S(2)}, u32[]{:S(2)}) collective-permute-start(bf16[168,1152]{1,0:T(8,128)(2,1)S(1)} %collective-permute-done), channel_id=1, source_target_pairs={{0,8},{1,57},{8,16},{9,1},{16,24},{17,9},{24,32},{25,17},{32,40},{... | collective-permute-start | bytes 1161224 | tf_op jit(solution)/shard_map/ppermute | solution.py:58
  65.2 12.6 %collective-permute-start.5 = (bf16[168,1152]{1,0:T(8,128)(2,1)S(1)}, bf16[168,1152]{1,0:T(8,128)(2,1)S(1)}, u32[]{:S(2)}, u32[]{:S(2)}) collective-permute-start(bf16[168,1152]{1,0:T(8,128)(2,1)S(1)} %collective-permute-done.3), channel_id=1, source_target_pairs={{0,56},{1,9},{8,0},{9,17},{16,8},{17,25},{24,16},{25,33},{32,24},{... | collective-permute-start | bytes 1161224 | tf_op jit(solution)/shard_map/ppermute | solution.py:58
  70.3 11.7 %collective-permute-start.4 = (bf16[168,1152]{1,0:T(8,128)(2,1)S(1)}, bf16[168,1152]{1,0:T(8,128)(2,1)S(1)}, u32[]{:S(2)}, u32[]{:S(2)}) collective-permute-start(bf16[168,1152]{1,0:T(8,128)(2,1)S(1)} %collective-permute-done.2), channel_id=1, source_target_pairs={{0,8},{1,57},{8,16},{9,1},{16,24},{17,9},{24,32},{25,17},{32,40},{... | collective-permute-start | bytes 1161224 | tf_op jit(solution)/shard_map/ppermute | solution.py:58
  77.9 12.5 %collective-permute-start.7 = (bf16[88,1152]{1,0:T(8,128)(2,1)S(1)}, bf16[88,1152]{1,0:T(8,128)(2,1)S(1)}, u32[]{:S(2)}, u32[]{:S(2)}) collective-permute-start(bf16[88,1152]{1,0:T(8,128)(2,1)S(1)} %slice.97), channel_id=1, source_target_pairs={{0,56},{1,9},{8,0},{9,17},{16,8},{17,25},{24,16},{25,33},{32,24},{... | collective-permute-start | bytes 608264 | tf_op jit(solution)/shard_map/ppermute | solution.py:58
  82.0 8.4 %collective-permute-start.6 = (bf16[80,1152]{1,0:T(8,128)(2,1)S(1)}, bf16[80,1152]{1,0:T(8,128)(2,1)S(1)}, u32[]{:S(2)}, u32[]{:S(2)}) collective-permute-start(bf16[80,1152]{1,0:T(8,128)(2,1)S(1)} %slice.95), channel_id=1, source_target_pairs={{0,8},{1,57},{8,16},{9,1},{16,24},{17,9},{24,32},{25,17},{32,40},{... | collective-permute-start | bytes 552968 | tf_op jit(solution)/shard_map/ppermute | solution.py:58
  90.3 1.8 %copy-start.6 = (bf16[1344,256]{1,0:T(8,128)(2,1)S(1)}, bf16[1344,256]{1,0:T(8,128)(2,1)}, u32[]{:S(2)}) copy-start(bf16[1344,256]{1,0:T(8,128)(2,1)} %convolution_convert_fusion.3) | copy-start | bytes 2064388
  90.4 3.3 %copy-start.2 = (bf16[8,168,768]{2,1,0:T(8,128)(2,1)}, bf16[8,168,768]{2,1,0:T(8,128)(2,1)S(1)}, u32[]{:S(2)}) copy-start(bf16[8,168,768]{2,1,0:T(8,128)(2,1)S(1)} %fusion.15) | copy-start | bytes 6193156
  91.2 0.9 copy-start.5
  93.7 30.7 %all-to-all-start.1 = ((bf16[8,168,384]{2,1,0:T(8,128)(2,1)}), bf16[8,168,384]{2,1,0:T(8,128)(2,1)S(1)}, u32[]{:S(2)}, u32[]{:S(2)}) async-start(bf16[8,168,384]{2,1,0:T(8,128)(2,1)} %bitcast.91), calls=%async_computation.1 | async-start | bytes 2064384 | tf_op jit(solution)/shard_map/all_to_all | solution.py:25
  102.6 2.1 %copy-start.3 = (bf16[8,168,768]{2,1,0:T(8,128)(2,1)S(1)}, bf16[8,168,768]{2,1,0:T(8,128)(2,1)}, u32[]{:S(2)}) copy-start(bf16[8,168,768]{2,1,0:T(8,128)(2,1)} %copy-done.2) | copy-start | bytes 6193156
  105.5 3.5 %collective-permute-start.8 = (bf16[672,256]{1,0:T(8,128)(2,1)S(1)}, bf16[672,256]{1,0:T(8,128)(2,1)S(1)}, u32[]{:S(2)}, u32[]{:S(2)}) collective-permute-start(bf16[672,256]{1,0:T(8,128)(2,1)S(1)} %constant_dynamic-slice_fusion), channel_id=1, source_target_pairs={{0,1},{1,0},{2,3},{3,2},{4,5},{5,4},{6,7},{7,6},{8,9},{9,8},{10,11... | collective-permute-start | bytes 1032200 | tf_op jit(solution)/shard_map/ppermute | solution.py:14
  109.1 19.7 %collective-permute-start.11 = (bf16[672,256]{1,0:T(8,128)(2,1)S(1)}, bf16[672,256]{1,0:T(8,128)(2,1)S(1)}, u32[]{:S(2)}, u32[]{:S(2)}) collective-permute-start(bf16[672,256]{1,0:T(8,128)(2,1)S(1)} %add_convert_fusion.1), channel_id=1, source_target_pairs={{0,6},{2,0},{4,2},{6,4},{1,7},{3,1},{5,3},{7,5},{8,14},{10,8},{12,... | collective-permute-start | bytes 1032200 | tf_op jit(solution)/shard_map/ppermute | solution.py:14
  113.8 15.0 %collective-permute-start.10 = (bf16[672,256]{1,0:T(8,128)(2,1)S(1)}, bf16[672,256]{1,0:T(8,128)(2,1)S(1)}, u32[]{:S(2)}, u32[]{:S(2)}) collective-permute-start(bf16[672,256]{1,0:T(8,128)(2,1)S(1)} %add_convert_fusion.1), channel_id=1, source_target_pairs={{0,4},{2,6},{4,0},{6,2},{1,5},{3,7},{5,1},{7,3},{8,12},{10,14},{12... | collective-permute-start | bytes 1032200 | tf_op jit(solution)/shard_map/ppermute | solution.py:14
  116.5 17.9 %collective-permute-start.9 = (bf16[672,256]{1,0:T(8,128)(2,1)S(1)}, bf16[672,256]{1,0:T(8,128)(2,1)S(1)}, u32[]{:S(2)}, u32[]{:S(2)}) collective-permute-start(bf16[672,256]{1,0:T(8,128)(2,1)S(1)} %add_convert_fusion.1), channel_id=1, source_target_pairs={{0,2},{2,4},{4,6},{6,0},{1,3},{3,5},{5,7},{7,1},{8,10},{10,12},{12... | collective-permute-start | bytes 1032200 | tf_op jit(solution)/shard_map/ppermute | solution.py:14
  134.6 5.7 %collective-permute-start.12 = (bf16[672,256]{1,0:T(8,128)(2,1)S(1)}, bf16[672,256]{1,0:T(8,128)(2,1)S(1)}, u32[]{:S(2)}, u32[]{:S(2)}) collective-permute-start(bf16[672,256]{1,0:T(8,128)(2,1)S(1)} %add_convert_fusion), channel_id=1, source_target_pairs={{0,1},{1,0},{2,3},{3,2},{4,5},{5,4},{6,7},{7,6},{8,9},{9,8},{10,11... | collective-permute-start | bytes 1032200 | tf_op jit(solution)/shard_map/ppermute | solution.py:14
  136.5 16.9 %all-to-all-start.2 = ((bf16[12,14,384]{2,1,0:T(8,128)(2,1)}), bf16[12,14,384]{2,1,0:T(8,128)(2,1)S(1)}, u32[]{:S(2)}, u32[]{:S(2)}) async-start(bf16[12,14,384]{2,1,0:T(8,128)(2,1)} %reshape.25), calls=%async_computation.2 | async-start | bytes 294912 | tf_op jit(solution)/shard_map/all_to_all | solution.py:25

commit v2 on v0

v2 whole, which is shorter than its diff:
```python
import jax
import jax.numpy as jnp
import numpy as np
from jax import lax
from jax.sharding import Mesh
from jax.sharding import PartitionSpec as P


FAR = 4
CHAINS = 2
FS_0 = ("fs_0h", "fs_0l")
FS = (*FS_0, "fs_1")


def shifted(array, axis, step):
    peers = lax.axis_size(axis)
    return lax.ppermute(array, axis, [(k, (k + step) % peers) for k in range(peers)])


def paired(array, axis, turn):
    peers = lax.axis_size(axis)
    pairs = []
    for k in range(peers):
        for core in range(2):
            other = (k + (1 if (k + core + turn) % 2 == 0 else -1)) % peers
            pairs.append((2 * k + core, 2 * other + core))
    return lax.ppermute(array, (*axis, "core"), pairs)


def sent_to_all(array, axis):
    peers = lax.axis_size(axis)
    return lax.all_to_all(
        jnp.broadcast_to(array[None], (peers, *array.shape)), axis, 0, 0, tiled=True
    )


def exchanged(parts, axis):
    got = lax.all_to_all(parts, axis, 0, 0, tiled=True)
    return got.astype(jnp.float32).sum(axis=0)


def contract_cols(left, right):
    return lax.dot_general(
        left, right, (((1,), (1,)), ((), ())), preferred_element_type=jnp.float32
    )


def picked(source):
    source = jnp.asarray(source, jnp.int32)
    spot = lax.broadcasted_iota(jnp.int32, (source.size, source.size), 1)
    return (source[:, None] == spot).astype(jnp.bfloat16)


def around(block, axis):
    peers = lax.axis_size(axis)
    rows = block.shape[0] // CHAINS
    place = lax.axis_index(axis)
    role = (place + lax.axis_index("core")) % 2
    whole = jnp.zeros((peers, *block.shape), block.dtype)

    def put(whole, part, owner, chain):
        owner = (owner + 2 * peers) % peers
        return lax.dynamic_update_slice(whole, part[None], (owner, chain * rows, 0))

    base = place - role
    own = [block[k * rows : (k + 1) * rows] for k in range(CHAINS)]
    got = [paired(b, axis, 0) for b in own]
    for k in range(CHAINS):
        whole = put(whole, own[k], place, k)
        whole = put(whole, got[k], base + 1 - role, k)
    held = [jnp.stack(pair) for pair in zip(own, got)]
    for step in range(1, peers // 2):
        held = [paired(h, axis, step) for h in held]
        odd = step % 2
        away = (step + 1) // 2 * (1 - 2 * odd) * (1 - 2 * role)
        first = odd + role - 2 * odd * role
        for k, h in enumerate(held):
            whole = put(whole, h[0], base + 2 * away + first, k)
            whole = put(whole, h[1], base + 2 * away + 1 - first, k)
    return whole.reshape(peers * block.shape[0], -1)


def added(left, right):
    return (left.astype(jnp.float32) + right.astype(jnp.float32)).astype(jnp.bfloat16)


def summed_over_tp(partial):
    half = partial.shape[0] // 2
    core = lax.axis_index("core")
    kept = lax.dynamic_slice_in_dim(partial, core * half, half)
    given = lax.dynamic_slice_in_dim(partial, (1 - core) * half, half)
    total = added(kept, shifted(given, "core", 1))
    total = added(total, paired(total, ("chip",), 0))
    other = paired(total, ("chip",), 1)
    total = added(total, other)
    other = shifted(total, "core", 1)
    first = jnp.where(core == 0, total, other)
    second = jnp.where(core == 0, other, total)
    return jnp.concatenate([first, second])


def gradients(tokens, cotangent, gate_weight, up_weight, down_weight):
    near, inner = lax.axis_size("fs_0l"), lax.axis_size("fs_1")
    rows, units = gate_weight.shape
    width = tokens.shape[1]

    weights = jnp.concatenate([gate_weight, up_weight, down_weight.T], axis=1)
    weights = sent_to_all(weights, "fs_1").reshape(inner * rows, 3 * units)
    weights = around(weights, FS_0)
    gate_up, down = weights[:, : 2 * units], weights[:, 2 * units :]

    spot = np.arange(width).reshape(FAR, near, inner, rows).transpose(2, 1, 0, 3).reshape(-1)
    turned_cotangent = contract_cols(picked(spot), cotangent).astype(jnp.bfloat16)
    turned_cotangent = lax.optimization_barrier(turned_cotangent)

    both = jnp.dot(tokens, gate_up, preferred_element_type=jnp.float32)
    gate_pre, up_pre = both[:, :units], both[:, units:]
    sigmoid_gate = jax.nn.sigmoid(gate_pre)
    activated = gate_pre * sigmoid_gate
    hidden = (activated * up_pre).astype(jnp.bfloat16)

    terms = jnp.dot(turned_cotangent, hidden, preferred_element_type=jnp.float32)
    terms = terms.astype(jnp.bfloat16).reshape(inner * near, FAR * rows, units)
    terms = exchanged(terms, ("fs_1", "fs_0l"))
    terms = terms.astype(jnp.bfloat16).reshape(FAR, rows, units)
    down_grad = exchanged(terms, "fs_0h").T

    hidden_grad = jnp.dot(cotangent, down, preferred_element_type=jnp.float32)
    gate_pre_grad = (
        hidden_grad * up_pre * sigmoid_gate * (1.0 + gate_pre * (1.0 - sigmoid_gate))
    ).astype(jnp.bfloat16)
    up_pre_grad = (hidden_grad * activated).astype(jnp.bfloat16)
    partial = contract_cols(gate_up, jnp.concatenate([gate_pre_grad, up_pre_grad], axis=1))
    total = summed_over_tp(partial.astype(jnp.bfloat16))
    return (total.T, down_grad)


def solution(mesh):
    torus = Mesh(
        mesh.devices.reshape(FAR, 12 // FAR, 8, mesh.shape["tp"] // 2, 2), (*FS, "chip", "core")
    )
    tp = ("chip", "core")
    in_specs = (P(FS, None), P(FS, None), P(FS, tp), P(FS, tp), P(tp, FS))
    out_specs = (P(FS, None), P(tp, FS))
    return jax.shard_map(
        gradients, mesh=torus, in_specs=in_specs, out_specs=out_specs, check_vma=False
    )
```

time: 172 us -> 154 us (0.90)
  the two profiles are of different devices: /device:TPU:10 before, /device:TPU:14 now
where the time goes in v2:
time: 154 us; the launch traced here: 153 us
  starting transfers between devices  75.1 us (49%)
  waiting for transfers between devices  63 us (41%)
  matrix products  7.25 us (5%)
  local copies, waits for them, and re-layouts  3.46 us (2%)
  other arithmetic  2.84 us (2%)
    ppermute x14, starting transfers between devices, paired(): return lax.ppermute(array, (*axis, 'core'), pairs)  52.6 us
    ppermute x14, waiting for transfers between devices, paired(): return lax.ppermute(array, (*axis, 'core'), pairs)  41.2 us
    all_to_all x2, starting transfers between devices, exchanged(): got = lax.all_to_all(parts, axis, 0, 0, tiled=True)  11.1 us
    all_to_all x2, waiting for transfers between devices, exchanged(): got = lax.all_to_all(parts, axis, 0, 0, tiled=True)  9.64 us
    all_to_all x1, waiting for transfers between devices, sent_to_all(): lax.all_to_all(jnp.broadcast_to(array[None], (peers, *array.shape)), axis...  8.86 us
    all_to_all x1, starting transfers between devices, sent_to_all(): lax.all_to_all(jnp.broadcast_to(array[None], (peers, *array.shape)), axis...  7.55 us
    ppermute x2, starting transfers between devices, shifted(): lax.ppermute(array, axis, [(k, (k + step) % peers) for k in range(peers)])  3.84 us
    ppermute x2, waiting for transfers between devices, shifted(): lax.ppermute(array, axis, [(k, (k + step) % peers) for k in range(peers)])  3.23 us
  transfers between devices with their start and end apart: 19, of which 13 were waited for; matrix products, arithmetic and copies ran while one was open for 4% of the time, Pallas kernels for 0%

profile of v2, /device:TPU:14, one launch (start us, length us, event | category | flops | bytes accessed | tf_op | source)
XLA Modules:
  0.0 152.8 jit_solution(11179437008710468293)
XLA Ops:
  0.6 0.0 copy-start
  0.6 0.8 pad_maximum_fusion.2
  1.5 0.7 broadcast_in_dim.23
  2.2 7.5 %all-to-all-start = ((bf16[8,14,1152]{2,1,0:T(8,128)(2,1)}), bf16[8,14,1152]{2,1,0:T(8,128)(2,1)S(1)}, u32[]{:S(2)}, u32[]{:S(2)}) async-start(bf16[8,14,1152]{2,1,0:T(8,128)(2,1)} %broadcast_in_dim.23), calls=%async_computation | async-start | bytes 589824 | tf_op jit(solution)/shard_map/all_to_all | solution.py:32
  9.7 0.0 copy-done
  9.7 2.2 %fusion.2 = bf16[1344,256]{1,0:T(8,128)(2,1)S(1)} fusion(bf16[256,1344]{0,1:T(8,128)(2,1)S(1)} %copy-done, s32[1344]{0:T(1024)} %constant.111.clone), kind=kOutput, calls=%fused_computation.5 | convolution fusion | flops 926994432 | bytes 1381632 | tf_op jit(solution)/shard_map/dot_general | solution.py:43
  12.0 8.9 %all-to-all-done = bf16[8,14,1152]{2,1,0:T(8,128)(2,1)S(1)} async-done(((bf16[8,14,1152]{2,1,0:T(8,128)(2,1)}), bf16[8,14,1152]{2,1,0:T(8,128)(2,1)S(1)}, u32[]{:S(2)}, u32[]{:S(2)}) %all-to-all-start) | async-done | bytes 258080 | tf_op jit(solution)/shard_map/all_to_all | solution.py:32
  21.1 4.3 %collective-permute-start = (bf16[56,1152]{1,0:T(8,128)(2,1)S(1)}, bf16[56,1152]{1,0:T(8,128)(2,1)S(1)}, u32[]{:S(2)}, u32[]{:S(2)}) collective-permute-start(bf16[56,1152]{1,0:T(8,128)(2,1)S(1)} %slice.85), channel_id=1, source_target_pairs={{0,64},{1,705},{64,0},{65,129},{128,192},{129,65},{192,128},{193,2... | collective-permute-start | bytes 387080 | tf_op jit(solution)/shard_map/ppermute | solution.py:27
  25.4 1.9 %collective-permute-start.1 = (bf16[56,1152]{1,0:T(8,128)(2,1)S(1)}, bf16[56,1152]{1,0:T(8,128)(2,1)S(1)}, u32[]{:S(2)}, u32[]{:S(2)}) collective-permute-start(bf16[56,1152]{1,0:T(8,128)(2,1)S(1)} %slice.87), channel_id=1, source_target_pairs={{0,64},{1,705},{64,0},{65,129},{128,192},{129,65},{192,128},{193,2... | collective-permute-start | bytes 387080 | tf_op jit(solution)/shard_map/ppermute | solution.py:27
  27.3 0.2 broadcast_in_dim.22
  27.6 0.7 collective-permute-done
  28.3 14.2 %collective-permute-start.2 = (bf16[2,56,1152]{2,1,0:T(8,128)(2,1)S(1)}, bf16[2,56,1152]{2,1,0:T(8,128)(2,1)S(1)}, u32[]{:S(2)}, u32[]{:S(2)}) collective-permute-start(bf16[2,56,1152]{2,1,0:T(8,128)(2,1)S(1)} %pad_maximum_fusion), channel_id=1, source_target_pairs={{0,704},{1,65},{64,128},{65,1},{128,64},{129,193},{192,256},{193,1... | collective-permute-start | bytes 774152 | tf_op jit(solution)/shard_map/ppermute | solution.py:27
  42.6 0.0 copy-start.3
  42.6 0.0 collective-permute-done.1
  42.7 3.2 %collective-permute-start.3 = (bf16[2,56,1152]{2,1,0:T(8,128)(2,1)S(1)}, bf16[2,56,1152]{2,1,0:T(8,128)(2,1)S(1)}, u32[]{:S(2)}, u32[]{:S(2)}) collective-permute-start(bf16[2,56,1152]{2,1,0:T(8,128)(2,1)S(1)} %pad_maximum_fusion.1), channel_id=1, source_target_pairs={{0,704},{1,65},{64,128},{65,1},{128,64},{129,193},{192,256},{193,1... | collective-permute-start | bytes 774152 | tf_op jit(solution)/shard_map/ppermute | solution.py:27
  45.9 1.0 collective-permute-done.2
  46.9 1.9 %collective-permute-start.4 = (bf16[2,56,1152]{2,1,0:T(8,128)(2,1)S(1)}, bf16[2,56,1152]{2,1,0:T(8,128)(2,1)S(1)}, u32[]{:S(2)}, u32[]{:S(2)}) collective-permute-start(bf16[2,56,1152]{2,1,0:T(8,128)(2,1)S(1)} %collective-permute-done.2), channel_id=1, source_target_pairs={{0,64},{1,705},{64,0},{65,129},{128,192},{129,65},{192,128},{193,2... | collective-permute-start | bytes 774152 | tf_op jit(solution)/shard_map/ppermute | solution.py:27
  48.8 6.1 %collective-permute-done.3 = bf16[2,56,1152]{2,1,0:T(8,128)(2,1)S(1)} collective-permute-done((bf16[2,56,1152]{2,1,0:T(8,128)(2,1)S(1)}, bf16[2,56,1152]{2,1,0:T(8,128)(2,1)S(1)}, u32[]{:S(2)}, u32[]{:S(2)}) %collective-permute-start.3) | collective-permute-done | bytes 258080 | tf_op jit(solution)/shard_map/ppermute | solution.py:27
  54.9 1.9 %collective-permute-start.5 = (bf16[2,56,1152]{2,1,0:T(8,128)(2,1)S(1)}, bf16[2,56,1152]{2,1,0:T(8,128)(2,1)S(1)}, u32[]{:S(2)}, u32[]{:S(2)}) collective-permute-start(bf16[2,56,1152]{2,1,0:T(8,128)(2,1)S(1)} %collective-permute-done.3), channel_id=1, source_target_pairs={{0,64},{1,705},{64,0},{65,129},{128,192},{129,65},{192,128},{193,2... | collective-permute-start | bytes 774152 | tf_op jit(solution)/shard_map/ppermute | solution.py:27
  56.9 0.0 collective-permute-done.4
  56.9 4.0 %collective-permute-start.6 = (bf16[2,56,1152]{2,1,0:T(8,128)(2,1)S(1)}, bf16[2,56,1152]{2,1,0:T(8,128)(2,1)S(1)}, u32[]{:S(2)}, u32[]{:S(2)}) collective-permute-start(bf16[2,56,1152]{2,1,0:T(8,128)(2,1)S(1)} %collective-permute-done.4), channel_id=1, source_target_pairs={{0,704},{1,65},{64,128},{65,1},{128,64},{129,193},{192,256},{193,1... | collective-permute-start | bytes 774152 | tf_op jit(solution)/shard_map/ppermute | solution.py:27
  60.9 4.3 %collective-permute-done.5 = bf16[2,56,1152]{2,1,0:T(8,128)(2,1)S(1)} collective-permute-done((bf16[2,56,1152]{2,1,0:T(8,128)(2,1)S(1)}, bf16[2,56,1152]{2,1,0:T(8,128)(2,1)S(1)}, u32[]{:S(2)}, u32[]{:S(2)}) %collective-permute-start.5) | collective-permute-done | bytes 258080 | tf_op jit(solution)/shard_map/ppermute | solution.py:27
  65.2 3.1 %collective-permute-start.7 = (bf16[2,56,1152]{2,1,0:T(8,128)(2,1)S(1)}, bf16[2,56,1152]{2,1,0:T(8,128)(2,1)S(1)}, u32[]{:S(2)}, u32[]{:S(2)}) collective-permute-start(bf16[2,56,1152]{2,1,0:T(8,128)(2,1)S(1)} %collective-permute-done.5), channel_id=1, source_target_pairs={{0,704},{1,65},{64,128},{65,1},{128,64},{129,193},{192,256},{193,1... | collective-permute-start | bytes 774152 | tf_op jit(solution)/shard_map/ppermute | solution.py:27
  68.4 0.0 collective-permute-done.6
  68.4 2.5 %collective-permute-start.8 = (bf16[2,56,1152]{2,1,0:T(8,128)(2,1)S(1)}, bf16[2,56,1152]{2,1,0:T(8,128)(2,1)S(1)}, u32[]{:S(2)}, u32[]{:S(2)}) collective-permute-start(bf16[2,56,1152]{2,1,0:T(8,128)(2,1)S(1)} %collective-permute-done.6), channel_id=1, source_target_pairs={{0,64},{1,705},{64,0},{65,129},{128,192},{129,65},{192,128},{193,2... | collective-permute-start | bytes 774152 | tf_op jit(solution)/shard_map/ppermute | solution.py:27
  70.9 5.3 %collective-permute-done.7 = bf16[2,56,1152]{2,1,0:T(8,128)(2,1)S(1)} collective-permute-done((bf16[2,56,1152]{2,1,0:T(8,128)(2,1)S(1)}, bf16[2,56,1152]{2,1,0:T(8,128)(2,1)S(1)}, u32[]{:S(2)}, u32[]{:S(2)}) %collective-permute-start.7) | collective-permute-done | bytes 258080 | tf_op jit(solution)/shard_map/ppermute | solution.py:27
  76.2 1.9 %collective-permute-start.9 = (bf16[2,56,1152]{2,1,0:T(8,128)(2,1)S(1)}, bf16[2,56,1152]{2,1,0:T(8,128)(2,1)S(1)}, u32[]{:S(2)}, u32[]{:S(2)}) collective-permute-start(bf16[2,56,1152]{2,1,0:T(8,128)(2,1)S(1)} %collective-permute-done.7), channel_id=1, source_target_pairs={{0,64},{1,705},{64,0},{65,129},{128,192},{129,65},{192,128},{193,2... | collective-permute-start | bytes 774152 | tf_op jit(solution)/shard_map/ppermute | solution.py:27
  78.2 0.0 collective-permute-done.8
  78.2 4.3 %collective-permute-start.10 = (bf16[2,56,1152]{2,1,0:T(8,128)(2,1)S(1)}, bf16[2,56,1152]{2,1,0:T(8,128)(2,1)S(1)}, u32[]{:S(2)}, u32[]{:S(2)}) collective-permute-start(bf16[2,56,1152]{2,1,0:T(8,128)(2,1)S(1)} %collective-permute-done.8), channel_id=1, source_target_pairs={{0,704},{1,65},{64,128},{65,1},{128,64},{129,193},{192,256},{193,1... | collective-permute-start | bytes 774152 | tf_op jit(solution)/shard_map/ppermute | solution.py:27
  82.5 4.6 %collective-permute-done.9 = bf16[2,56,1152]{2,1,0:T(8,128)(2,1)S(1)} collective-permute-done((bf16[2,56,1152]{2,1,0:T(8,128)(2,1)S(1)}, bf16[2,56,1152]{2,1,0:T(8,128)(2,1)S(1)}, u32[]{:S(2)}, u32[]{:S(2)}) %collective-permute-start.9) | collective-permute-done | bytes 258080 | tf_op jit(solution)/shard_map/ppermute | solution.py:27
  87.1 4.3 %collective-permute-start.11 = (bf16[2,56,1152]{2,1,0:T(8,128)(2,1)S(1)}, bf16[2,56,1152]{2,1,0:T(8,128)(2,1)S(1)}, u32[]{:S(2)}, u32[]{:S(2)}) collective-permute-start(bf16[2,56,1152]{2,1,0:T(8,128)(2,1)S(1)} %collective-permute-done.9), channel_id=1, source_target_pairs={{0,704},{1,65},{64,128},{65,1},{128,64},{129,193},{192,256},{193,1... | collective-permute-start | bytes 774152 | tf_op jit(solution)/shard_map/ppermute | solution.py:27
  91.5 0.0 collective-permute-done.10
  91.6 5.0 %collective-permute-done.11 = bf16[2,56,1152]{2,1,0:T(8,128)(2,1)S(1)} collective-permute-done((bf16[2,56,1152]{2,1,0:T(8,128)(2,1)S(1)}, bf16[2,56,1152]{2,1,0:T(8,128)(2,1)S(1)}, u32[]{:S(2)}, u32[]{:S(2)}) %collective-permute-start.11) | collective-permute-done | bytes 258080 | tf_op jit(solution)/shard_map/ppermute | solution.py:27
  96.6 0.0 copy-start.1
  96.6 0.0 copy-done.3
  96.6 0.8 fusion.6
  97.4 0.8 copy-done.1
  98.2 1.6 %convolution_convert_fusion = bf16[1344,384]{1,0:T(8,128)(2,1)} fusion(bf16[1344,256]{1,0:T(8,128)(2,1)S(1)} %fusion.2, f32[256,768]{0,1:T(8,128)S(1)} %fusion.6), kind=kOutput, calls=%fused_computation.3 | convolution fusion | flops 265347072 | bytes 2506752 | tf_op jit(solution)/shard_map/dot_general | solution.py:122
  99.8 6.1 %all-to-all-start.1 = ((bf16[24,56,384]{2,1,0:T(8,128)(2,1)}), bf16[24,56,384]{2,1,0:T(8,128)(2,1)S(1)}, u32[]{:S(2)}, u32[]{:S(2)}) async-start(bf16[24,56,384]{2,1,0:T(8,128)(2,1)} %bitcast.7), calls=%async_computation.1 | async-start | bytes 2064384 | tf_op jit(solution)/shard_map/all_to_all | solution.py:38
  105.9 0.0 copy-start.2
  106.0 1.9 %multiply_convert_fusion.2 = (bf16[256,384]{0,1:T(8,128)(2,1)S(1)}, bf16[256,384]{0,1:T(8,128)(2,1)S(1)}) fusion(f32[256,768]{0,1:T(8,128)S(1)} %fusion.6, bf16[256,1344]{0,1:T(8,128)(2,1)S(1)} %copy-done, bf16[1344,1152]{1,0:T(8,128)(2,1)} %bitcast.19), kind=kOutput, calls=%fused_computation.21 | convolution fusion | flops 265519104 | bytes 2899968 | tf_op jit(solution)/shard_map/dot_general | solution.py:128
  107.9 0.3 copy-done.2
  108.1 0.7 convolution_convert_fusion.1
  108.9 1.9 %collective-permute-start.12 = (bf16[672,256]{1,0:T(8,128)(2,1)S(1)}, bf16[672,256]{1,0:T(8,128)(2,1)S(1)}, u32[]{:S(2)}, u32[]{:S(2)}) collective-permute-start(bf16[672,256]{1,0:T(8,128)(2,1)S(1)} %constant_dynamic-slice_fusion), channel_id=1, source_target_pairs={{0,1},{1,0},{2,3},{3,2},{4,5},{5,4},{6,7},{7,6},{8,9},{9,8},{10,11... | collective-permute-start | bytes 1032200 | tf_op jit(solution)/shard_map/ppermute | solution.py:17
  110.8 1.6 %collective-permute-done.12 = bf16[672,256]{1,0:T(8,128)(2,1)S(1)} collective-permute-done((bf16[672,256]{1,0:T(8,128)(2,1)S(1)}, bf16[672,256]{1,0:T(8,128)(2,1)S(1)}, u32[]{:S(2)}, u32[]{:S(2)}) %collective-permute-start.12) | collective-permute-done | bytes 344096 | tf_op jit(solution)/shard_map/ppermute | solution.py:17
  112.5 0.1 add_convert_fusion.2
  112.5 2.7 %collective-permute-start.13 = (bf16[672,256]{1,0:T(8,128)(2,1)S(1)}, bf16[672,256]{1,0:T(8,128)(2,1)S(1)}, u32[]{:S(2)}, u32[]{:S(2)}) collective-permute-start(bf16[672,256]{1,0:T(8,128)(2,1)S(1)} %add_convert_fusion.2), channel_id=1, source_target_pairs={{0,2},{1,7},{2,0},{3,5},{4,6},{5,3},{6,4},{7,1},{8,10},{9,15},{10,... | collective-permute-start | bytes 1032200 | tf_op jit(solution)/shard_map/ppermute | solution.py:27
  115.3 6.4 %collective-permute-done.13 = bf16[672,256]{1,0:T(8,128)(2,1)S(1)} collective-permute-done((bf16[672,256]{1,0:T(8,128)(2,1)S(1)}, bf16[672,256]{1,0:T(8,128)(2,1)S(1)}, u32[]{:S(2)}, u32[]{:S(2)}) %collective-permute-start.13) | collective-permute-done | bytes 344096 | tf_op jit(solution)/shard_map/ppermute | solution.py:27
  121.7 0.1 add_convert_fusion.1
  121.8 2.4 %collective-permute-start.14 = (bf16[672,256]{1,0:T(8,128)(2,1)S(1)}, bf16[672,256]{1,0:T(8,128)(2,1)S(1)}, u32[]{:S(2)}, u32[]{:S(2)}) collective-permute-start(bf16[672,256]{1,0:T(8,128)(2,1)S(1)} %add_convert_fusion.1), channel_id=1, source_target_pairs={{0,6},{1,3},{2,4},{3,1},{4,2},{5,7},{6,0},{7,5},{8,14},{9,11},{10,... | collective-permute-start | bytes 1032200 | tf_op jit(solution)/shard_map/ppermute | solution.py:27
  124.2 8.0 %collective-permute-done.14 = bf16[672,256]{1,0:T(8,128)(2,1)S(1)} collective-permute-done((bf16[672,256]{1,0:T(8,128)(2,1)S(1)}, bf16[672,256]{1,0:T(8,128)(2,1)S(1)}, u32[]{:S(2)}, u32[]{:S(2)}) %collective-permute-start.14) | collective-permute-done | bytes 344096 | tf_op jit(solution)/shard_map/ppermute | solution.py:27
  132.1 0.1 add_convert_fusion
  132.2 1.9 %collective-permute-start.15 = (bf16[672,256]{1,0:T(8,128)(2,1)S(1)}, bf16[672,256]{1,0:T(8,128)(2,1)S(1)}, u32[]{:S(2)}, u32[]{:S(2)}) collective-permute-start(bf16[672,256]{1,0:T(8,128)(2,1)S(1)} %add_convert_fusion), channel_id=1, source_target_pairs={{0,1},{1,0},{2,3},{3,2},{4,5},{5,4},{6,7},{7,6},{8,9},{9,8},{10,11... | collective-permute-start | bytes 1032200 | tf_op jit(solution)/shard_map/ppermute | solution.py:17
  134.2 1.6 %collective-permute-done.15 = bf16[672,256]{1,0:T(8,128)(2,1)S(1)} collective-permute-done((bf16[672,256]{1,0:T(8,128)(2,1)S(1)}, bf16[672,256]{1,0:T(8,128)(2,1)S(1)}, u32[]{:S(2)}, u32[]{:S(2)}) %collective-permute-start.15) | collective-permute-done | bytes 344096 | tf_op jit(solution)/shard_map/ppermute | solution.py:17
  135.8 0.0 all-to-all-done.1
  135.8 0.1 reduce_sum.21
  136.0 0.6 reshape.22
  136.6 5.0 %all-to-all-start.2 = ((bf16[4,14,384]{2,1,0:T(8,128)(2,1)}), bf16[4,14,384]{2,1,0:T(8,128)(2,1)S(1)}, u32[]{:S(2)}, u32[]{:S(2)}) async-start(bf16[4,14,384]{2,1,0:T(8,128)(2,1)} %reshape.22), calls=%async_computation.2 | async-start | bytes 98304 | tf_op jit(solution)/shard_map/all_to_all | solution.py:38
  141.6 0.9 maximum_bitcast_fusion
  142.5 9.6 %all-to-all-done.2 = bf16[4,14,384]{2,1,0:T(8,128)(2,1)S(1)} async-done(((bf16[4,14,384]{2,1,0:T(8,128)(2,1)}), bf16[4,14,384]{2,1,0:T(8,128)(2,1)S(1)}, u32[]{:S(2)}, u32[]{:S(2)}) %all-to-all-start.2) | async-done | bytes 43040 | tf_op jit(solution)/shard_map/all_to_all | solution.py:38
  152.1 0.6 convert_reduce_fusion
  (33 shorter events, 0.9 us)
Async XLA Ops:
  0.6 9.1 %copy-start = (bf16[256,1344]{0,1:T(8,128)(2,1)S(1)}, bf16[256,1344]{0,1:T(8,128)(2,1)}, u32[]{:S(2)}) copy-start(bf16[256,1344]{0,1:T(8,128)(2,1)} %param.7) | copy-start | bytes 2064388
  2.2 18.7 %all-to-all-start = ((bf16[8,14,1152]{2,1,0:T(8,128)(2,1)}), bf16[8,14,1152]{2,1,0:T(8,128)(2,1)S(1)}, u32[]{:S(2)}, u32[]{:S(2)}) async-start(bf16[8,14,1152]{2,1,0:T(8,128)(2,1)} %broadcast_in_dim.23), calls=%async_computation | async-start | bytes 589824 | tf_op jit(solution)/shard_map/all_to_all | solution.py:32
  21.1 7.2 %collective-permute-start = (bf16[56,1152]{1,0:T(8,128)(2,1)S(1)}, bf16[56,1152]{1,0:T(8,128)(2,1)S(1)}, u32[]{:S(2)}, u32[]{:S(2)}) collective-permute-start(bf16[56,1152]{1,0:T(8,128)(2,1)S(1)} %slice.85), channel_id=1, source_target_pairs={{0,64},{1,705},{64,0},{65,129},{128,192},{129,65},{192,128},{193,2... | collective-permute-start | bytes 387080 | tf_op jit(solution)/shard_map/ppermute | solution.py:27
  25.4 17.2 %collective-permute-start.1 = (bf16[56,1152]{1,0:T(8,128)(2,1)S(1)}, bf16[56,1152]{1,0:T(8,128)(2,1)S(1)}, u32[]{:S(2)}, u32[]{:S(2)}) collective-permute-start(bf16[56,1152]{1,0:T(8,128)(2,1)S(1)} %slice.87), channel_id=1, source_target_pairs={{0,64},{1,705},{64,0},{65,129},{128,192},{129,65},{192,128},{193,2... | collective-permute-start | bytes 387080 | tf_op jit(solution)/shard_map/ppermute | solution.py:27
  28.3 18.5 %collective-permute-start.2 = (bf16[2,56,1152]{2,1,0:T(8,128)(2,1)S(1)}, bf16[2,56,1152]{2,1,0:T(8,128)(2,1)S(1)}, u32[]{:S(2)}, u32[]{:S(2)}) collective-permute-start(bf16[2,56,1152]{2,1,0:T(8,128)(2,1)S(1)} %pad_maximum_fusion), channel_id=1, source_target_pairs={{0,704},{1,65},{64,128},{65,1},{128,64},{129,193},{192,256},{193,1... | collective-permute-start | bytes 774152 | tf_op jit(solution)/shard_map/ppermute | solution.py:27
  42.6 54.0 %copy-start.3 = (bf16[256,1344]{0,1:T(8,128)(2,1)S(1)}, bf16[256,1344]{0,1:T(8,128)(2,1)}, u32[]{:S(2)}) copy-start(bf16[256,1344]{0,1:T(8,128)(2,1)} %param.6) | copy-start | bytes 2064388
  42.7 12.2 %collective-permute-start.3 = (bf16[2,56,1152]{2,1,0:T(8,128)(2,1)S(1)}, bf16[2,56,1152]{2,1,0:T(8,128)(2,1)S(1)}, u32[]{:S(2)}, u32[]{:S(2)}) collective-permute-start(bf16[2,56,1152]{2,1,0:T(8,128)(2,1)S(1)} %pad_maximum_fusion.1), channel_id=1, source_target_pairs={{0,704},{1,65},{64,128},{65,1},{128,64},{129,193},{192,256},{193,1... | collective-permute-start | bytes 774152 | tf_op jit(solution)/shard_map/ppermute | solution.py:27
  46.9 10.1 %collective-permute-start.4 = (bf16[2,56,1152]{2,1,0:T(8,128)(2,1)S(1)}, bf16[2,56,1152]{2,1,0:T(8,128)(2,1)S(1)}, u32[]{:S(2)}, u32[]{:S(2)}) collective-permute-start(bf16[2,56,1152]{2,1,0:T(8,128)(2,1)S(1)} %collective-permute-done.2), channel_id=1, source_target_pairs={{0,64},{1,705},{64,0},{65,129},{128,192},{129,65},{192,128},{193,2... | collective-permute-start | bytes 774152 | tf_op jit(solution)/shard_map/ppermute | solution.py:27
  54.9 10.3 %collective-permute-start.5 = (bf16[2,56,1152]{2,1,0:T(8,128)(2,1)S(1)}, bf16[2,56,1152]{2,1,0:T(8,128)(2,1)S(1)}, u32[]{:S(2)}, u32[]{:S(2)}) collective-permute-start(bf16[2,56,1152]{2,1,0:T(8,128)(2,1)S(1)} %collective-permute-done.3), channel_id=1, source_target_pairs={{0,64},{1,705},{64,0},{65,129},{128,192},{129,65},{192,128},{193,2... | collective-permute-start | bytes 774152 | tf_op jit(solution)/shard_map/ppermute | solution.py:27
  56.9 11.5 %collective-permute-start.6 = (bf16[2,56,1152]{2,1,0:T(8,128)(2,1)S(1)}, bf16[2,56,1152]{2,1,0:T(8,128)(2,1)S(1)}, u32[]{:S(2)}, u32[]{:S(2)}) collective-permute-start(bf16[2,56,1152]{2,1,0:T(8,128)(2,1)S(1)} %collective-permute-done.4), channel_id=1, source_target_pairs={{0,704},{1,65},{64,128},{65,1},{128,64},{129,193},{192,256},{193,1... | collective-permute-start | bytes 774152 | tf_op jit(solution)/shard_map/ppermute | solution.py:27
  65.2 11.0 %collective-permute-start.7 = (bf16[2,56,1152]{2,1,0:T(8,128)(2,1)S(1)}, bf16[2,56,1152]{2,1,0:T(8,128)(2,1)S(1)}, u32[]{:S(2)}, u32[]{:S(2)}) collective-permute-start(bf16[2,56,1152]{2,1,0:T(8,128)(2,1)S(1)} %collective-permute-done.5), channel_id=1, source_target_pairs={{0,704},{1,65},{64,128},{65,1},{128,64},{129,193},{192,256},{193,1... | collective-permute-start | bytes 774152 | tf_op jit(solution)/shard_map/ppermute | solution.py:27
  68.4 9.8 %collective-permute-start.8 = (bf16[2,56,1152]{2,1,0:T(8,128)(2,1)S(1)}, bf16[2,56,1152]{2,1,0:T(8,128)(2,1)S(1)}, u32[]{:S(2)}, u32[]{:S(2)}) collective-permute-start(bf16[2,56,1152]{2,1,0:T(8,128)(2,1)S(1)} %collective-permute-done.6), channel_id=1, source_target_pairs={{0,64},{1,705},{64,0},{65,129},{128,192},{129,65},{192,128},{193,2... | collective-permute-start | bytes 774152 | tf_op jit(solution)/shard_map/ppermute | solution.py:27
  76.2 10.9 %collective-permute-start.9 = (bf16[2,56,1152]{2,1,0:T(8,128)(2,1)S(1)}, bf16[2,56,1152]{2,1,0:T(8,128)(2,1)S(1)}, u32[]{:S(2)}, u32[]{:S(2)}) collective-permute-start(bf16[2,56,1152]{2,1,0:T(8,128)(2,1)S(1)} %collective-permute-done.7), channel_id=1, source_target_pairs={{0,64},{1,705},{64,0},{65,129},{128,192},{129,65},{192,128},{193,2... | collective-permute-start | bytes 774152 | tf_op jit(solution)/shard_map/ppermute | solution.py:27
  78.2 13.3 %collective-permute-start.10 = (bf16[2,56,1152]{2,1,0:T(8,128)(2,1)S(1)}, bf16[2,56,1152]{2,1,0:T(8,128)(2,1)S(1)}, u32[]{:S(2)}, u32[]{:S(2)}) collective-permute-start(bf16[2,56,1152]{2,1,0:T(8,128)(2,1)S(1)} %collective-permute-done.8), channel_id=1, source_target_pairs={{0,704},{1,65},{64,128},{65,1},{128,64},{129,193},{192,256},{193,1... | collective-permute-start | bytes 774152 | tf_op jit(solution)/shard_map/ppermute | solution.py:27
  87.1 9.4 %collective-permute-start.11 = (bf16[2,56,1152]{2,1,0:T(8,128)(2,1)S(1)}, bf16[2,56,1152]{2,1,0:T(8,128)(2,1)S(1)}, u32[]{:S(2)}, u32[]{:S(2)}) collective-permute-start(bf16[2,56,1152]{2,1,0:T(8,128)(2,1)S(1)} %collective-permute-done.9), channel_id=1, source_target_pairs={{0,704},{1,65},{64,128},{65,1},{128,64},{129,193},{192,256},{193,1... | collective-permute-start | bytes 774152 | tf_op jit(solution)/shard_map/ppermute | solution.py:27
  96.6 1.6 %copy-start.1 = (bf16[12,112,1152]{2,1,0:T(8,128)(2,1)}, bf16[12,112,1152]{2,1,0:T(8,128)(2,1)S(1)}, u32[]{:S(2)}) copy-start(bf16[12,112,1152]{2,1,0:T(8,128)(2,1)S(1)} %slice_dynamic-update-slice_fusion) | copy-start | bytes 9289732
  99.8 36.0 %all-to-all-start.1 = ((bf16[24,56,384]{2,1,0:T(8,128)(2,1)}), bf16[24,56,384]{2,1,0:T(8,128)(2,1)S(1)}, u32[]{:S(2)}, u32[]{:S(2)}) async-start(bf16[24,56,384]{2,1,0:T(8,128)(2,1)} %bitcast.7), calls=%async_computation.1 | async-start | bytes 2064384 | tf_op jit(solution)/shard_map/all_to_all | solution.py:38
  105.9 2.2 %copy-start.2 = (bf16[12,112,1152]{2,1,0:T(8,128)(2,1)S(1)}, bf16[12,112,1152]{2,1,0:T(8,128)(2,1)}, u32[]{:S(2)}) copy-start(bf16[12,112,1152]{2,1,0:T(8,128)(2,1)} %copy-done.1) | copy-start | bytes 9289732
  108.9 3.5 %collective-permute-start.12 = (bf16[672,256]{1,0:T(8,128)(2,1)S(1)}, bf16[672,256]{1,0:T(8,128)(2,1)S(1)}, u32[]{:S(2)}, u32[]{:S(2)}) collective-permute-start(bf16[672,256]{1,0:T(8,128)(2,1)S(1)} %constant_dynamic-slice_fusion), channel_id=1, source_target_pairs={{0,1},{1,0},{2,3},{3,2},{4,5},{5,4},{6,7},{7,6},{8,9},{9,8},{10,11... | collective-permute-start | bytes 1032200 | tf_op jit(solution)/shard_map/ppermute | solution.py:17
  112.5 9.1 %collective-permute-start.13 = (bf16[672,256]{1,0:T(8,128)(2,1)S(1)}, bf16[672,256]{1,0:T(8,128)(2,1)S(1)}, u32[]{:S(2)}, u32[]{:S(2)}) collective-permute-start(bf16[672,256]{1,0:T(8,128)(2,1)S(1)} %add_convert_fusion.2), channel_id=1, source_target_pairs={{0,2},{1,7},{2,0},{3,5},{4,6},{5,3},{6,4},{7,1},{8,10},{9,15},{10,... | collective-permute-start | bytes 1032200 | tf_op jit(solution)/shard_map/ppermute | solution.py:27
  121.8 10.4 %collective-permute-start.14 = (bf16[672,256]{1,0:T(8,128)(2,1)S(1)}, bf16[672,256]{1,0:T(8,128)(2,1)S(1)}, u32[]{:S(2)}, u32[]{:S(2)}) collective-permute-start(bf16[672,256]{1,0:T(8,128)(2,1)S(1)} %add_convert_fusion.1), channel_id=1, source_target_pairs={{0,6},{1,3},{2,4},{3,1},{4,2},{5,7},{6,0},{7,5},{8,14},{9,11},{10,... | collective-permute-start | bytes 1032200 | tf_op jit(solution)/shard_map/ppermute | solution.py:27
  132.2 3.5 %collective-permute-start.15 = (bf16[672,256]{1,0:T(8,128)(2,1)S(1)}, bf16[672,256]{1,0:T(8,128)(2,1)S(1)}, u32[]{:S(2)}, u32[]{:S(2)}) collective-permute-start(bf16[672,256]{1,0:T(8,128)(2,1)S(1)} %add_convert_fusion), channel_id=1, source_target_pairs={{0,1},{1,0},{2,3},{3,2},{4,5},{5,4},{6,7},{7,6},{8,9},{9,8},{10,11... | collective-permute-start | bytes 1032200 | tf_op jit(solution)/shard_map/ppermute | solution.py:17
  136.6 15.5 %all-to-all-start.2 = ((bf16[4,14,384]{2,1,0:T(8,128)(2,1)}), bf16[4,14,384]{2,1,0:T(8,128)(2,1)S(1)}, u32[]{:S(2)}, u32[]{:S(2)}) async-start(bf16[4,14,384]{2,1,0:T(8,128)(2,1)} %reshape.22), calls=%async_computation.2 | async-start | bytes 98304 | tf_op jit(solution)/shard_map/all_to_all | solution.py:38

commit v3 on v2

v3 whole, which is shorter than its diff:
```python
import jax
import jax.numpy as jnp
import numpy as np
from jax import lax
from jax.sharding import Mesh
from jax.sharding import PartitionSpec as P


FAR = 4
FS_0 = ("fs_0h", "fs_0l")
FS_1 = ("fs_1h", "fs_1l")
FS = (*FS_0, *FS_1)


def shifted(array, axis, step):
    peers = lax.axis_size(axis)
    return lax.ppermute(array, axis, [(k, (k + step) % peers) for k in range(peers)])


def sent_to_all(array, axis):
    peers = lax.axis_size(axis)
    return lax.all_to_all(
        jnp.broadcast_to(array[None], (peers, *array.shape)), axis, 0, 0, tiled=True
    )


def exchanged(parts, axis):
    got = lax.all_to_all(parts, axis, 0, 0, tiled=True)
    return got.astype(jnp.float32).sum(axis=0)


def contract_rows(left, right):
    return lax.dot_general(
        left, right, (((0,), (0,)), ((), ())), preferred_element_type=jnp.float32
    )


def contract_cols(left, right):
    return lax.dot_general(
        left, right, (((1,), (1,)), ((), ())), preferred_element_type=jnp.float32
    )


def picked(source):
    source = jnp.asarray(source, jnp.int32)
    spot = lax.broadcasted_iota(jnp.int32, (source.size, source.size), 1)
    return (source[:, None] == spot).astype(jnp.bfloat16)


def gathered(block):
    block = sent_to_all(block, (FS_0[0], FS_1[0]))
    block = block.reshape(-1, block.shape[2])
    rows, columns = block.shape
    near = lax.axis_size(FS_0[1])
    place = lax.axis_index(FS_0[1])
    held = jnp.zeros((near, rows, columns), block.dtype)
    for part, owner in (
        (block, place),
        (shifted(block, FS_0, 1), (place + near - 1) % near),
        (shifted(block, FS_0, -1), (place + 1) % near),
    ):
        held = lax.dynamic_update_slice(held, part[None], (owner, 0, 0))
    held = held.reshape(near * rows, columns)
    half = near * rows // 2
    side = lax.axis_index(FS_1[1])
    whole = jnp.zeros((2, near * rows, columns), block.dtype)
    for part, owner, start in (
        (held, side, 0),
        (shifted(held[:half], FS_1, -1), 1 - side, 0),
        (shifted(held[half:], FS_1, 1), 1 - side, half),
    ):
        whole = lax.dynamic_update_slice(whole, part[None], (owner, start, 0))
    return whole.reshape(2 * near * rows, columns)


def paired(array, turn):
    chips = lax.axis_size("chip")
    pairs = []
    for chip in range(chips):
        for core in range(2):
            other = (chip + (1 if (chip + core + turn) % 2 == 0 else -1)) % chips
            pairs.append((2 * chip + core, 2 * other + core))
    return lax.ppermute(array, ("chip", "core"), pairs)


def added(left, right):
    return (left.astype(jnp.float32) + right.astype(jnp.float32)).astype(jnp.bfloat16)


def summed_over_tp(partial):
    half = partial.shape[0] // 2
    core = lax.axis_index("core")
    kept = lax.dynamic_slice_in_dim(partial, core * half, half)
    given = lax.dynamic_slice_in_dim(partial, (1 - core) * half, half)
    total = added(kept, shifted(given, "core", 1))
    total = added(total, paired(total, 0))
    other = paired(total, 1)
    total = added(total, other)
    other = shifted(total, "core", 1)
    first = jnp.where(core == 0, total, other)
    second = jnp.where(core == 0, other, total)
    return jnp.concatenate([first, second])


def gradients(tokens, cotangent, gate_weight, up_weight, down_weight):
    near, inner = lax.axis_size("fs_0l"), lax.axis_size(FS_1)
    rows, units = gate_weight.shape
    width = tokens.shape[1]

    weights = gathered(jnp.concatenate([gate_weight, up_weight, down_weight.T], axis=1))
    gate_up, down = weights[:, : 2 * units], weights[:, 2 * units :]

    spot = np.arange(width).reshape(FAR, near, inner // 2, 2, rows)
    held = spot.transpose(3, 1, 0, 2, 4).reshape(-1)
    sent = spot.transpose(2, 3, 1, 0, 4).reshape(-1)
    into, back = picked(held), picked(np.argsort(held))
    into, back = lax.optimization_barrier((into, back))
    held_tokens = contract_cols(into, tokens).astype(jnp.bfloat16)
    held_cotangent = contract_cols(into, cotangent).astype(jnp.bfloat16)
    sent_cotangent = contract_cols(picked(sent), cotangent).astype(jnp.bfloat16)
    held_tokens, held_cotangent, sent_cotangent = lax.optimization_barrier(
        (held_tokens, held_cotangent, sent_cotangent)
    )

    both = contract_rows(held_tokens, gate_up)
    gate_pre, up_pre = both[:, :units], both[:, units:]
    sigmoid_gate = jax.nn.sigmoid(gate_pre)
    activated = gate_pre * sigmoid_gate
    hidden = (activated * up_pre).astype(jnp.bfloat16)

    terms = jnp.dot(sent_cotangent, hidden, preferred_element_type=jnp.float32)
    terms = terms.astype(jnp.bfloat16).reshape(inner * near, FAR * rows, units)
    terms = exchanged(terms, (*FS_1, "fs_0l"))
    terms = terms.astype(jnp.bfloat16).reshape(FAR, rows, units)
    down_grad = exchanged(terms, "fs_0h").T

    hidden_grad = contract_rows(held_cotangent, down)
    gate_pre_grad = (
        hidden_grad * up_pre * sigmoid_gate * (1.0 + gate_pre * (1.0 - sigmoid_gate))
    ).astype(jnp.bfloat16)
    up_pre_grad = (hidden_grad * activated).astype(jnp.bfloat16)
    partial = contract_cols(gate_up, jnp.concatenate([gate_pre_grad, up_pre_grad], axis=1))
    partial = jnp.dot(back, partial.astype(jnp.bfloat16), preferred_element_type=jnp.float32)
    total = summed_over_tp(partial.astype(jnp.bfloat16))
    return (total.T, down_grad)


def solution(mesh):
    torus = Mesh(
        mesh.devices.reshape(FAR, 12 // FAR, 4, 2, mesh.shape["tp"] // 2, 2), (*FS, "chip", "core")
    )
    tp = ("chip", "core")
    in_specs = (P(FS, None), P(FS, None), P(FS, tp), P(FS, tp), P(tp, FS))
    out_specs = (P(FS, None), P(tp, FS))
    return jax.shard_map(
        gradients, mesh=torus, in_specs=in_specs, out_specs=out_specs, check_vma=False
    )
```

time: 154 us -> 169 us (1.097)
  matrix products: 7.25 us -> 21.4 us
  starting transfers between devices: 75.1 us -> 66.6 us
  other arithmetic: 2.84 us -> 7.42 us
  local copies, waits for them, and re-layouts: 3.46 us -> 6.77 us
  waiting for transfers between devices: 63 us -> 65 us
    ppermute x14 -> x2, starting transfers between devices: 52.6 us -> 5.12 us  [paired(): return lax.ppermute(array, ('chip', 'core'), pairs)]
    ppermute x14 -> x2, waiting for transfers between devices: 41.2 us -> 14.4 us  [paired(): return lax.ppermute(array, ('chip', 'core'), pairs)]
    ppermute x2 -> x6, waiting for transfers between devices: 3.23 us -> 26.2 us  [shifted(): lax.ppermute(array, axis, [(k, (k + step) % peers) for k in range(peers)])]
    ppermute x2 -> x6, starting transfers between devices: 3.84 us -> 26.6 us  [shifted(): lax.ppermute(array, axis, [(k, (k + step) % peers) for k in range(peers)])]
    all_to_all x1, starting transfers between devices: 7.55 us -> 19 us  [sent_to_all(): lax.all_to_all(jnp.broadcast_to(array[None], (peers, *array.shape)), axis...]
    dot_general x2 -> x3, matrix products: 2.9 us -> 10.9 us  [contract_cols(): lax.dot_general(left, right, (((1,), (1,)), ((), ())), preferred_element_...]
    dot_general x3 -> x4, matrix products: 4.35 us -> 10.6 us  [the longest x1 5.5 us: gradients(): jnp.dot(back, partial.astype(jnp.bfloat16), preferred_element_type=jnp.fl...]
    all_to_all x1, waiting for transfers between devices: 8.86 us -> 14.8 us  [sent_to_all(): lax.all_to_all(jnp.broadcast_to(array[None], (peers, *array.shape)), axis...]
  transfers between devices with their start and end apart: 19 -> 11, of which waited for: 13 -> 10; matrix products, arithmetic and copies ran while one was open for 4% -> 17% of each run, Pallas kernels for 0% -> 0%
where the time goes in v3:
time: 169 us; the launch traced here: 168 us
  starting transfers between devices  66.6 us (39%)
  waiting for transfers between devices  65 us (38%)
  matrix products  21.4 us (13%)
  other arithmetic  7.42 us (4%)
  local copies, waits for them, and re-layouts  6.77 us (4%)
    ppermute x6, starting transfers between devices, shifted(): lax.ppermute(array, axis, [(k, (k + step) % peers) for k in range(peers)])  26.6 us
    ppermute x6, waiting for transfers between devices, shifted(): lax.ppermute(array, axis, [(k, (k + step) % peers) for k in range(peers)])  26.2 us
    all_to_all x1, starting transfers between devices, sent_to_all(): lax.all_to_all(jnp.broadcast_to(array[None], (peers, *array.shape)), axis...  19 us
    all_to_all x2, starting transfers between devices, exchanged(): got = lax.all_to_all(parts, axis, 0, 0, tiled=True)  15.9 us
    all_to_all x1, waiting for transfers between devices, sent_to_all(): lax.all_to_all(jnp.broadcast_to(array[None], (peers, *array.shape)), axis...  14.8 us
    ppermute x2, waiting for transfers between devices, paired(): return lax.ppermute(array, ('chip', 'core'), pairs)  14.4 us
    dot_general x3, matrix products, contract_cols(): lax.dot_general(left, right, (((1,), (1,)), ((), ())), preferred_element_...  10.9 us
    all_to_all x2, waiting for transfers between devices, exchanged(): got = lax.all_to_all(parts, axis, 0, 0, tiled=True)  9.64 us
  transfers between devices with their start and end apart: 11, of which 10 were waited for; matrix products, arithmetic and copies ran while one was open for 17% of the time, Pallas kernels for 0%

profile of v3, /device:TPU:14, one launch (start us, length us, event | category | flops | bytes accessed | tf_op | source)
XLA Modules:
  0.0 168.1 jit_solution(15301426625599648831)
XLA Ops:
  0.6 0.0 copy-start
  0.6 0.8 pad_maximum_fusion
  1.5 0.9 broadcast_in_dim.29
  2.3 19.0 %all-to-all-start = ((bf16[16,14,1152]{2,1,0:T(8,128)(2,1)}), bf16[16,14,1152]{2,1,0:T(8,128)(2,1)S(1)}, u32[]{:S(2)}, u32[]{:S(2)}) async-start(bf16[16,14,1152]{2,1,0:T(8,128)(2,1)} %broadcast_in_dim.29), calls=%async_computation | async-start | bytes 1179648 | tf_op jit(solution)/shard_map/all_to_all | solution.py:22
  21.3 4.6 %fusion = (bf16[1344,1344]{1,0:T(8,128)(2,1)}, bf16[1344,1344]{1,0:T(8,128)(2,1)}) fusion(s32[1344]{0:T(1024)} %constant.52.clone, s32[1344]{0:T(1024)} %constant.53.clone), kind=kLoop, calls=%fused_computation.3 | loop fusion | flops 7225344 | bytes 7236096 | tf_op jit(solution)/shard_map/convert_element_type | solution.py:47
  26.0 14.8 %all-to-all-done = bf16[16,14,1152]{2,1,0:T(8,128)(2,1)S(1)} async-done(((bf16[16,14,1152]{2,1,0:T(8,128)(2,1)}), bf16[16,14,1152]{2,1,0:T(8,128)(2,1)S(1)}, u32[]{:S(2)}, u32[]{:S(2)}) %all-to-all-start) | async-done | bytes 516128 | tf_op jit(solution)/shard_map/all_to_all | solution.py:22
  40.8 0.9 reshape.23
  41.8 12.1 %collective-permute-start = (bf16[224,1152]{1,0:T(8,128)(2,1)}, bf16[224,1152]{1,0:T(8,128)(2,1)}, u32[]{:S(2)}, u32[]{:S(2)}) collective-permute-start(bf16[224,1152]{1,0:T(8,128)(2,1)} %reshape.23), channel_id=1, source_target_pairs={{0,64},{64,128},{128,192},{192,256},{256,320},{320,384},{384,448},... | collective-permute-start | bytes 1548296 | tf_op jit(solution)/shard_map/ppermute | solution.py:17
  53.9 0.0 copy-done
  53.9 4.2 %convolution_convert_fusion.3 = bf16[1344,256]{1,0:T(8,128)(2,1)} fusion(bf16[1344,1344]{1,0:T(8,128)(2,1)} %get-tuple-element.8, bf16[256,1344]{0,1:T(8,128)(2,1)S(1)} %copy-done), kind=kOutput, calls=%fused_computation.10 | convolution fusion | flops 925188096 | bytes 4988928 | tf_op jit(solution)/shard_map/dot_general | solution.py:39
  58.0 4.4 %collective-permute-start.1 = (bf16[224,1152]{1,0:T(8,128)(2,1)}, bf16[224,1152]{1,0:T(8,128)(2,1)S(1)}, u32[]{:S(2)}, u32[]{:S(2)}) collective-permute-start(bf16[224,1152]{1,0:T(8,128)(2,1)} %reshape.23), channel_id=1, source_target_pairs={{0,704},{64,0},{128,64},{192,128},{256,192},{320,256},{384,320},{4... | collective-permute-start | bytes 1548296 | tf_op jit(solution)/shard_map/ppermute | solution.py:17
  62.4 0.2 broadcast_in_dim_reshape.6
  62.6 0.1 broadcast_in_dim.28
  62.7 0.0 copy-start.3
  62.7 0.1 constant_dynamic-update-slice_fusion
  62.8 3.3 %collective-permute-done = bf16[224,1152]{1,0:T(8,128)(2,1)} collective-permute-done((bf16[224,1152]{1,0:T(8,128)(2,1)}, bf16[224,1152]{1,0:T(8,128)(2,1)}, u32[]{:S(2)}, u32[]{:S(2)}) %collective-permute-start) | collective-permute-done | bytes 516128 | tf_op jit(solution)/shard_map/ppermute | solution.py:17
  66.1 1.1 bitcast_dynamic-update-slice_fusion.4
  67.2 4.9 %collective-permute-done.1 = bf16[224,1152]{1,0:T(8,128)(2,1)S(1)} collective-permute-done((bf16[224,1152]{1,0:T(8,128)(2,1)}, bf16[224,1152]{1,0:T(8,128)(2,1)S(1)}, u32[]{:S(2)}, u32[]{:S(2)}) %collective-permute-start.1) | collective-permute-done | bytes 516128 | tf_op jit(solution)/shard_map/ppermute | solution.py:17
  72.1 0.1 bitcast_dynamic-update-slice_fusion.3
  72.1 1.0 fusion.23
  73.1 3.7 %collective-permute-start.2 = (bf16[336,1152]{1,0:T(8,128)(2,1)}, bf16[336,1152]{1,0:T(8,128)(2,1)}, u32[]{:S(2)}, u32[]{:S(2)}) collective-permute-start(bf16[336,1152]{1,0:T(8,128)(2,1)} %get-tuple-element.13), channel_id=1, source_target_pairs={{0,56},{8,0},{16,8},{24,16},{32,24},{40,32},{48,40},{56,48},{1,57}... | collective-permute-start | bytes 2322440 | tf_op jit(solution)/shard_map/ppermute | solution.py:17
  76.8 0.0 copy-done.3
  76.8 2.4 %fusion.4 = bf16[1344,256]{1,0:T(8,128)(2,1)} fusion(bf16[256,1344]{0,1:T(8,128)(2,1)S(1)} %copy-done, s32[1344]{0:T(1024)S(1)} %copy-done.3), kind=kOutput, calls=%fused_computation.12 | convolution fusion | flops 926994432 | bytes 1381632 | tf_op jit(solution)/shard_map/dot_general | solution.py:39
  79.2 4.3 %convolution_convert_fusion.4 = bf16[1344,256]{1,0:T(8,128)(2,1)} fusion(bf16[1344,1344]{1,0:T(8,128)(2,1)} %get-tuple-element.8, bf16[256,1344]{0,1:T(8,128)(2,1)} %param.8), kind=kOutput, calls=%fused_computation.11 | convolution fusion | flops 925188096 | bytes 4988928 | tf_op jit(solution)/shard_map/dot_general | solution.py:39
  83.5 2.5 %collective-permute-start.3 = (bf16[336,1152]{1,0:T(8,128)(2,1)S(1)}, bf16[336,1152]{1,0:T(8,128)(2,1)S(1)}, u32[]{:S(2)}, u32[]{:S(2)}) collective-permute-start(bf16[336,1152]{1,0:T(8,128)(2,1)S(1)} %get-tuple-element.12), channel_id=1, source_target_pairs={{0,8},{8,16},{16,24},{24,32},{32,40},{40,48},{48,56},{56,0},{1,9},... | collective-permute-start | bytes 2322440 | tf_op jit(solution)/shard_map/ppermute | solution.py:17
  86.1 0.2 broadcast_in_dim.27
  86.3 0.0 copy-start.2
  86.3 0.2 bitcast_dynamic-update-slice_fusion
  86.6 0.0 copy-start.4
  86.6 6.5 %collective-permute-done.2 = bf16[336,1152]{1,0:T(8,128)(2,1)} collective-permute-done((bf16[336,1152]{1,0:T(8,128)(2,1)}, bf16[336,1152]{1,0:T(8,128)(2,1)}, u32[]{:S(2)}, u32[]{:S(2)}) %collective-permute-start.2) | collective-permute-done | bytes 774176 | tf_op jit(solution)/shard_map/ppermute | solution.py:17
  93.0 1.2 bitcast_dynamic-update-slice_fusion.2
  94.3 8.3 %collective-permute-done.3 = bf16[336,1152]{1,0:T(8,128)(2,1)S(1)} collective-permute-done((bf16[336,1152]{1,0:T(8,128)(2,1)S(1)}, bf16[336,1152]{1,0:T(8,128)(2,1)S(1)}, u32[]{:S(2)}, u32[]{:S(2)}) %collective-permute-start.3) | collective-permute-done | bytes 774176 | tf_op jit(solution)/shard_map/ppermute | solution.py:17
  102.6 0.1 bitcast_dynamic-update-slice_fusion.1
  102.7 0.0 copy-start.1
  102.7 0.0 copy-done.2
  102.7 0.8 fusion.6
  103.5 0.0 copy-done.4
  103.5 0.0 copy-start.5
  103.5 1.7 convolution_convert_fusion
  105.2 0.0 copy-done.1
  105.2 7.1 %all-to-all-start.1 = ((bf16[24,56,384]{2,1,0:T(8,128)(2,1)}), bf16[24,56,384]{2,1,0:T(8,128)(2,1)S(1)}, u32[]{:S(2)}, u32[]{:S(2)}) async-start(bf16[24,56,384]{2,1,0:T(8,128)(2,1)} %bitcast.9), calls=%async_computation.1 | async-start | bytes 2064384 | tf_op jit(solution)/shard_map/all_to_all | solution.py:28
  112.3 0.0 copy-done.5
  112.3 2.6 %multiply_convert_fusion.2 = (bf16[256,384]{1,0:T(8,128)(2,1)S(1)}, bf16[256,384]{1,0:T(8,128)(2,1)}) fusion(f32[256,768]{1,0:T(8,128)S(1)} %fusion.6, bf16[1344,256]{1,0:T(8,128)(2,1)S(1)} %copy-done.5, bf16[1344,1152]{1,0:T(8,128)(2,1)} %bitcast.30), kind=kOutput, calls=%fused_computation.32 | convolution fusion | flops 265519104 | bytes 2899968 | tf_op jit(solution)/shard_map/dot_general | solution.py:33
  114.9 5.5 %convolution_convert_fusion.1 = bf16[1344,256]{1,0:T(8,128)(2,1)S(1)} fusion(bf16[1344,1344]{1,0:T(8,128)(2,1)} %get-tuple-element.7, bf16[1344,1152]{1,0:T(8,128)(2,1)} %bitcast.31, bf16[256,384]{1,0:T(8,128)(2,1)} %get-tuple-element.15, bf16[256,384]{1,0:T(8,128)(2,1)S(1)} %get-tuple-element.14), kind=kOutput, calls=%fused_computation.8 | convolution fusion | flops 1454800896 | bytes 6930432 | tf_op jit(solution)/shard_map/dot_general | solution.py:143
  120.4 1.9 %collective-permute-start.4 = (bf16[672,256]{1,0:T(8,128)(2,1)S(1)}, bf16[672,256]{1,0:T(8,128)(2,1)S(1)}, u32[]{:S(2)}, u32[]{:S(2)}) collective-permute-start(bf16[672,256]{1,0:T(8,128)(2,1)S(1)} %constant_dynamic-slice_fusion), channel_id=1, source_target_pairs={{0,1},{1,0},{2,3},{3,2},{4,5},{5,4},{6,7},{7,6},{8,9},{9,8},{10,11... | collective-permute-start | bytes 1032200 | tf_op jit(solution)/shard_map/ppermute | solution.py:17
  122.4 1.6 collective-permute-done.4
  124.0 0.1 add_convert_fusion.2
  124.1 2.7 %collective-permute-start.5 = (bf16[672,256]{1,0:T(8,128)(2,1)S(1)}, bf16[672,256]{1,0:T(8,128)(2,1)S(1)}, u32[]{:S(2)}, u32[]{:S(2)}) collective-permute-start(bf16[672,256]{1,0:T(8,128)(2,1)S(1)} %add_convert_fusion.2), channel_id=1, source_target_pairs={{0,2},{1,7},{2,0},{3,5},{4,6},{5,3},{6,4},{7,1},{8,10},{9,15},{10,... | collective-permute-start | bytes 1032200 | tf_op jit(solution)/shard_map/ppermute | solution.py:83
  126.8 6.4 %collective-permute-done.5 = bf16[672,256]{1,0:T(8,128)(2,1)S(1)} collective-permute-done((bf16[672,256]{1,0:T(8,128)(2,1)S(1)}, bf16[672,256]{1,0:T(8,128)(2,1)S(1)}, u32[]{:S(2)}, u32[]{:S(2)}) %collective-permute-start.5) | collective-permute-done | bytes 344096 | tf_op jit(solution)/shard_map/ppermute | solution.py:83
  133.2 0.1 add_convert_fusion.1
  133.3 2.4 %collective-permute-start.6 = (bf16[672,256]{1,0:T(8,128)(2,1)S(1)}, bf16[672,256]{1,0:T(8,128)(2,1)S(1)}, u32[]{:S(2)}, u32[]{:S(2)}) collective-permute-start(bf16[672,256]{1,0:T(8,128)(2,1)S(1)} %add_convert_fusion.1), channel_id=1, source_target_pairs={{0,6},{1,3},{2,4},{3,1},{4,2},{5,7},{6,0},{7,5},{8,14},{9,11},{10,... | collective-permute-start | bytes 1032200 | tf_op jit(solution)/shard_map/ppermute | solution.py:83
  135.7 8.0 %collective-permute-done.6 = bf16[672,256]{1,0:T(8,128)(2,1)S(1)} collective-permute-done((bf16[672,256]{1,0:T(8,128)(2,1)S(1)}, bf16[672,256]{1,0:T(8,128)(2,1)S(1)}, u32[]{:S(2)}, u32[]{:S(2)}) %collective-permute-start.6) | collective-permute-done | bytes 344096 | tf_op jit(solution)/shard_map/ppermute | solution.py:83
  143.7 0.1 add_convert_fusion
  143.7 1.9 %collective-permute-start.7 = (bf16[672,256]{1,0:T(8,128)(2,1)S(1)}, bf16[672,256]{1,0:T(8,128)(2,1)S(1)}, u32[]{:S(2)}, u32[]{:S(2)}) collective-permute-start(bf16[672,256]{1,0:T(8,128)(2,1)S(1)} %add_convert_fusion), channel_id=1, source_target_pairs={{0,1},{1,0},{2,3},{3,2},{4,5},{5,4},{6,7},{7,6},{8,9},{9,8},{10,11... | collective-permute-start | bytes 1032200 | tf_op jit(solution)/shard_map/ppermute | solution.py:17
  145.7 1.6 collective-permute-done.7
  147.3 0.0 all-to-all-done.1
  147.3 0.1 reduce_sum.21
  147.5 0.6 reshape.27
  148.1 8.8 %all-to-all-start.2 = ((bf16[4,14,384]{2,1,0:T(8,128)(2,1)}), bf16[4,14,384]{2,1,0:T(8,128)(2,1)S(1)}, u32[]{:S(2)}, u32[]{:S(2)}) async-start(bf16[4,14,384]{2,1,0:T(8,128)(2,1)} %reshape.27), calls=%async_computation.2 | async-start | bytes 98304 | tf_op jit(solution)/shard_map/all_to_all | solution.py:28
  157.0 0.9 maximum_bitcast_fusion
  157.9 9.6 %all-to-all-done.2 = bf16[4,14,384]{2,1,0:T(8,128)(2,1)S(1)} async-done(((bf16[4,14,384]{2,1,0:T(8,128)(2,1)}), bf16[4,14,384]{2,1,0:T(8,128)(2,1)S(1)}, u32[]{:S(2)}, u32[]{:S(2)}) %all-to-all-start.2) | async-done | bytes 43040 | tf_op jit(solution)/shard_map/all_to_all | solution.py:28
  167.5 0.6 convert_reduce_fusion
  (2 shorter events, 0.1 us)
Async XLA Ops:
  0.6 53.2 %copy-start = (bf16[256,1344]{0,1:T(8,128)(2,1)S(1)}, bf16[256,1344]{0,1:T(8,128)(2,1)}, u32[]{:S(2)}) copy-start(bf16[256,1344]{0,1:T(8,128)(2,1)} %param.9) | copy-start | bytes 2064388
  2.3 38.5 %all-to-all-start = ((bf16[16,14,1152]{2,1,0:T(8,128)(2,1)}), bf16[16,14,1152]{2,1,0:T(8,128)(2,1)S(1)}, u32[]{:S(2)}, u32[]{:S(2)}) async-start(bf16[16,14,1152]{2,1,0:T(8,128)(2,1)} %broadcast_in_dim.29), calls=%async_computation | async-start | bytes 1179648 | tf_op jit(solution)/shard_map/all_to_all | solution.py:22
  41.8 24.3 %collective-permute-start = (bf16[224,1152]{1,0:T(8,128)(2,1)}, bf16[224,1152]{1,0:T(8,128)(2,1)}, u32[]{:S(2)}, u32[]{:S(2)}) collective-permute-start(bf16[224,1152]{1,0:T(8,128)(2,1)} %reshape.23), channel_id=1, source_target_pairs={{0,64},{64,128},{128,192},{192,256},{256,320},{320,384},{384,448},... | collective-permute-start | bytes 1548296 | tf_op jit(solution)/shard_map/ppermute | solution.py:17
  58.0 14.0 %collective-permute-start.1 = (bf16[224,1152]{1,0:T(8,128)(2,1)}, bf16[224,1152]{1,0:T(8,128)(2,1)S(1)}, u32[]{:S(2)}, u32[]{:S(2)}) collective-permute-start(bf16[224,1152]{1,0:T(8,128)(2,1)} %reshape.23), channel_id=1, source_target_pairs={{0,704},{64,0},{128,64},{192,128},{256,192},{320,256},{384,320},{4... | collective-permute-start | bytes 1548296 | tf_op jit(solution)/shard_map/ppermute | solution.py:17
  62.7 14.1 %copy-start.3 = (s32[1344]{0:T(1024)S(1)}, s32[1344]{0:T(1024)}, u32[]{:S(2)}) copy-start(s32[1344]{0:T(1024)} %constant.54.clone) | copy-start | bytes 16132
  73.1 19.9 %collective-permute-start.2 = (bf16[336,1152]{1,0:T(8,128)(2,1)}, bf16[336,1152]{1,0:T(8,128)(2,1)}, u32[]{:S(2)}, u32[]{:S(2)}) collective-permute-start(bf16[336,1152]{1,0:T(8,128)(2,1)} %get-tuple-element.13), channel_id=1, source_target_pairs={{0,56},{8,0},{16,8},{24,16},{32,24},{40,32},{48,40},{56,48},{1,57}... | collective-permute-start | bytes 2322440 | tf_op jit(solution)/shard_map/ppermute | solution.py:17
  83.5 19.0 %collective-permute-start.3 = (bf16[336,1152]{1,0:T(8,128)(2,1)S(1)}, bf16[336,1152]{1,0:T(8,128)(2,1)S(1)}, u32[]{:S(2)}, u32[]{:S(2)}) collective-permute-start(bf16[336,1152]{1,0:T(8,128)(2,1)S(1)} %get-tuple-element.12), channel_id=1, source_target_pairs={{0,8},{8,16},{16,24},{24,32},{32,40},{40,48},{48,56},{56,0},{1,9},... | collective-permute-start | bytes 2322440 | tf_op jit(solution)/shard_map/ppermute | solution.py:17
  86.3 16.4 %copy-start.2 = (bf16[1344,256]{1,0:T(8,128)(2,1)S(1)}, bf16[1344,256]{1,0:T(8,128)(2,1)}, u32[]{:S(2)}) copy-start(bf16[1344,256]{1,0:T(8,128)(2,1)} %convolution_convert_fusion.4) | copy-start | bytes 2064388
  86.6 17.0 %copy-start.4 = (bf16[1344,256]{1,0:T(8,128)(2,1)S(1)}, bf16[1344,256]{1,0:T(8,128)(2,1)}, u32[]{:S(2)}) copy-start(bf16[1344,256]{1,0:T(8,128)(2,1)} %fusion.4) | copy-start | bytes 2064388
  102.7 2.5 %copy-start.1 = (bf16[2,672,1152]{2,1,0:T(8,128)(2,1)}, bf16[2,672,1152]{2,1,0:T(8,128)(2,1)S(1)}, u32[]{:S(2)}) copy-start(bf16[2,672,1152]{2,1,0:T(8,128)(2,1)S(1)} %bitcast_dynamic-update-slice_fusion.1) | copy-start | bytes 9289732
  103.5 8.8 %copy-start.5 = (bf16[1344,256]{1,0:T(8,128)(2,1)S(1)}, bf16[1344,256]{1,0:T(8,128)(2,1)}, u32[]{:S(2)}) copy-start(bf16[1344,256]{1,0:T(8,128)(2,1)} %convolution_convert_fusion.3) | copy-start | bytes 2064388
  105.2 42.1 %all-to-all-start.1 = ((bf16[24,56,384]{2,1,0:T(8,128)(2,1)}), bf16[24,56,384]{2,1,0:T(8,128)(2,1)S(1)}, u32[]{:S(2)}, u32[]{:S(2)}) async-start(bf16[24,56,384]{2,1,0:T(8,128)(2,1)} %bitcast.9), calls=%async_computation.1 | async-start | bytes 2064384 | tf_op jit(solution)/shard_map/all_to_all | solution.py:28
  120.4 3.5 %collective-permute-start.4 = (bf16[672,256]{1,0:T(8,128)(2,1)S(1)}, bf16[672,256]{1,0:T(8,128)(2,1)S(1)}, u32[]{:S(2)}, u32[]{:S(2)}) collective-permute-start(bf16[672,256]{1,0:T(8,128)(2,1)S(1)} %constant_dynamic-slice_fusion), channel_id=1, source_target_pairs={{0,1},{1,0},{2,3},{3,2},{4,5},{5,4},{6,7},{7,6},{8,9},{9,8},{10,11... | collective-permute-start | bytes 1032200 | tf_op jit(solution)/shard_map/ppermute | solution.py:17
  124.1 9.1 %collective-permute-start.5 = (bf16[672,256]{1,0:T(8,128)(2,1)S(1)}, bf16[672,256]{1,0:T(8,128)(2,1)S(1)}, u32[]{:S(2)}, u32[]{:S(2)}) collective-permute-start(bf16[672,256]{1,0:T(8,128)(2,1)S(1)} %add_convert_fusion.2), channel_id=1, source_target_pairs={{0,2},{1,7},{2,0},{3,5},{4,6},{5,3},{6,4},{7,1},{8,10},{9,15},{10,... | collective-permute-start | bytes 1032200 | tf_op jit(solution)/shard_map/ppermute | solution.py:83
  133.3 10.4 %collective-permute-start.6 = (bf16[672,256]{1,0:T(8,128)(2,1)S(1)}, bf16[672,256]{1,0:T(8,128)(2,1)S(1)}, u32[]{:S(2)}, u32[]{:S(2)}) collective-permute-start(bf16[672,256]{1,0:T(8,128)(2,1)S(1)} %add_convert_fusion.1), channel_id=1, source_target_pairs={{0,6},{1,3},{2,4},{3,1},{4,2},{5,7},{6,0},{7,5},{8,14},{9,11},{10,... | collective-permute-start | bytes 1032200 | tf_op jit(solution)/shard_map/ppermute | solution.py:83
  143.7 3.5 %collective-permute-start.7 = (bf16[672,256]{1,0:T(8,128)(2,1)S(1)}, bf16[672,256]{1,0:T(8,128)(2,1)S(1)}, u32[]{:S(2)}, u32[]{:S(2)}) collective-permute-start(bf16[672,256]{1,0:T(8,128)(2,1)S(1)} %add_convert_fusion), channel_id=1, source_target_pairs={{0,1},{1,0},{2,3},{3,2},{4,5},{5,4},{6,7},{7,6},{8,9},{9,8},{10,11... | collective-permute-start | bytes 1032200 | tf_op jit(solution)/shard_map/ppermute | solution.py:17
  148.1 19.4 %all-to-all-start.2 = ((bf16[4,14,384]{2,1,0:T(8,128)(2,1)}), bf16[4,14,384]{2,1,0:T(8,128)(2,1)S(1)}, u32[]{:S(2)}, u32[]{:S(2)}) async-start(bf16[4,14,384]{2,1,0:T(8,128)(2,1)} %reshape.27), calls=%async_computation.2 | async-start | bytes 98304 | tf_op jit(solution)/shard_map/all_to_all | solution.py:28

commit v4 on v3

v4 whole, which is shorter than its diff:
```python
import jax
import jax.numpy as jnp
from jax import lax
from jax.sharding import Mesh
from jax.sharding import PartitionSpec as P


FAR = 4
FS_0 = ("fs_0h", "fs_0l")
FS = (*FS_0, "fs_1")
WIDE = ("fs_0h", "fs_1")


def shifted(array, axis, step):
    peers = lax.axis_size(axis)
    return lax.ppermute(array, axis, [(k, (k + step) % peers) for k in range(peers)])


def sent_to_all(array, axis):
    peers = lax.axis_size(axis)
    return lax.all_to_all(
        jnp.broadcast_to(array[None], (peers, *array.shape)), axis, 0, 0, tiled=True
    )


def exchanged(parts, axis):
    got = lax.all_to_all(parts, axis, 0, 0, tiled=True)
    return got.astype(jnp.float32).sum(axis=0)


def contract_rows(left, right):
    return lax.dot_general(
        left, right, (((0,), (0,)), ((), ())), preferred_element_type=jnp.float32
    )


def contract_cols(left, right):
    return lax.dot_general(
        left, right, (((1,), (1,)), ((), ())), preferred_element_type=jnp.float32
    )


def next_near(step):
    near = lax.axis_size(FS_0[1])
    return (lax.axis_index(FS_0[1]) + near + step) % near


def gathered(block):
    block = sent_to_all(block, WIDE)
    block = block.reshape(FAR, -1, block.shape[2])
    below, above = shifted(block, FS_0, 1), shifted(block, FS_0, -1)
    shape = (FAR, lax.axis_size(FS_0[1]), *block.shape[1:])
    whole = jnp.zeros(shape, block.dtype)
    for part, step in ((block, 0), (below, -1), (above, 1)):
        whole = lax.dynamic_update_slice(whole, part[:, None], (0, next_near(step), 0, 0))
    return whole.reshape(-1, block.shape[2])


def scattered(terms, rows):
    terms = terms.reshape(FAR, lax.axis_size(FS_0[1]), -1, terms.shape[1])
    mine, over, under = (
        lax.dynamic_index_in_dim(terms, next_near(step), 1, keepdims=False)
        for step in (0, 1, -1)
    )
    total = mine.astype(jnp.float32)
    total = total + shifted(over, FS_0, 1).astype(jnp.float32)
    total = total + shifted(under, FS_0, -1).astype(jnp.float32)
    total = total.astype(jnp.bfloat16).reshape(-1, rows, terms.shape[3])
    return exchanged(total, WIDE)


def paired(array, turn):
    chips = lax.axis_size("chip")
    pairs = []
    for chip in range(chips):
        for core in range(2):
            other = (chip + (1 if (chip + core + turn) % 2 == 0 else -1)) % chips
            pairs.append((2 * chip + core, 2 * other + core))
    return lax.ppermute(array, ("chip", "core"), pairs)


def added(left, right):
    return (left.astype(jnp.float32) + right.astype(jnp.float32)).astype(jnp.bfloat16)


def summed_over_tp(partial):
    half = partial.shape[0] // 2
    core = lax.axis_index("core")
    kept = lax.dynamic_slice_in_dim(partial, core * half, half)
    given = lax.dynamic_slice_in_dim(partial, (1 - core) * half, half)
    total = added(kept, shifted(given, "core", 1))
    total = added(total, paired(total, 0))
    other = paired(total, 1)
    total = added(total, other)
    other = shifted(total, "core", 1)
    first = jnp.where(core == 0, total, other)
    second = jnp.where(core == 0, other, total)
    return jnp.concatenate([first, second])


def gradients(tokens, cotangent, gate_weight, up_weight, down_weight):
    rows, units = gate_weight.shape
    gate_up = gathered(jnp.concatenate([gate_weight, up_weight], axis=1))
    down = gathered(down_weight.T)

    both = jnp.dot(tokens, gate_up, preferred_element_type=jnp.float32)
    gate_pre, up_pre = both[:, :units], both[:, units:]
    sigmoid_gate = jax.nn.sigmoid(gate_pre)
    activated = gate_pre * sigmoid_gate
    hidden = (activated * up_pre).astype(jnp.bfloat16)

    terms = contract_rows(cotangent, hidden).astype(jnp.bfloat16)
    down_grad = scattered(terms, rows).T

    hidden_grad = jnp.dot(cotangent, down, preferred_element_type=jnp.float32)
    gate_pre_grad = (
        hidden_grad * up_pre * sigmoid_gate * (1.0 + gate_pre * (1.0 - sigmoid_gate))
    ).astype(jnp.bfloat16)
    up_pre_grad = (hidden_grad * activated).astype(jnp.bfloat16)
    partial = contract_cols(gate_up, jnp.concatenate([gate_pre_grad, up_pre_grad], axis=1))
    total = summed_over_tp(partial.astype(jnp.bfloat16))
    return (total.T, down_grad)


def solution(mesh):
    torus = Mesh(
        mesh.devices.reshape(FAR, 12 // FAR, 8, mesh.shape["tp"] // 2, 2), (*FS, "chip", "core")
    )
    tp = ("chip", "core")
    in_specs = (P(FS, None), P(FS, None), P(FS, tp), P(FS, tp), P(tp, FS))
    out_specs = (P(FS, None), P(tp, FS))
    return jax.shard_map(
        gradients, mesh=torus, in_specs=in_specs, out_specs=out_specs, check_vma=False
    )
```

time: 169 us -> 163 us (0.964)
  the two profiles are of different devices: /device:TPU:14 before, /device:TPU:142 now
where the time goes in v4:
time: 163 us
  waiting for transfers between devices  79.8 us (49%)
  starting transfers between devices  64.1 us (39%)
  local copies, waits for them, and re-layouts  11.2 us (7%)
  other arithmetic  3.73 us (2%)
  matrix products  2.69 us (2%)
    all_to_all x2, waiting for transfers between devices, sent_to_all(): lax.all_to_all(jnp.broadcast_to(array[None], (peers, *array.shape)), axis...  44.4 us
    ppermute x8, starting transfers between devices, shifted(): lax.ppermute(array, axis, [(k, (k + step) % peers) for k in range(peers)])  25.4 us
    all_to_all x2, starting transfers between devices, sent_to_all(): lax.all_to_all(jnp.broadcast_to(array[None], (peers, *array.shape)), axis...  21.9 us
    ppermute x8, waiting for transfers between devices, shifted(): lax.ppermute(array, axis, [(k, (k + step) % peers) for k in range(peers)])  18.3 us
    all_to_all x1, starting transfers between devices, exchanged(): got = lax.all_to_all(parts, axis, 0, 0, tiled=True)  11.7 us
    all_to_all x1, waiting for transfers between devices, exchanged(): got = lax.all_to_all(parts, axis, 0, 0, tiled=True)  9.14 us
    ppermute x2, waiting for transfers between devices, paired(): return lax.ppermute(array, ('chip', 'core'), pairs)  7.96 us
    ppermute x2, starting transfers between devices, paired(): return lax.ppermute(array, ('chip', 'core'), pairs)  5.13 us
  transfers between devices with their start and end apart: 13, of which 8 were waited for; matrix products, arithmetic and copies ran while one was open for 7% of the time, Pallas kernels for 0%

profile of v4, /device:TPU:142, one launch (start us, length us, event | category | flops | bytes accessed | tf_op | source)
XLA Modules:
  0.0 162.6 jit_solution(12019218317959426902)
XLA Ops:
  0.6 0.0 copy-start
  0.6 1.6 broadcast_in_dim.35
  2.2 18.0 %all-to-all-start.1 = ((bf16[32,14,384]{2,1,0:T(8,128)(2,1)}), bf16[32,14,384]{2,1,0:T(8,128)(2,1)S(1)}, u32[]{:S(2)}, u32[]{:S(2)}) async-start(bf16[32,14,384]{2,1,0:T(8,128)(2,1)} %broadcast_in_dim.35), calls=%async_computation.1 | async-start | bytes 786432 | tf_op jit(solution)/shard_map/all_to_all | solution.py:21
  20.2 0.7 pad_maximum_fusion
  20.9 22.7 %all-to-all-done.1 = bf16[32,14,384]{2,1,0:T(8,128)(2,1)S(1)} async-done(((bf16[32,14,384]{2,1,0:T(8,128)(2,1)}), bf16[32,14,384]{2,1,0:T(8,128)(2,1)S(1)}, u32[]{:S(2)}, u32[]{:S(2)}) %all-to-all-start.1) | async-done | bytes 344096 | tf_op jit(solution)/shard_map/all_to_all | solution.py:21
  43.6 0.9 broadcast_in_dim.31
  44.6 3.9 %all-to-all-start = ((bf16[32,14,768]{2,1,0:T(8,128)(2,1)}), bf16[32,14,768]{2,1,0:T(8,128)(2,1)S(1)}, u32[]{:S(2)}, u32[]{:S(2)}) async-start(bf16[32,14,768]{2,1,0:T(8,128)(2,1)} %broadcast_in_dim.31), calls=%async_computation | async-start | bytes 1572864 | tf_op jit(solution)/shard_map/all_to_all | solution.py:21
  48.5 0.8 reshape.28
  49.3 4.6 %collective-permute-start.2 = (bf16[4,112,384]{2,1,0:T(8,128)(2,1)}, bf16[4,112,384]{2,1,0:T(8,128)(2,1)}, u32[]{:S(2)}, u32[]{:S(2)}) collective-permute-start(bf16[4,112,384]{2,1,0:T(8,128)(2,1)} %reshape.28), channel_id=1, source_target_pairs={{0,64},{64,128},{128,192},{192,256},{256,320},{320,384},{384,448},... | collective-permute-start | bytes 1032200 | tf_op jit(solution)/shard_map/ppermute | solution.py:16
  54.0 1.9 %collective-permute-start.3 = (bf16[4,112,384]{2,1,0:T(8,128)(2,1)}, bf16[4,112,384]{2,1,0:T(8,128)(2,1)}, u32[]{:S(2)}, u32[]{:S(2)}) collective-permute-start(bf16[4,112,384]{2,1,0:T(8,128)(2,1)} %reshape.28), channel_id=1, source_target_pairs={{0,704},{64,0},{128,64},{192,128},{256,192},{320,256},{384,320},{4... | collective-permute-start | bytes 1032200 | tf_op jit(solution)/shard_map/ppermute | solution.py:16
  56.0 0.1 broadcast_in_dim_reshape.7
  56.1 0.1 broadcast_in_dim.34
  56.2 0.1 bitcast_dynamic-update-slice_fusion.5
  56.2 21.7 %all-to-all-done = bf16[32,14,768]{2,1,0:T(8,128)(2,1)S(1)} async-done(((bf16[32,14,768]{2,1,0:T(8,128)(2,1)}), bf16[32,14,768]{2,1,0:T(8,128)(2,1)S(1)}, u32[]{:S(2)}, u32[]{:S(2)}) %all-to-all-start) | async-done | bytes 688160 | tf_op jit(solution)/shard_map/all_to_all | solution.py:21
  78.0 1.0 reshape.26
  79.0 6.3 %collective-permute-start = (bf16[4,112,768]{2,1,0:T(8,128)(2,1)}, bf16[4,112,768]{2,1,0:T(8,128)(2,1)}, u32[]{:S(2)}, u32[]{:S(2)}) collective-permute-start(bf16[4,112,768]{2,1,0:T(8,128)(2,1)} %reshape.26), channel_id=1, source_target_pairs={{0,64},{64,128},{128,192},{192,256},{256,320},{320,384},{384,448},... | collective-permute-start | bytes 2064392 | tf_op jit(solution)/shard_map/ppermute | solution.py:16
  85.3 0.0 collective-permute-done.2
  85.3 1.0 bitcast_dynamic-update-slice_fusion.4
  86.4 1.9 %collective-permute-start.1 = (bf16[4,112,768]{2,1,0:T(8,128)(2,1)}, bf16[4,112,768]{2,1,0:T(8,128)(2,1)}, u32[]{:S(2)}, u32[]{:S(2)}) collective-permute-start(bf16[4,112,768]{2,1,0:T(8,128)(2,1)} %reshape.26), channel_id=1, source_target_pairs={{0,704},{64,0},{128,64},{192,128},{256,192},{320,256},{384,320},{4... | collective-permute-start | bytes 2064392 | tf_op jit(solution)/shard_map/ppermute | solution.py:16
  88.3 0.0 collective-permute-done.3
  88.3 1.0 bitcast_dynamic-update-slice_fusion.3
  89.3 0.2 broadcast_in_dim_reshape.6
  89.6 0.1 broadcast_in_dim.30
  89.7 0.0 copy-start.1
  89.7 0.1 bitcast_dynamic-update-slice_fusion.2
  89.8 10.1 %collective-permute-done = bf16[4,112,768]{2,1,0:T(8,128)(2,1)} collective-permute-done((bf16[4,112,768]{2,1,0:T(8,128)(2,1)}, bf16[4,112,768]{2,1,0:T(8,128)(2,1)}, u32[]{:S(2)}, u32[]{:S(2)}) %collective-permute-start) | collective-permute-done | bytes 688160 | tf_op jit(solution)/shard_map/ppermute | solution.py:16
  99.9 1.1 bitcast_dynamic-update-slice_fusion.1
  101.0 2.0 %collective-permute-done.1 = bf16[4,112,768]{2,1,0:T(8,128)(2,1)} collective-permute-done((bf16[4,112,768]{2,1,0:T(8,128)(2,1)}, bf16[4,112,768]{2,1,0:T(8,128)(2,1)}, u32[]{:S(2)}, u32[]{:S(2)}) %collective-permute-start.1) | collective-permute-done | bytes 688160 | tf_op jit(solution)/shard_map/ppermute | solution.py:16
  103.0 1.1 bitcast_dynamic-update-slice_fusion
  104.1 0.0 copy-done.1
  104.1 0.8 convolution_bitcast_fusion
  105.0 0.0 copy-done
  105.0 0.5 multiply_convert_fusion.2
  105.5 0.7 convolution_convert_fusion.1
  106.3 1.9 %collective-permute-start.4 = (bf16[672,256]{1,0:T(8,128)(2,1)S(1)}, bf16[672,256]{1,0:T(8,128)(2,1)S(1)}, u32[]{:S(2)}, u32[]{:S(2)}) collective-permute-start(bf16[672,256]{1,0:T(8,128)(2,1)S(1)} %constant_dynamic-slice_fusion), channel_id=1, source_target_pairs={{0,1},{1,0},{2,3},{3,2},{4,5},{5,4},{6,7},{7,6},{8,9},{9,8},{10,11... | collective-permute-start | bytes 1032200 | tf_op jit(solution)/shard_map/ppermute | solution.py:16
  108.2 0.6 convolution_convert_fusion
  108.8 0.9 dynamic-slice_bitcast_fusion.1
  109.8 3.5 %collective-permute-start.9 = (bf16[4,112,384]{2,1,0:T(8,128)(2,1)}, bf16[4,112,384]{2,1,0:T(8,128)(2,1)S(1)}, u32[]{:S(2)}, u32[]{:S(2)}) collective-permute-start(bf16[4,112,384]{2,1,0:T(8,128)(2,1)} %get-tuple-element.5), channel_id=1, source_target_pairs={{0,704},{64,0},{128,64},{192,128},{256,192},{320,256},{384,320},{4... | collective-permute-start | bytes 1032200 | tf_op jit(solution)/shard_map/ppermute | solution.py:16
  113.3 3.2 %collective-permute-start.8 = (bf16[4,112,384]{2,1,0:T(8,128)(2,1)}, bf16[4,112,384]{2,1,0:T(8,128)(2,1)}, u32[]{:S(2)}, u32[]{:S(2)}) collective-permute-start(bf16[4,112,384]{2,1,0:T(8,128)(2,1)} %get-tuple-element.4), channel_id=1, source_target_pairs={{0,64},{64,128},{128,192},{192,256},{256,320},{320,384},{384,448},... | collective-permute-start | bytes 1032200 | tf_op jit(solution)/shard_map/ppermute | solution.py:16
  116.5 0.0 collective-permute-done.4
  116.5 0.1 add_convert_fusion.2
  116.6 2.7 %collective-permute-start.5 = (bf16[672,256]{1,0:T(8,128)(2,1)S(1)}, bf16[672,256]{1,0:T(8,128)(2,1)S(1)}, u32[]{:S(2)}, u32[]{:S(2)}) collective-permute-start(bf16[672,256]{1,0:T(8,128)(2,1)S(1)} %add_convert_fusion.2), channel_id=1, source_target_pairs={{0,2},{1,7},{2,0},{3,5},{4,6},{5,3},{6,4},{7,1},{8,10},{9,15},{10,... | collective-permute-start | bytes 1032200 | tf_op jit(solution)/shard_map/ppermute | solution.py:79
  119.4 4.1 %collective-permute-done.9 = bf16[4,112,384]{2,1,0:T(8,128)(2,1)S(1)} collective-permute-done((bf16[4,112,384]{2,1,0:T(8,128)(2,1)}, bf16[4,112,384]{2,1,0:T(8,128)(2,1)S(1)}, u32[]{:S(2)}, u32[]{:S(2)}) %collective-permute-start.9) | collective-permute-done | bytes 344096 | tf_op jit(solution)/shard_map/ppermute | solution.py:16
  123.5 2.2 %collective-permute-done.8 = bf16[4,112,384]{2,1,0:T(8,128)(2,1)} collective-permute-done((bf16[4,112,384]{2,1,0:T(8,128)(2,1)}, bf16[4,112,384]{2,1,0:T(8,128)(2,1)}, u32[]{:S(2)}, u32[]{:S(2)}) %collective-permute-start.8) | collective-permute-done | bytes 344096 | tf_op jit(solution)/shard_map/ppermute | solution.py:16
  125.7 1.1 fusion.1
  126.8 0.8 reshape.31
  127.6 11.7 %all-to-all-start.2 = ((bf16[32,14,384]{2,1,0:T(8,128)(2,1)}), bf16[32,14,384]{2,1,0:T(8,128)(2,1)S(1)}, u32[]{:S(2)}, u32[]{:S(2)}) async-start(bf16[32,14,384]{2,1,0:T(8,128)(2,1)} %reshape.31), calls=%async_computation.2 | async-start | bytes 786432 | tf_op jit(solution)/shard_map/all_to_all | solution.py:27
  139.3 0.0 collective-permute-done.5
  139.3 0.1 add_convert_fusion.1
  139.4 2.4 %collective-permute-start.6 = (bf16[672,256]{1,0:T(8,128)(2,1)S(1)}, bf16[672,256]{1,0:T(8,128)(2,1)S(1)}, u32[]{:S(2)}, u32[]{:S(2)}) collective-permute-start(bf16[672,256]{1,0:T(8,128)(2,1)S(1)} %add_convert_fusion.1), channel_id=1, source_target_pairs={{0,6},{1,3},{2,4},{3,1},{4,2},{5,7},{6,0},{7,5},{8,14},{9,11},{10,... | collective-permute-start | bytes 1032200 | tf_op jit(solution)/shard_map/ppermute | solution.py:79
  141.8 8.0 %collective-permute-done.6 = bf16[672,256]{1,0:T(8,128)(2,1)S(1)} collective-permute-done((bf16[672,256]{1,0:T(8,128)(2,1)S(1)}, bf16[672,256]{1,0:T(8,128)(2,1)S(1)}, u32[]{:S(2)}, u32[]{:S(2)}) %collective-permute-start.6) | collective-permute-done | bytes 344096 | tf_op jit(solution)/shard_map/ppermute | solution.py:79
  149.8 0.1 add_convert_fusion
  149.9 1.9 %collective-permute-start.7 = (bf16[672,256]{1,0:T(8,128)(2,1)S(1)}, bf16[672,256]{1,0:T(8,128)(2,1)S(1)}, u32[]{:S(2)}, u32[]{:S(2)}) collective-permute-start(bf16[672,256]{1,0:T(8,128)(2,1)S(1)} %add_convert_fusion), channel_id=1, source_target_pairs={{0,1},{1,0},{2,3},{3,2},{4,5},{5,4},{6,7},{7,6},{8,9},{9,8},{10,11... | collective-permute-start | bytes 1032200 | tf_op jit(solution)/shard_map/ppermute | solution.py:16
  151.8 9.1 %all-to-all-done.2 = bf16[32,14,384]{2,1,0:T(8,128)(2,1)S(1)} async-done(((bf16[32,14,384]{2,1,0:T(8,128)(2,1)}), bf16[32,14,384]{2,1,0:T(8,128)(2,1)S(1)}, u32[]{:S(2)}, u32[]{:S(2)}) %all-to-all-start.2) | async-done | bytes 344096 | tf_op jit(solution)/shard_map/all_to_all | solution.py:27
  160.9 0.7 convert_reduce_fusion
  161.6 0.0 collective-permute-done.7
  161.7 0.9 maximum_bitcast_fusion
  (2 shorter events, 0.1 us)
Async XLA Ops:
  0.6 104.3 %copy-start = (bf16[256,1344]{0,1:T(8,128)(2,1)S(1)}, bf16[256,1344]{0,1:T(8,128)(2,1)}, u32[]{:S(2)}) copy-start(bf16[256,1344]{0,1:T(8,128)(2,1)} %param.6) | copy-start | bytes 2064388
  2.2 41.4 %all-to-all-start.1 = ((bf16[32,14,384]{2,1,0:T(8,128)(2,1)}), bf16[32,14,384]{2,1,0:T(8,128)(2,1)S(1)}, u32[]{:S(2)}, u32[]{:S(2)}) async-start(bf16[32,14,384]{2,1,0:T(8,128)(2,1)} %broadcast_in_dim.35), calls=%async_computation.1 | async-start | bytes 786432 | tf_op jit(solution)/shard_map/all_to_all | solution.py:21
  44.6 33.4 %all-to-all-start = ((bf16[32,14,768]{2,1,0:T(8,128)(2,1)}), bf16[32,14,768]{2,1,0:T(8,128)(2,1)S(1)}, u32[]{:S(2)}, u32[]{:S(2)}) async-start(bf16[32,14,768]{2,1,0:T(8,128)(2,1)} %broadcast_in_dim.31), calls=%async_computation | async-start | bytes 1572864 | tf_op jit(solution)/shard_map/all_to_all | solution.py:21
  49.3 36.0 %collective-permute-start.2 = (bf16[4,112,384]{2,1,0:T(8,128)(2,1)}, bf16[4,112,384]{2,1,0:T(8,128)(2,1)}, u32[]{:S(2)}, u32[]{:S(2)}) collective-permute-start(bf16[4,112,384]{2,1,0:T(8,128)(2,1)} %reshape.28), channel_id=1, source_target_pairs={{0,64},{64,128},{128,192},{192,256},{256,320},{320,384},{384,448},... | collective-permute-start | bytes 1032200 | tf_op jit(solution)/shard_map/ppermute | solution.py:16
  54.0 34.3 %collective-permute-start.3 = (bf16[4,112,384]{2,1,0:T(8,128)(2,1)}, bf16[4,112,384]{2,1,0:T(8,128)(2,1)}, u32[]{:S(2)}, u32[]{:S(2)}) collective-permute-start(bf16[4,112,384]{2,1,0:T(8,128)(2,1)} %reshape.28), channel_id=1, source_target_pairs={{0,704},{64,0},{128,64},{192,128},{256,192},{320,256},{384,320},{4... | collective-permute-start | bytes 1032200 | tf_op jit(solution)/shard_map/ppermute | solution.py:16
  79.0 20.9 %collective-permute-start = (bf16[4,112,768]{2,1,0:T(8,128)(2,1)}, bf16[4,112,768]{2,1,0:T(8,128)(2,1)}, u32[]{:S(2)}, u32[]{:S(2)}) collective-permute-start(bf16[4,112,768]{2,1,0:T(8,128)(2,1)} %reshape.26), channel_id=1, source_target_pairs={{0,64},{64,128},{128,192},{192,256},{256,320},{320,384},{384,448},... | collective-permute-start | bytes 2064392 | tf_op jit(solution)/shard_map/ppermute | solution.py:16
  86.4 16.6 %collective-permute-start.1 = (bf16[4,112,768]{2,1,0:T(8,128)(2,1)}, bf16[4,112,768]{2,1,0:T(8,128)(2,1)}, u32[]{:S(2)}, u32[]{:S(2)}) collective-permute-start(bf16[4,112,768]{2,1,0:T(8,128)(2,1)} %reshape.26), channel_id=1, source_target_pairs={{0,704},{64,0},{128,64},{192,128},{256,192},{320,256},{384,320},{4... | collective-permute-start | bytes 2064392 | tf_op jit(solution)/shard_map/ppermute | solution.py:16
  89.7 14.4 %copy-start.1 = (bf16[256,1344]{0,1:T(8,128)(2,1)S(1)}, bf16[256,1344]{0,1:T(8,128)(2,1)}, u32[]{:S(2)}) copy-start(bf16[256,1344]{0,1:T(8,128)(2,1)} %param.5) | copy-start | bytes 2064388
  106.3 10.3 %collective-permute-start.4 = (bf16[672,256]{1,0:T(8,128)(2,1)S(1)}, bf16[672,256]{1,0:T(8,128)(2,1)S(1)}, u32[]{:S(2)}, u32[]{:S(2)}) collective-permute-start(bf16[672,256]{1,0:T(8,128)(2,1)S(1)} %constant_dynamic-slice_fusion), channel_id=1, source_target_pairs={{0,1},{1,0},{2,3},{3,2},{4,5},{5,4},{6,7},{7,6},{8,9},{9,8},{10,11... | collective-permute-start | bytes 1032200 | tf_op jit(solution)/shard_map/ppermute | solution.py:16
  109.8 13.8 %collective-permute-start.9 = (bf16[4,112,384]{2,1,0:T(8,128)(2,1)}, bf16[4,112,384]{2,1,0:T(8,128)(2,1)S(1)}, u32[]{:S(2)}, u32[]{:S(2)}) collective-permute-start(bf16[4,112,384]{2,1,0:T(8,128)(2,1)} %get-tuple-element.5), channel_id=1, source_target_pairs={{0,704},{64,0},{128,64},{192,128},{256,192},{320,256},{384,320},{4... | collective-permute-start | bytes 1032200 | tf_op jit(solution)/shard_map/ppermute | solution.py:16
  113.3 12.4 %collective-permute-start.8 = (bf16[4,112,384]{2,1,0:T(8,128)(2,1)}, bf16[4,112,384]{2,1,0:T(8,128)(2,1)}, u32[]{:S(2)}, u32[]{:S(2)}) collective-permute-start(bf16[4,112,384]{2,1,0:T(8,128)(2,1)} %get-tuple-element.4), channel_id=1, source_target_pairs={{0,64},{64,128},{128,192},{192,256},{256,320},{320,384},{384,448},... | collective-permute-start | bytes 1032200 | tf_op jit(solution)/shard_map/ppermute | solution.py:16
  116.6 22.7 %collective-permute-start.5 = (bf16[672,256]{1,0:T(8,128)(2,1)S(1)}, bf16[672,256]{1,0:T(8,128)(2,1)S(1)}, u32[]{:S(2)}, u32[]{:S(2)}) collective-permute-start(bf16[672,256]{1,0:T(8,128)(2,1)S(1)} %add_convert_fusion.2), channel_id=1, source_target_pairs={{0,2},{1,7},{2,0},{3,5},{4,6},{5,3},{6,4},{7,1},{8,10},{9,15},{10,... | collective-permute-start | bytes 1032200 | tf_op jit(solution)/shard_map/ppermute | solution.py:79
  127.6 33.3 %all-to-all-start.2 = ((bf16[32,14,384]{2,1,0:T(8,128)(2,1)}), bf16[32,14,384]{2,1,0:T(8,128)(2,1)S(1)}, u32[]{:S(2)}, u32[]{:S(2)}) async-start(bf16[32,14,384]{2,1,0:T(8,128)(2,1)} %reshape.31), calls=%async_computation.2 | async-start | bytes 786432 | tf_op jit(solution)/shard_map/all_to_all | solution.py:27
  139.4 10.4 %collective-permute-start.6 = (bf16[672,256]{1,0:T(8,128)(2,1)S(1)}, bf16[672,256]{1,0:T(8,128)(2,1)S(1)}, u32[]{:S(2)}, u32[]{:S(2)}) collective-permute-start(bf16[672,256]{1,0:T(8,128)(2,1)S(1)} %add_convert_fusion.1), channel_id=1, source_target_pairs={{0,6},{1,3},{2,4},{3,1},{4,2},{5,7},{6,0},{7,5},{8,14},{9,11},{10,... | collective-permute-start | bytes 1032200 | tf_op jit(solution)/shard_map/ppermute | solution.py:79
  149.9 11.8 %collective-permute-start.7 = (bf16[672,256]{1,0:T(8,128)(2,1)S(1)}, bf16[672,256]{1,0:T(8,128)(2,1)S(1)}, u32[]{:S(2)}, u32[]{:S(2)}) collective-permute-start(bf16[672,256]{1,0:T(8,128)(2,1)S(1)} %add_convert_fusion), channel_id=1, source_target_pairs={{0,1},{1,0},{2,3},{3,2},{4,5},{5,4},{6,7},{7,6},{8,9},{9,8},{10,11... | collective-permute-start | bytes 1032200 | tf_op jit(solution)/shard_map/ppermute | solution.py:16

commit v5 on v4

--- a/solution.py
+++ b/solution.py
@@ -1,5 +1,6 @@
 import jax
 import jax.numpy as jnp
+import numpy as np
 from jax import lax
 from jax.sharding import Mesh
 from jax.sharding import PartitionSpec as P
@@ -8,7 +9,6 @@
 FAR = 4
 FS_0 = ("fs_0h", "fs_0l")
 FS = (*FS_0, "fs_1")
-WIDE = ("fs_0h", "fs_1")
 
 
 def shifted(array, axis, step):
@@ -40,33 +40,31 @@
     )
 
 
-def next_near(step):
-    near = lax.axis_size(FS_0[1])
-    return (lax.axis_index(FS_0[1]) + near + step) % near
+def picked(source):
+    source = jnp.asarray(source, jnp.int32)
+    spot = lax.broadcasted_iota(jnp.int32, (source.size, source.size), 1)
+    return (source[:, None] == spot).astype(jnp.bfloat16)
 
 
-def gathered(block):
-    block = sent_to_all(block, WIDE)
-    block = block.reshape(FAR, -1, block.shape[2])
-    below, above = shifted(block, FS_0, 1), shifted(block, FS_0, -1)
-    shape = (FAR, lax.axis_size(FS_0[1]), *block.shape[1:])
-    whole = jnp.zeros(shape, block.dtype)
-    for part, step in ((block, 0), (below, -1), (above, 1)):
-        whole = lax.dynamic_update_slice(whole, part[:, None], (0, next_near(step), 0, 0))
-    return whole.reshape(-1, block.shape[2])
+def around(block, axis):
+    peers = lax.axis_size(axis)
+    rows = block.shape[0]
+    half = rows // 2
+    place = lax.axis_index(axis)
 
+    def put(whole, part, owner, start):
+        owner = (owner + peers) % peers
+        return lax.dynamic_update_slice(whole, part[None], (owner, start, 0))
 
-def scattered(terms, rows):
-    terms = terms.reshape(FAR, lax.axis_size(FS_0[1]), -1, terms.shape[1])
-    mine, over, under = (
-        lax.dynamic_index_in_dim(terms, next_near(step), 1, keepdims=False)
-        for step in (0, 1, -1)
-    )
-    total = mine.astype(jnp.float32)
-    total = total + shifted(over, FS_0, 1).astype(jnp.float32)
-    total = total + shifted(under, FS_0, -1).astype(jnp.float32)
-    total = total.astype(jnp.bfloat16).reshape(-1, rows, terms.shape[3])
-    return exchanged(total, WIDE)
+    whole = put(jnp.zeros((peers, *block.shape), block.dtype), block, place, 0)
+    up = down = block
+    for step in range(1, peers // 2):
+        up, down = shifted(up, axis, 1), shifted(down, axis, -1)
+        whole = put(whole, up, place - step, 0)
+        whole = put(whole, down, place + step, 0)
+    whole = put(whole, shifted(up[:half], axis, 1), place + peers // 2, 0)
+    whole = put(whole, shifted(down[half:], axis, -1), place + peers // 2, half)
+    return whole.reshape(peers * rows, -1)
 
 
 def paired(array, turn):
@@ -99,9 +97,19 @@
 
 
 def gradients(tokens, cotangent, gate_weight, up_weight, down_weight):
+    near, inner = lax.axis_size("fs_0l"), lax.axis_size("fs_1")
     rows, units = gate_weight.shape
-    gate_up = gathered(jnp.concatenate([gate_weight, up_weight], axis=1))
-    down = gathered(down_weight.T)
+    width = tokens.shape[1]
+
+    gate_up = jnp.concatenate([gate_weight, up_weight], axis=1)
+    gate_up = sent_to_all(gate_up, "fs_1").reshape(inner * rows, 2 * units)
+    gate_up = around(gate_up, FS_0)
+    down = sent_to_all(down_weight.T, FS_0[::-1]).reshape(-1, units)
+    down = sent_to_all(down, "fs_1").reshape(width, units)
+
+    spot = np.arange(width).reshape(FAR, near, inner, rows).transpose(2, 1, 0, 3).reshape(-1)
+    turned_cotangent = contract_cols(picked(spot), cotangent).astype(jnp.bfloat16)
+    turned_cotangent = lax.optimization_barrier(turned_cotangent)
 
     both = jnp.dot(tokens, gate_up, preferred_element_type=jnp.float32)
     gate_pre, up_pre = both[:, :units], both[:, units:]
@@ -109,10 +117,13 @@
     activated = gate_pre * sigmoid_gate
     hidden = (activated * up_pre).astype(jnp.bfloat16)
 
-    terms = contract_rows(cotangent, hidden).astype(jnp.bfloat16)
-    down_grad = scattered(terms, rows).T
+    terms = jnp.dot(turned_cotangent, hidden, preferred_element_type=jnp.float32)
+    terms = terms.astype(jnp.bfloat16).reshape(inner * near, FAR * rows, units)
+    terms = exchanged(terms, ("fs_1", "fs_0l"))
+    terms = terms.astype(jnp.bfloat16).reshape(FAR, rows, units)
+    down_grad = exchanged(terms, "fs_0h").T
 
-    hidden_grad = jnp.dot(cotangent, down, preferred_element_type=jnp.float32)
+    hidden_grad = contract_rows(turned_cotangent, down)
     gate_pre_grad = (
         hidden_grad * up_pre * sigmoid_gate * (1.0 + gate_pre * (1.0 - sigmoid_gate))
     ).astype(jnp.bfloat16)

time: 163 us -> 162 us (level)
  the two profiles are of different devices: /device:TPU:142 before, /device:TPU:8 now
where the time goes in v5:
time: 162 us; the launch traced here: 161 us
  starting transfers between devices  88.2 us (54%)
  waiting for transfers between devices  33.8 us (21%)
  blocking collectives  20.2 us (12%)
  matrix products  8.2 us (5%)
  local copies, waits for them, and re-layouts  6.63 us (4%)
  other arithmetic  2.76 us (2%)
    ppermute x14, starting transfers between devices, shifted(): lax.ppermute(array, axis, [(k, (k + step) % peers) for k in range(peers)])  47.3 us
    all_to_all x1, blocking collectives, sent_to_all(): lax.all_to_all(jnp.broadcast_to(array[None], (peers, *array.shape)), axis...  20.2 us
    all_to_all x2, starting transfers between devices, sent_to_all(): lax.all_to_all(jnp.broadcast_to(array[None], (peers, *array.shape)), axis...  17 us
    all_to_all x2, starting transfers between devices, exchanged(): got = lax.all_to_all(parts, axis, 0, 0, tiled=True)  15.8 us
    ppermute x14, waiting for transfers between devices, shifted(): lax.ppermute(array, axis, [(k, (k + step) % peers) for k in range(peers)])  11.5 us
    ppermute x2, waiting for transfers between devices, paired(): return lax.ppermute(array, ('chip', 'core'), pairs)  11.4 us
    all_to_all x2, waiting for transfers between devices, exchanged(): got = lax.all_to_all(parts, axis, 0, 0, tiled=True)  9.64 us
    ppermute x2, starting transfers between devices, paired(): return lax.ppermute(array, ('chip', 'core'), pairs)  8.06 us
  transfers between devices with their start and end apart: 20, of which 13 were waited for; matrix products, arithmetic and copies ran while one was open for 8% of the time, Pallas kernels for 0%

profile of v5, /device:TPU:8, one launch (start us, length us, event | category | flops | bytes accessed | tf_op | source)
XLA Modules:
  0.0 160.8 jit_solution(2478205695918798126)
XLA Ops:
  0.6 0.0 copy-start
  0.6 0.8 pad_maximum_fusion
  1.5 20.2 %all_to_all.25 = bf16[8,14,768]{2,1,0:T(8,128)(2,1)S(1)} all-to-all(bf16[8,14,768]{2,1,0:T(8,128)(2,1)S(1)} %broadcast_in_dim.60), channel_id=1, replica_groups=mesh['fs_0h'=4,'fs_0l'=3,'fs_1'=8,'chip'=4,'core'=2] {'fs_1'}, dimensions={0} | all-to-all | bytes 344064 | tf_op jit(solution)/shard_map/all_to_all | solution.py:21
  21.6 1.4 broadcast_in_dim.73
  23.0 11.4 %all-to-all-start.1 = ((bf16[12,14,384]{2,1,0:T(8,128)(2,1)}), bf16[12,14,384]{2,1,0:T(8,128)(2,1)S(1)}, u32[]{:S(2)}, u32[]{:S(2)}) async-start(bf16[12,14,384]{2,1,0:T(8,128)(2,1)} %broadcast_in_dim.73), calls=%async_computation.1 | async-start | bytes 294912 | tf_op jit(solution)/shard_map/all_to_all | solution.py:21
  34.4 0.7 reshape.23
  35.1 3.9 %collective-permute-start = (bf16[112,768]{1,0:T(8,128)(2,1)}, bf16[112,768]{1,0:T(8,128)(2,1)}, u32[]{:S(2)}, u32[]{:S(2)}) collective-permute-start(bf16[112,768]{1,0:T(8,128)(2,1)} %reshape.23), channel_id=1, source_target_pairs={{0,64},{64,128},{128,192},{192,256},{256,320},{320,384},{384,448},... | collective-permute-start | bytes 516104 | tf_op jit(solution)/shard_map/ppermute | solution.py:16
  39.0 3.2 %collective-permute-start.1 = (bf16[112,768]{1,0:T(8,128)(2,1)}, bf16[112,768]{1,0:T(8,128)(2,1)S(1)}, u32[]{:S(2)}, u32[]{:S(2)}) collective-permute-start(bf16[112,768]{1,0:T(8,128)(2,1)} %reshape.23), channel_id=1, source_target_pairs={{0,704},{64,0},{128,64},{192,128},{256,192},{320,256},{384,320},{4... | collective-permute-start | bytes 516104 | tf_op jit(solution)/shard_map/ppermute | solution.py:16
  42.2 3.0 %fusion.2 = bf16[1344,256]{1,0:T(8,128)(2,1)} fusion(bf16[256,1344]{0,1:T(8,128)(2,1)S(1)} %copy-done, s32[1344]{0:T(1024)} %constant.98.clone), kind=kOutput, calls=%fused_computation.5 | convolution fusion | flops 926994432 | bytes 1381632 | tf_op jit(solution)/shard_map/dot_general | solution.py:38
  45.2 0.1 broadcast_in_dim_reshape.4
  45.3 0.1 broadcast_in_dim.59
  45.4 1.2 all-to-all-done.1
  46.7 1.1 broadcast_in_dim.75
  47.8 5.7 %all-to-all-start.2 = ((bf16[8,168,384]{2,1,0:T(8,128)(2,1)}), bf16[8,168,384]{2,1,0:T(8,128)(2,1)}, u32[]{:S(2)}, u32[]{:S(2)}) async-start(bf16[8,168,384]{2,1,0:T(8,128)(2,1)} %broadcast_in_dim.75), calls=%async_computation.2 | async-start | bytes 2064384 | tf_op jit(solution)/shard_map/all_to_all | solution.py:21
  53.5 0.0 collective-permute-done
  53.5 2.1 %collective-permute-start.2 = (bf16[112,768]{1,0:T(8,128)(2,1)}, bf16[112,768]{1,0:T(8,128)(2,1)S(1)}, u32[]{:S(2)}, u32[]{:S(2)}) collective-permute-start(bf16[112,768]{1,0:T(8,128)(2,1)} %collective-permute-done), channel_id=1, source_target_pairs={{0,64},{64,128},{128,192},{192,256},{256,320},{320,384},{384,448},... | collective-permute-start | bytes 516104 | tf_op jit(solution)/shard_map/ppermute | solution.py:16
  55.5 0.0 collective-permute-done.1
  55.5 5.1 %collective-permute-start.3 = (bf16[112,768]{1,0:T(8,128)(2,1)S(1)}, bf16[112,768]{1,0:T(8,128)(2,1)S(1)}, u32[]{:S(2)}, u32[]{:S(2)}) collective-permute-start(bf16[112,768]{1,0:T(8,128)(2,1)S(1)} %collective-permute-done.1), channel_id=1, source_target_pairs={{0,704},{64,0},{128,64},{192,128},{256,192},{320,256},{384,320},{4... | collective-permute-start | bytes 516104 | tf_op jit(solution)/shard_map/ppermute | solution.py:16
  60.7 0.9 bitcast_dynamic-update-slice_fusion.9
  61.6 0.7 collective-permute-done.2
  62.3 1.9 %collective-permute-start.4 = (bf16[112,768]{1,0:T(8,128)(2,1)S(1)}, bf16[112,768]{1,0:T(8,128)(2,1)S(1)}, u32[]{:S(2)}, u32[]{:S(2)}) collective-permute-start(bf16[112,768]{1,0:T(8,128)(2,1)S(1)} %collective-permute-done.2), channel_id=1, source_target_pairs={{0,64},{64,128},{128,192},{192,256},{256,320},{320,384},{384,448},... | collective-permute-start | bytes 516104 | tf_op jit(solution)/shard_map/ppermute | solution.py:16
  64.2 0.0 collective-permute-done.3
  64.2 5.1 %collective-permute-start.5 = (bf16[112,768]{1,0:T(8,128)(2,1)S(1)}, bf16[112,768]{1,0:T(8,128)(2,1)S(1)}, u32[]{:S(2)}, u32[]{:S(2)}) collective-permute-start(bf16[112,768]{1,0:T(8,128)(2,1)S(1)} %collective-permute-done.3), channel_id=1, source_target_pairs={{0,704},{64,0},{128,64},{192,128},{256,192},{320,256},{384,320},{4... | collective-permute-start | bytes 516104 | tf_op jit(solution)/shard_map/ppermute | solution.py:16
  69.4 1.9 %collective-permute-done.4 = bf16[112,768]{1,0:T(8,128)(2,1)S(1)} collective-permute-done((bf16[112,768]{1,0:T(8,128)(2,1)S(1)}, bf16[112,768]{1,0:T(8,128)(2,1)S(1)}, u32[]{:S(2)}, u32[]{:S(2)}) %collective-permute-start.4) | collective-permute-done | bytes 172064 | tf_op jit(solution)/shard_map/ppermute | solution.py:16
  71.4 1.9 %collective-permute-start.6 = (bf16[112,768]{1,0:T(8,128)(2,1)S(1)}, bf16[112,768]{1,0:T(8,128)(2,1)S(1)}, u32[]{:S(2)}, u32[]{:S(2)}) collective-permute-start(bf16[112,768]{1,0:T(8,128)(2,1)S(1)} %collective-permute-done.4), channel_id=1, source_target_pairs={{0,64},{64,128},{128,192},{192,256},{256,320},{320,384},{384,448},... | collective-permute-start | bytes 516104 | tf_op jit(solution)/shard_map/ppermute | solution.py:16
  73.3 0.0 collective-permute-done.5
  73.3 5.4 %collective-permute-start.7 = (bf16[112,768]{1,0:T(8,128)(2,1)S(1)}, bf16[112,768]{1,0:T(8,128)(2,1)S(1)}, u32[]{:S(2)}, u32[]{:S(2)}) collective-permute-start(bf16[112,768]{1,0:T(8,128)(2,1)S(1)} %collective-permute-done.5), channel_id=1, source_target_pairs={{0,704},{64,0},{128,64},{192,128},{256,192},{320,256},{384,320},{4... | collective-permute-start | bytes 516104 | tf_op jit(solution)/shard_map/ppermute | solution.py:16
  78.8 2.4 %collective-permute-done.6 = bf16[112,768]{1,0:T(8,128)(2,1)S(1)} collective-permute-done((bf16[112,768]{1,0:T(8,128)(2,1)S(1)}, bf16[112,768]{1,0:T(8,128)(2,1)S(1)}, u32[]{:S(2)}, u32[]{:S(2)}) %collective-permute-start.6) | collective-permute-done | bytes 172064 | tf_op jit(solution)/shard_map/ppermute | solution.py:16
  81.2 1.9 %collective-permute-start.8 = (bf16[112,768]{1,0:T(8,128)(2,1)S(1)}, bf16[112,768]{1,0:T(8,128)(2,1)S(1)}, u32[]{:S(2)}, u32[]{:S(2)}) collective-permute-start(bf16[112,768]{1,0:T(8,128)(2,1)S(1)} %collective-permute-done.6), channel_id=1, source_target_pairs={{0,64},{64,128},{128,192},{192,256},{256,320},{320,384},{384,448},... | collective-permute-start | bytes 516104 | tf_op jit(solution)/shard_map/ppermute | solution.py:16
  83.1 0.1 collective-permute-done.7
  83.2 5.6 %collective-permute-start.9 = (bf16[112,768]{1,0:T(8,128)(2,1)S(1)}, bf16[112,768]{1,0:T(8,128)(2,1)S(1)}, u32[]{:S(2)}, u32[]{:S(2)}) collective-permute-start(bf16[112,768]{1,0:T(8,128)(2,1)S(1)} %collective-permute-done.7), channel_id=1, source_target_pairs={{0,704},{64,0},{128,64},{192,128},{256,192},{320,256},{384,320},{4... | collective-permute-start | bytes 516104 | tf_op jit(solution)/shard_map/ppermute | solution.py:16
  88.9 1.1 collective-permute-done.8
  90.0 1.9 %collective-permute-start.10 = (bf16[56,768]{1,0:T(8,128)(2,1)S(1)}, bf16[56,768]{1,0:T(8,128)(2,1)S(1)}, u32[]{:S(2)}, u32[]{:S(2)}) collective-permute-start(bf16[56,768]{1,0:T(8,128)(2,1)S(1)} %slice.16), channel_id=1, source_target_pairs={{0,64},{64,128},{128,192},{192,256},{256,320},{320,384},{384,448},... | collective-permute-start | bytes 258056 | tf_op jit(solution)/shard_map/ppermute | solution.py:16
  91.9 0.0 collective-permute-done.9
  92.0 5.4 %collective-permute-start.11 = (bf16[56,768]{1,0:T(8,128)(2,1)S(1)}, bf16[56,768]{1,0:T(8,128)(2,1)S(1)}, u32[]{:S(2)}, u32[]{:S(2)}) collective-permute-start(bf16[56,768]{1,0:T(8,128)(2,1)S(1)} %slice.17), channel_id=1, source_target_pairs={{0,704},{64,0},{128,64},{192,128},{256,192},{320,256},{384,320},{4... | collective-permute-start | bytes 258056 | tf_op jit(solution)/shard_map/ppermute | solution.py:16
  97.5 0.1 collective-permute-done.10
  97.6 1.9 %collective-permute-done.11 = bf16[56,768]{1,0:T(8,128)(2,1)S(1)} collective-permute-done((bf16[56,768]{1,0:T(8,128)(2,1)S(1)}, bf16[56,768]{1,0:T(8,128)(2,1)S(1)}, u32[]{:S(2)}, u32[]{:S(2)}) %collective-permute-start.11) | collective-permute-done | bytes 86048 | tf_op jit(solution)/shard_map/ppermute | solution.py:16
  99.5 0.0 copy-start.6
  99.5 0.8 convolution_bitcast_fusion
  100.4 0.5 copy-done.1
  100.8 0.9 copy-done.4
  101.7 1.6 convolution_convert_fusion
  103.3 0.0 all-to-all-done.2
  103.3 8.3 %all-to-all-start.3 = ((bf16[24,56,384]{2,1,0:T(8,128)(2,1)}), bf16[24,56,384]{2,1,0:T(8,128)(2,1)S(1)}, u32[]{:S(2)}, u32[]{:S(2)}) async-start(bf16[24,56,384]{2,1,0:T(8,128)(2,1)} %bitcast.42), calls=%async_computation.3 | async-start | bytes 2064384 | tf_op jit(solution)/shard_map/all_to_all | solution.py:27
  111.6 2.0 %multiply_convert_fusion.2 = (bf16[256,384]{1,0:T(8,128)(2,1)S(1)}, bf16[256,384]{1,0:T(8,128)(2,1)S(1)}) fusion(f32[256,768]{1,0:T(8,128)S(1)} %copy-done.5, bf16[1344,256]{1,0:T(8,128)(2,1)S(1)} %copy-done.7, bf16[1344,384]{1,0:T(8,128)(2,1)} %bitcast.14), kind=kOutput, calls=%fused_computation.16 | convolution fusion | flops 265519104 | bytes 2899968 | tf_op jit(solution)/shard_map/dot_general | solution.py:32
  113.7 0.7 convolution_convert_fusion.1
  114.4 1.9 %collective-permute-start.12 = (bf16[672,256]{1,0:T(8,128)(2,1)S(1)}, bf16[672,256]{1,0:T(8,128)(2,1)S(1)}, u32[]{:S(2)}, u32[]{:S(2)}) collective-permute-start(bf16[672,256]{1,0:T(8,128)(2,1)S(1)} %constant_dynamic-slice_fusion), channel_id=1, source_target_pairs={{0,1},{1,0},{2,3},{3,2},{4,5},{5,4},{6,7},{7,6},{8,9},{9,8},{10,11... | collective-permute-start | bytes 1032200 | tf_op jit(solution)/shard_map/ppermute | solution.py:16
  116.4 1.6 %collective-permute-done.12 = bf16[672,256]{1,0:T(8,128)(2,1)S(1)} collective-permute-done((bf16[672,256]{1,0:T(8,128)(2,1)S(1)}, bf16[672,256]{1,0:T(8,128)(2,1)S(1)}, u32[]{:S(2)}, u32[]{:S(2)}) %collective-permute-start.12) | collective-permute-done | bytes 344096 | tf_op jit(solution)/shard_map/ppermute | solution.py:16
  118.0 0.1 add_convert_fusion.2
  118.1 3.4 %collective-permute-start.13 = (bf16[672,256]{1,0:T(8,128)(2,1)S(1)}, bf16[672,256]{1,0:T(8,128)(2,1)S(1)}, u32[]{:S(2)}, u32[]{:S(2)}) collective-permute-start(bf16[672,256]{1,0:T(8,128)(2,1)S(1)} %add_convert_fusion.2), channel_id=1, source_target_pairs={{0,2},{1,7},{2,0},{3,5},{4,6},{5,3},{6,4},{7,1},{8,10},{9,15},{10,... | collective-permute-start | bytes 1032200 | tf_op jit(solution)/shard_map/ppermute | solution.py:77
  121.5 5.7 %collective-permute-done.13 = bf16[672,256]{1,0:T(8,128)(2,1)S(1)} collective-permute-done((bf16[672,256]{1,0:T(8,128)(2,1)S(1)}, bf16[672,256]{1,0:T(8,128)(2,1)S(1)}, u32[]{:S(2)}, u32[]{:S(2)}) %collective-permute-start.13) | collective-permute-done | bytes 344096 | tf_op jit(solution)/shard_map/ppermute | solution.py:77
  127.2 0.1 add_convert_fusion.1
  127.3 4.7 %collective-permute-start.14 = (bf16[672,256]{1,0:T(8,128)(2,1)S(1)}, bf16[672,256]{1,0:T(8,128)(2,1)S(1)}, u32[]{:S(2)}, u32[]{:S(2)}) collective-permute-start(bf16[672,256]{1,0:T(8,128)(2,1)S(1)} %add_convert_fusion.1), channel_id=1, source_target_pairs={{0,6},{1,3},{2,4},{3,1},{4,2},{5,7},{6,0},{7,5},{8,14},{9,11},{10,... | collective-permute-start | bytes 1032200 | tf_op jit(solution)/shard_map/ppermute | solution.py:77
  132.0 5.7 %collective-permute-done.14 = bf16[672,256]{1,0:T(8,128)(2,1)S(1)} collective-permute-done((bf16[672,256]{1,0:T(8,128)(2,1)S(1)}, bf16[672,256]{1,0:T(8,128)(2,1)S(1)}, u32[]{:S(2)}, u32[]{:S(2)}) %collective-permute-start.14) | collective-permute-done | bytes 344096 | tf_op jit(solution)/shard_map/ppermute | solution.py:77
  137.7 0.1 add_convert_fusion
  137.8 1.9 %collective-permute-start.15 = (bf16[672,256]{1,0:T(8,128)(2,1)S(1)}, bf16[672,256]{1,0:T(8,128)(2,1)S(1)}, u32[]{:S(2)}, u32[]{:S(2)}) collective-permute-start(bf16[672,256]{1,0:T(8,128)(2,1)S(1)} %add_convert_fusion), channel_id=1, source_target_pairs={{0,1},{1,0},{2,3},{3,2},{4,5},{5,4},{6,7},{7,6},{8,9},{9,8},{10,11... | collective-permute-start | bytes 1032200 | tf_op jit(solution)/shard_map/ppermute | solution.py:16
  139.7 1.6 %collective-permute-done.15 = bf16[672,256]{1,0:T(8,128)(2,1)S(1)} collective-permute-done((bf16[672,256]{1,0:T(8,128)(2,1)S(1)}, bf16[672,256]{1,0:T(8,128)(2,1)S(1)}, u32[]{:S(2)}, u32[]{:S(2)}) %collective-permute-start.15) | collective-permute-done | bytes 344096 | tf_op jit(solution)/shard_map/ppermute | solution.py:16
  141.4 0.0 all-to-all-done.3
  141.4 0.1 reduce_sum.21
  141.5 0.6 reshape.27
  142.2 7.5 %all-to-all-start.4 = ((bf16[4,14,384]{2,1,0:T(8,128)(2,1)}), bf16[4,14,384]{2,1,0:T(8,128)(2,1)S(1)}, u32[]{:S(2)}, u32[]{:S(2)}) async-start(bf16[4,14,384]{2,1,0:T(8,128)(2,1)} %reshape.27), calls=%async_computation.4 | async-start | bytes 98304 | tf_op jit(solution)/shard_map/all_to_all | solution.py:27
  149.7 0.9 maximum_bitcast_fusion
  150.6 9.6 %all-to-all-done.4 = bf16[4,14,384]{2,1,0:T(8,128)(2,1)S(1)} async-done(((bf16[4,14,384]{2,1,0:T(8,128)(2,1)}), bf16[4,14,384]{2,1,0:T(8,128)(2,1)S(1)}, u32[]{:S(2)}, u32[]{:S(2)}) %all-to-all-start.4) | async-done | bytes 43040 | tf_op jit(solution)/shard_map/all_to_all | solution.py:27
  160.2 0.6 convert_reduce_fusion
  (30 shorter events, 0.4 us)
Async XLA Ops:
  0.6 41.5 %copy-start = (bf16[256,1344]{0,1:T(8,128)(2,1)S(1)}, bf16[256,1344]{0,1:T(8,128)(2,1)}, u32[]{:S(2)}) copy-start(bf16[256,1344]{0,1:T(8,128)(2,1)} %param.7) | copy-start | bytes 2064388
  23.0 23.7 %all-to-all-start.1 = ((bf16[12,14,384]{2,1,0:T(8,128)(2,1)}), bf16[12,14,384]{2,1,0:T(8,128)(2,1)S(1)}, u32[]{:S(2)}, u32[]{:S(2)}) async-start(bf16[12,14,384]{2,1,0:T(8,128)(2,1)} %broadcast_in_dim.73), calls=%async_computation.1 | async-start | bytes 294912 | tf_op jit(solution)/shard_map/all_to_all | solution.py:21
  35.1 18.4 %collective-permute-start = (bf16[112,768]{1,0:T(8,128)(2,1)}, bf16[112,768]{1,0:T(8,128)(2,1)}, u32[]{:S(2)}, u32[]{:S(2)}) collective-permute-start(bf16[112,768]{1,0:T(8,128)(2,1)} %reshape.23), channel_id=1, source_target_pairs={{0,64},{64,128},{128,192},{192,256},{256,320},{320,384},{384,448},... | collective-permute-start | bytes 516104 | tf_op jit(solution)/shard_map/ppermute | solution.py:16
  39.0 16.5 %collective-permute-start.1 = (bf16[112,768]{1,0:T(8,128)(2,1)}, bf16[112,768]{1,0:T(8,128)(2,1)S(1)}, u32[]{:S(2)}, u32[]{:S(2)}) collective-permute-start(bf16[112,768]{1,0:T(8,128)(2,1)} %reshape.23), channel_id=1, source_target_pairs={{0,704},{64,0},{128,64},{192,128},{256,192},{320,256},{384,320},{4... | collective-permute-start | bytes 516104 | tf_op jit(solution)/shard_map/ppermute | solution.py:16
  47.8 55.5 %all-to-all-start.2 = ((bf16[8,168,384]{2,1,0:T(8,128)(2,1)}), bf16[8,168,384]{2,1,0:T(8,128)(2,1)}, u32[]{:S(2)}, u32[]{:S(2)}) async-start(bf16[8,168,384]{2,1,0:T(8,128)(2,1)} %broadcast_in_dim.75), calls=%async_computation.2 | async-start | bytes 2064384 | tf_op jit(solution)/shard_map/all_to_all | solution.py:21
  53.5 46.1 %copy-start.3 = (bf16[256,1344]{0,1:T(8,128)(2,1)S(1)}, bf16[256,1344]{0,1:T(8,128)(2,1)}, u32[]{:S(2)}) copy-start(bf16[256,1344]{0,1:T(8,128)(2,1)} %param.6) | copy-start | bytes 2064388
  53.5 8.9 %collective-permute-start.2 = (bf16[112,768]{1,0:T(8,128)(2,1)}, bf16[112,768]{1,0:T(8,128)(2,1)S(1)}, u32[]{:S(2)}, u32[]{:S(2)}) collective-permute-start(bf16[112,768]{1,0:T(8,128)(2,1)} %collective-permute-done), channel_id=1, source_target_pairs={{0,64},{64,128},{128,192},{192,256},{256,320},{320,384},{384,448},... | collective-permute-start | bytes 516104 | tf_op jit(solution)/shard_map/ppermute | solution.py:16
  55.5 8.7 %collective-permute-start.3 = (bf16[112,768]{1,0:T(8,128)(2,1)S(1)}, bf16[112,768]{1,0:T(8,128)(2,1)S(1)}, u32[]{:S(2)}, u32[]{:S(2)}) collective-permute-start(bf16[112,768]{1,0:T(8,128)(2,1)S(1)} %collective-permute-done.1), channel_id=1, source_target_pairs={{0,704},{64,0},{128,64},{192,128},{256,192},{320,256},{384,320},{4... | collective-permute-start | bytes 516104 | tf_op jit(solution)/shard_map/ppermute | solution.py:16
  62.3 9.1 %collective-permute-start.4 = (bf16[112,768]{1,0:T(8,128)(2,1)S(1)}, bf16[112,768]{1,0:T(8,128)(2,1)S(1)}, u32[]{:S(2)}, u32[]{:S(2)}) collective-permute-start(bf16[112,768]{1,0:T(8,128)(2,1)S(1)} %collective-permute-done.2), channel_id=1, source_target_pairs={{0,64},{64,128},{128,192},{192,256},{256,320},{320,384},{384,448},... | collective-permute-start | bytes 516104 | tf_op jit(solution)/shard_map/ppermute | solution.py:16
  64.2 9.1 %collective-permute-start.5 = (bf16[112,768]{1,0:T(8,128)(2,1)S(1)}, bf16[112,768]{1,0:T(8,128)(2,1)S(1)}, u32[]{:S(2)}, u32[]{:S(2)}) collective-permute-start(bf16[112,768]{1,0:T(8,128)(2,1)S(1)} %collective-permute-done.3), channel_id=1, source_target_pairs={{0,704},{64,0},{128,64},{192,128},{256,192},{320,256},{384,320},{4... | collective-permute-start | bytes 516104 | tf_op jit(solution)/shard_map/ppermute | solution.py:16
  71.4 9.8 %collective-permute-start.6 = (bf16[112,768]{1,0:T(8,128)(2,1)S(1)}, bf16[112,768]{1,0:T(8,128)(2,1)S(1)}, u32[]{:S(2)}, u32[]{:S(2)}) collective-permute-start(bf16[112,768]{1,0:T(8,128)(2,1)S(1)} %collective-permute-done.4), channel_id=1, source_target_pairs={{0,64},{64,128},{128,192},{192,256},{256,320},{320,384},{384,448},... | collective-permute-start | bytes 516104 | tf_op jit(solution)/shard_map/ppermute | solution.py:16
  73.3 9.9 %collective-permute-start.7 = (bf16[112,768]{1,0:T(8,128)(2,1)S(1)}, bf16[112,768]{1,0:T(8,128)(2,1)S(1)}, u32[]{:S(2)}, u32[]{:S(2)}) collective-permute-start(bf16[112,768]{1,0:T(8,128)(2,1)S(1)} %collective-permute-done.5), channel_id=1, source_target_pairs={{0,704},{64,0},{128,64},{192,128},{256,192},{320,256},{384,320},{4... | collective-permute-start | bytes 516104 | tf_op jit(solution)/shard_map/ppermute | solution.py:16
  81.2 8.8 %collective-permute-start.8 = (bf16[112,768]{1,0:T(8,128)(2,1)S(1)}, bf16[112,768]{1,0:T(8,128)(2,1)S(1)}, u32[]{:S(2)}, u32[]{:S(2)}) collective-permute-start(bf16[112,768]{1,0:T(8,128)(2,1)S(1)} %collective-permute-done.6), channel_id=1, source_target_pairs={{0,64},{64,128},{128,192},{192,256},{256,320},{320,384},{384,448},... | collective-permute-start | bytes 516104 | tf_op jit(solution)/shard_map/ppermute | solution.py:16
  83.2 8.7 %collective-permute-start.9 = (bf16[112,768]{1,0:T(8,128)(2,1)S(1)}, bf16[112,768]{1,0:T(8,128)(2,1)S(1)}, u32[]{:S(2)}, u32[]{:S(2)}) collective-permute-start(bf16[112,768]{1,0:T(8,128)(2,1)S(1)} %collective-permute-done.7), channel_id=1, source_target_pairs={{0,704},{64,0},{128,64},{192,128},{256,192},{320,256},{384,320},{4... | collective-permute-start | bytes 516104 | tf_op jit(solution)/shard_map/ppermute | solution.py:16
  90.0 7.6 %collective-permute-start.10 = (bf16[56,768]{1,0:T(8,128)(2,1)S(1)}, bf16[56,768]{1,0:T(8,128)(2,1)S(1)}, u32[]{:S(2)}, u32[]{:S(2)}) collective-permute-start(bf16[56,768]{1,0:T(8,128)(2,1)S(1)} %slice.16), channel_id=1, source_target_pairs={{0,64},{64,128},{128,192},{192,256},{256,320},{320,384},{384,448},... | collective-permute-start | bytes 258056 | tf_op jit(solution)/shard_map/ppermute | solution.py:16
  92.0 7.5 %collective-permute-start.11 = (bf16[56,768]{1,0:T(8,128)(2,1)S(1)}, bf16[56,768]{1,0:T(8,128)(2,1)S(1)}, u32[]{:S(2)}, u32[]{:S(2)}) collective-permute-start(bf16[56,768]{1,0:T(8,128)(2,1)S(1)} %slice.17), channel_id=1, source_target_pairs={{0,704},{64,0},{128,64},{192,128},{256,192},{320,256},{384,320},{4... | collective-permute-start | bytes 258056 | tf_op jit(solution)/shard_map/ppermute | solution.py:16
  99.5 1.3 copy-start.1
  99.5 2.2 %copy-start.6 = (bf16[1344,256]{1,0:T(8,128)(2,1)S(1)}, bf16[1344,256]{1,0:T(8,128)(2,1)}, u32[]{:S(2)}) copy-start(bf16[1344,256]{1,0:T(8,128)(2,1)} %fusion.2) | copy-start | bytes 2064388
  100.8 0.9 copy-start.4
  103.3 8.3 %copy-start.5 = (f32[256,768]{1,0:T(8,128)S(1)}, f32[256,768]{1,0:T(8,128)}, u32[]{:S(2)}) copy-start(f32[256,768]{1,0:T(8,128)} %copy-done.4) | copy-start | bytes 2359300
  103.3 8.3 %copy-start.7 = (bf16[1344,256]{1,0:T(8,128)(2,1)S(1)}, bf16[1344,256]{1,0:T(8,128)(2,1)}, u32[]{:S(2)}) copy-start(bf16[1344,256]{1,0:T(8,128)(2,1)} %fusion.2) | copy-start | bytes 2064388
  103.3 38.0 %all-to-all-start.3 = ((bf16[24,56,384]{2,1,0:T(8,128)(2,1)}), bf16[24,56,384]{2,1,0:T(8,128)(2,1)S(1)}, u32[]{:S(2)}, u32[]{:S(2)}) async-start(bf16[24,56,384]{2,1,0:T(8,128)(2,1)} %bitcast.42), calls=%async_computation.3 | async-start | bytes 2064384 | tf_op jit(solution)/shard_map/all_to_all | solution.py:27
  111.6 2.0 %copy-start.2 = (bf16[12,112,768]{2,1,0:T(8,128)(2,1)S(1)}, bf16[12,112,768]{2,1,0:T(8,128)(2,1)}, u32[]{:S(2)}) copy-start(bf16[12,112,768]{2,1,0:T(8,128)(2,1)} %copy-done.1) | copy-start | bytes 6193156
  114.4 3.5 %collective-permute-start.12 = (bf16[672,256]{1,0:T(8,128)(2,1)S(1)}, bf16[672,256]{1,0:T(8,128)(2,1)S(1)}, u32[]{:S(2)}, u32[]{:S(2)}) collective-permute-start(bf16[672,256]{1,0:T(8,128)(2,1)S(1)} %constant_dynamic-slice_fusion), channel_id=1, source_target_pairs={{0,1},{1,0},{2,3},{3,2},{4,5},{5,4},{6,7},{7,6},{8,9},{9,8},{10,11... | collective-permute-start | bytes 1032200 | tf_op jit(solution)/shard_map/ppermute | solution.py:16
  118.1 9.1 %collective-permute-start.13 = (bf16[672,256]{1,0:T(8,128)(2,1)S(1)}, bf16[672,256]{1,0:T(8,128)(2,1)S(1)}, u32[]{:S(2)}, u32[]{:S(2)}) collective-permute-start(bf16[672,256]{1,0:T(8,128)(2,1)S(1)} %add_convert_fusion.2), channel_id=1, source_target_pairs={{0,2},{1,7},{2,0},{3,5},{4,6},{5,3},{6,4},{7,1},{8,10},{9,15},{10,... | collective-permute-start | bytes 1032200 | tf_op jit(solution)/shard_map/ppermute | solution.py:77
  127.3 10.4 %collective-permute-start.14 = (bf16[672,256]{1,0:T(8,128)(2,1)S(1)}, bf16[672,256]{1,0:T(8,128)(2,1)S(1)}, u32[]{:S(2)}, u32[]{:S(2)}) collective-permute-start(bf16[672,256]{1,0:T(8,128)(2,1)S(1)} %add_convert_fusion.1), channel_id=1, source_target_pairs={{0,6},{1,3},{2,4},{3,1},{4,2},{5,7},{6,0},{7,5},{8,14},{9,11},{10,... | collective-permute-start | bytes 1032200 | tf_op jit(solution)/shard_map/ppermute | solution.py:77
  137.8 3.5 %collective-permute-start.15 = (bf16[672,256]{1,0:T(8,128)(2,1)S(1)}, bf16[672,256]{1,0:T(8,128)(2,1)S(1)}, u32[]{:S(2)}, u32[]{:S(2)}) collective-permute-start(bf16[672,256]{1,0:T(8,128)(2,1)S(1)} %add_convert_fusion), channel_id=1, source_target_pairs={{0,1},{1,0},{2,3},{3,2},{4,5},{5,4},{6,7},{7,6},{8,9},{9,8},{10,11... | collective-permute-start | bytes 1032200 | tf_op jit(solution)/shard_map/ppermute | solution.py:16
  142.2 18.0 %all-to-all-start.4 = ((bf16[4,14,384]{2,1,0:T(8,128)(2,1)}), bf16[4,14,384]{2,1,0:T(8,128)(2,1)S(1)}, u32[]{:S(2)}, u32[]{:S(2)}) async-start(bf16[4,14,384]{2,1,0:T(8,128)(2,1)} %reshape.27), calls=%async_computation.4 | async-start | bytes 98304 | tf_op jit(solution)/shard_map/all_to_all | solution.py:27

commit v6 on v5

--- a/solution.py
+++ b/solution.py
@@ -28,12 +28,6 @@
     return got.astype(jnp.float32).sum(axis=0)
 
 
-def contract_rows(left, right):
-    return lax.dot_general(
-        left, right, (((0,), (0,)), ((), ())), preferred_element_type=jnp.float32
-    )
-
-
 def contract_cols(left, right):
     return lax.dot_general(
         left, right, (((1,), (1,)), ((), ())), preferred_element_type=jnp.float32
@@ -46,25 +40,29 @@
     return (source[:, None] == spot).astype(jnp.bfloat16)
 
 
-def around(block, axis):
+def around(block, axis, widths):
     peers = lax.axis_size(axis)
     rows = block.shape[0]
     half = rows // 2
     place = lax.axis_index(axis)
+    ends = np.cumsum(widths)
+    wholes = [jnp.zeros((peers, rows, w), block.dtype) for w in widths]
 
-    def put(whole, part, owner, start):
+    def put(part, owner, start):
         owner = (owner + peers) % peers
-        return lax.dynamic_update_slice(whole, part[None], (owner, start, 0))
+        for k, (end, w) in enumerate(zip(ends, widths)):
+            piece = part[None, :, end - w : end]
+            wholes[k] = lax.dynamic_update_slice(wholes[k], piece, (owner, start, 0))
 
-    whole = put(jnp.zeros((peers, *block.shape), block.dtype), block, place, 0)
+    put(block, place, 0)
     up = down = block
     for step in range(1, peers // 2):
         up, down = shifted(up, axis, 1), shifted(down, axis, -1)
-        whole = put(whole, up, place - step, 0)
-        whole = put(whole, down, place + step, 0)
-    whole = put(whole, shifted(up[:half], axis, 1), place + peers // 2, 0)
-    whole = put(whole, shifted(down[half:], axis, -1), place + peers // 2, half)
-    return whole.reshape(peers * rows, -1)
+        put(up, place - step, 0)
+        put(down, place + step, 0)
+    put(shifted(up[:half], axis, 1), place + peers // 2, 0)
+    put(shifted(down[half:], axis, -1), place + peers // 2, half)
+    return [w.reshape(peers * rows, -1) for w in wholes]
 
 
 def paired(array, turn):
@@ -101,11 +99,9 @@
     rows, units = gate_weight.shape
     width = tokens.shape[1]
 
-    gate_up = jnp.concatenate([gate_weight, up_weight], axis=1)
-    gate_up = sent_to_all(gate_up, "fs_1").reshape(inner * rows, 2 * units)
-    gate_up = around(gate_up, FS_0)
-    down = sent_to_all(down_weight.T, FS_0[::-1]).reshape(-1, units)
-    down = sent_to_all(down, "fs_1").reshape(width, units)
+    weights = jnp.concatenate([gate_weight, up_weight, down_weight.T], axis=1)
+    weights = sent_to_all(weights, "fs_1").reshape(inner * rows, 3 * units)
+    gate_up, down = around(weights, FS_0, (2 * units, units))
 
     spot = np.arange(width).reshape(FAR, near, inner, rows).transpose(2, 1, 0, 3).reshape(-1)
     turned_cotangent = contract_cols(picked(spot), cotangent).astype(jnp.bfloat16)
@@ -123,7 +119,7 @@
     terms = terms.astype(jnp.bfloat16).reshape(FAR, rows, units)
     down_grad = exchanged(terms, "fs_0h").T
 
-    hidden_grad = contract_rows(turned_cotangent, down)
+    hidden_grad = jnp.dot(cotangent, down, preferred_element_type=jnp.float32)
     gate_pre_grad = (
         hidden_grad * up_pre * sigmoid_gate * (1.0 + gate_pre * (1.0 - sigmoid_gate))
     ).astype(jnp.bfloat16)

time: 162 us -> 148 us (0.914)
  the two profiles are of different devices: /device:TPU:8 before, /device:TPU:14 now
where the time goes in v6:
time: 148 us; the launch traced here: 147 us
  starting transfers between devices  81.4 us (55%)
  waiting for transfers between devices  52.1 us (35%)
  matrix products  7.1 us (5%)
  other arithmetic  2.79 us (2%)
  local copies, waits for them, and re-layouts  2.74 us (2%)
    ppermute x14, starting transfers between devices, shifted(): lax.ppermute(array, axis, [(k, (k + step) % peers) for k in range(peers)])  56.6 us
    ppermute x14, waiting for transfers between devices, shifted(): lax.ppermute(array, axis, [(k, (k + step) % peers) for k in range(peers)])  19.3 us
    ppermute x2, waiting for transfers between devices, paired(): return lax.ppermute(array, ('chip', 'core'), pairs)  14.4 us
    all_to_all x2, starting transfers between devices, exchanged(): got = lax.all_to_all(parts, axis, 0, 0, tiled=True)  12.1 us
    all_to_all x2, waiting for transfers between devices, exchanged(): got = lax.all_to_all(parts, axis, 0, 0, tiled=True)  9.65 us
    all_to_all x1, waiting for transfers between devices, sent_to_all(): lax.all_to_all(jnp.broadcast_to(array[None], (peers, *array.shape)), axis...  8.86 us
    all_to_all x1, starting transfers between devices, sent_to_all(): lax.all_to_all(jnp.broadcast_to(array[None], (peers, *array.shape)), axis...  7.55 us
    ppermute x2, starting transfers between devices, paired(): return lax.ppermute(array, ('chip', 'core'), pairs)  5.12 us
  transfers between devices with their start and end apart: 19, of which 14 were waited for; matrix products, arithmetic and copies ran while one was open for 5% of the time, Pallas kernels for 0%

profile of v6, /device:TPU:14, one launch (start us, length us, event | category | flops | bytes accessed | tf_op | source)
XLA Modules:
  0.0 147.4 jit_solution(14554018966053196754)
XLA Ops:
  0.6 0.0 copy-start
  0.6 0.8 pad_maximum_fusion
  1.5 0.7 broadcast_in_dim.92
  2.2 7.5 %all-to-all-start = ((bf16[8,14,1152]{2,1,0:T(8,128)(2,1)}), bf16[8,14,1152]{2,1,0:T(8,128)(2,1)S(1)}, u32[]{:S(2)}, u32[]{:S(2)}) async-start(bf16[8,14,1152]{2,1,0:T(8,128)(2,1)} %broadcast_in_dim.92), calls=%async_computation | async-start | bytes 589824 | tf_op jit(solution)/shard_map/all_to_all | solution.py:21
  9.7 0.0 copy-done
  9.7 2.2 %fusion.2 = bf16[1344,256]{1,0:T(8,128)(2,1)S(1)} fusion(bf16[256,1344]{0,1:T(8,128)(2,1)S(1)} %copy-done, s32[1344]{0:T(1024)} %constant.99.clone), kind=kOutput, calls=%fused_computation.5 | convolution fusion | flops 926994432 | bytes 1381632 | tf_op jit(solution)/shard_map/dot_general | solution.py:32
  12.0 8.9 %all-to-all-done = bf16[8,14,1152]{2,1,0:T(8,128)(2,1)S(1)} async-done(((bf16[8,14,1152]{2,1,0:T(8,128)(2,1)}), bf16[8,14,1152]{2,1,0:T(8,128)(2,1)S(1)}, u32[]{:S(2)}, u32[]{:S(2)}) %all-to-all-start) | async-done | bytes 258080 | tf_op jit(solution)/shard_map/all_to_all | solution.py:21
  20.9 0.1 reshape.21
  20.9 4.3 %collective-permute-start = (bf16[112,1152]{1,0:T(8,128)(2,1)S(1)}, bf16[112,1152]{1,0:T(8,128)(2,1)S(1)}, u32[]{:S(2)}, u32[]{:S(2)}) collective-permute-start(bf16[112,1152]{1,0:T(8,128)(2,1)S(1)} %reshape.21), channel_id=1, source_target_pairs={{0,64},{64,128},{128,192},{192,256},{256,320},{320,384},{384,448},... | collective-permute-start | bytes 774152 | tf_op jit(solution)/shard_map/ppermute | solution.py:16
  25.2 12.2 %collective-permute-start.1 = (bf16[112,1152]{1,0:T(8,128)(2,1)S(1)}, bf16[112,1152]{1,0:T(8,128)(2,1)S(1)}, u32[]{:S(2)}, u32[]{:S(2)}) collective-permute-start(bf16[112,1152]{1,0:T(8,128)(2,1)S(1)} %reshape.21), channel_id=1, source_target_pairs={{0,704},{64,0},{128,64},{192,128},{256,192},{320,256},{384,320},{4... | collective-permute-start | bytes 774152 | tf_op jit(solution)/shard_map/ppermute | solution.py:16
  37.5 0.1 broadcast_in_dim.106
  37.6 0.1 broadcast_in_dim.91
  37.8 2.1 %collective-permute-done = bf16[112,1152]{1,0:T(8,128)(2,1)S(1)} collective-permute-done((bf16[112,1152]{1,0:T(8,128)(2,1)S(1)}, bf16[112,1152]{1,0:T(8,128)(2,1)S(1)}, u32[]{:S(2)}, u32[]{:S(2)}) %collective-permute-start) | collective-permute-done | bytes 258080 | tf_op jit(solution)/shard_map/ppermute | solution.py:16
  39.8 1.9 %collective-permute-start.2 = (bf16[112,1152]{1,0:T(8,128)(2,1)S(1)}, bf16[112,1152]{1,0:T(8,128)(2,1)S(1)}, u32[]{:S(2)}, u32[]{:S(2)}) collective-permute-start(bf16[112,1152]{1,0:T(8,128)(2,1)S(1)} %collective-permute-done), channel_id=1, source_target_pairs={{0,64},{64,128},{128,192},{192,256},{256,320},{320,384},{384,448},... | collective-permute-start | bytes 774152 | tf_op jit(solution)/shard_map/ppermute | solution.py:16
  41.8 0.0 collective-permute-done.1
  41.8 5.1 %collective-permute-start.3 = (bf16[112,1152]{1,0:T(8,128)(2,1)S(1)}, bf16[112,1152]{1,0:T(8,128)(2,1)S(1)}, u32[]{:S(2)}, u32[]{:S(2)}) collective-permute-start(bf16[112,1152]{1,0:T(8,128)(2,1)S(1)} %collective-permute-done.1), channel_id=1, source_target_pairs={{0,704},{64,0},{128,64},{192,128},{256,192},{320,256},{384,320},{4... | collective-permute-start | bytes 774152 | tf_op jit(solution)/shard_map/ppermute | solution.py:16
  47.0 2.2 %collective-permute-done.2 = bf16[112,1152]{1,0:T(8,128)(2,1)S(1)} collective-permute-done((bf16[112,1152]{1,0:T(8,128)(2,1)S(1)}, bf16[112,1152]{1,0:T(8,128)(2,1)S(1)}, u32[]{:S(2)}, u32[]{:S(2)}) %collective-permute-start.2) | collective-permute-done | bytes 258080 | tf_op jit(solution)/shard_map/ppermute | solution.py:16
  49.3 1.9 %collective-permute-start.4 = (bf16[112,1152]{1,0:T(8,128)(2,1)S(1)}, bf16[112,1152]{1,0:T(8,128)(2,1)S(1)}, u32[]{:S(2)}, u32[]{:S(2)}) collective-permute-start(bf16[112,1152]{1,0:T(8,128)(2,1)S(1)} %collective-permute-done.2), channel_id=1, source_target_pairs={{0,64},{64,128},{128,192},{192,256},{256,320},{320,384},{384,448},... | collective-permute-start | bytes 774152 | tf_op jit(solution)/shard_map/ppermute | solution.py:16
  51.2 0.0 collective-permute-done.3
  51.2 5.1 %collective-permute-start.5 = (bf16[112,1152]{1,0:T(8,128)(2,1)S(1)}, bf16[112,1152]{1,0:T(8,128)(2,1)S(1)}, u32[]{:S(2)}, u32[]{:S(2)}) collective-permute-start(bf16[112,1152]{1,0:T(8,128)(2,1)S(1)} %collective-permute-done.3), channel_id=1, source_target_pairs={{0,704},{64,0},{128,64},{192,128},{256,192},{320,256},{384,320},{4... | collective-permute-start | bytes 774152 | tf_op jit(solution)/shard_map/ppermute | solution.py:16
  56.4 0.0 copy-start.3
  56.4 2.7 %collective-permute-done.4 = bf16[112,1152]{1,0:T(8,128)(2,1)S(1)} collective-permute-done((bf16[112,1152]{1,0:T(8,128)(2,1)S(1)}, bf16[112,1152]{1,0:T(8,128)(2,1)S(1)}, u32[]{:S(2)}, u32[]{:S(2)}) %collective-permute-start.4) | collective-permute-done | bytes 258080 | tf_op jit(solution)/shard_map/ppermute | solution.py:16
  59.1 1.9 %collective-permute-start.6 = (bf16[112,1152]{1,0:T(8,128)(2,1)S(1)}, bf16[112,1152]{1,0:T(8,128)(2,1)S(1)}, u32[]{:S(2)}, u32[]{:S(2)}) collective-permute-start(bf16[112,1152]{1,0:T(8,128)(2,1)S(1)} %collective-permute-done.4), channel_id=1, source_target_pairs={{0,64},{64,128},{128,192},{192,256},{256,320},{320,384},{384,448},... | collective-permute-start | bytes 774152 | tf_op jit(solution)/shard_map/ppermute | solution.py:16
  61.0 0.0 collective-permute-done.5
  61.0 5.4 %collective-permute-start.7 = (bf16[112,1152]{1,0:T(8,128)(2,1)S(1)}, bf16[112,1152]{1,0:T(8,128)(2,1)S(1)}, u32[]{:S(2)}, u32[]{:S(2)}) collective-permute-start(bf16[112,1152]{1,0:T(8,128)(2,1)S(1)} %collective-permute-done.5), channel_id=1, source_target_pairs={{0,704},{64,0},{128,64},{192,128},{256,192},{320,256},{384,320},{4... | collective-permute-start | bytes 774152 | tf_op jit(solution)/shard_map/ppermute | solution.py:16
  66.6 3.5 %collective-permute-done.6 = bf16[112,1152]{1,0:T(8,128)(2,1)S(1)} collective-permute-done((bf16[112,1152]{1,0:T(8,128)(2,1)S(1)}, bf16[112,1152]{1,0:T(8,128)(2,1)S(1)}, u32[]{:S(2)}, u32[]{:S(2)}) %collective-permute-start.6) | collective-permute-done | bytes 258080 | tf_op jit(solution)/shard_map/ppermute | solution.py:16
  70.1 1.9 %collective-permute-start.8 = (bf16[112,1152]{1,0:T(8,128)(2,1)S(1)}, bf16[112,1152]{1,0:T(8,128)(2,1)S(1)}, u32[]{:S(2)}, u32[]{:S(2)}) collective-permute-start(bf16[112,1152]{1,0:T(8,128)(2,1)S(1)} %collective-permute-done.6), channel_id=1, source_target_pairs={{0,64},{64,128},{128,192},{192,256},{256,320},{320,384},{384,448},... | collective-permute-start | bytes 774152 | tf_op jit(solution)/shard_map/ppermute | solution.py:16
  72.0 0.1 collective-permute-done.7
  72.1 5.6 %collective-permute-start.9 = (bf16[112,1152]{1,0:T(8,128)(2,1)S(1)}, bf16[112,1152]{1,0:T(8,128)(2,1)S(1)}, u32[]{:S(2)}, u32[]{:S(2)}) collective-permute-start(bf16[112,1152]{1,0:T(8,128)(2,1)S(1)} %collective-permute-done.7), channel_id=1, source_target_pairs={{0,704},{64,0},{128,64},{192,128},{256,192},{320,256},{384,320},{4... | collective-permute-start | bytes 774152 | tf_op jit(solution)/shard_map/ppermute | solution.py:16
  77.8 3.1 %collective-permute-done.8 = bf16[112,1152]{1,0:T(8,128)(2,1)S(1)} collective-permute-done((bf16[112,1152]{1,0:T(8,128)(2,1)S(1)}, bf16[112,1152]{1,0:T(8,128)(2,1)S(1)}, u32[]{:S(2)}, u32[]{:S(2)}) %collective-permute-start.8) | collective-permute-done | bytes 258080 | tf_op jit(solution)/shard_map/ppermute | solution.py:16
  80.9 1.9 %collective-permute-start.10 = (bf16[56,1152]{1,0:T(8,128)(2,1)S(1)}, bf16[56,1152]{1,0:T(8,128)(2,1)S(1)}, u32[]{:S(2)}, u32[]{:S(2)}) collective-permute-start(bf16[56,1152]{1,0:T(8,128)(2,1)S(1)} %slice.131), channel_id=1, source_target_pairs={{0,64},{64,128},{128,192},{192,256},{256,320},{320,384},{384,448},... | collective-permute-start | bytes 387080 | tf_op jit(solution)/shard_map/ppermute | solution.py:16
  82.8 0.0 collective-permute-done.9
  82.9 5.5 %collective-permute-start.11 = (bf16[56,1152]{1,0:T(8,128)(2,1)S(1)}, bf16[56,1152]{1,0:T(8,128)(2,1)S(1)}, u32[]{:S(2)}, u32[]{:S(2)}) collective-permute-start(bf16[56,1152]{1,0:T(8,128)(2,1)S(1)} %slice.133), channel_id=1, source_target_pairs={{0,704},{64,0},{128,64},{192,128},{256,192},{320,256},{384,320},{4... | collective-permute-start | bytes 387080 | tf_op jit(solution)/shard_map/ppermute | solution.py:16
  88.5 0.5 collective-permute-done.10
  89.0 1.8 %collective-permute-done.11 = bf16[56,1152]{1,0:T(8,128)(2,1)S(1)} collective-permute-done((bf16[56,1152]{1,0:T(8,128)(2,1)S(1)}, bf16[56,1152]{1,0:T(8,128)(2,1)S(1)}, u32[]{:S(2)}, u32[]{:S(2)}) %collective-permute-start.11) | collective-permute-done | bytes 129056 | tf_op jit(solution)/shard_map/ppermute | solution.py:16
  90.8 0.0 copy-start.1
  90.9 0.0 copy-done.3
  90.9 0.8 convolution_bitcast_fusion
  91.7 0.5 copy-done.1
  92.2 1.6 %convolution_convert_fusion = bf16[1344,384]{1,0:T(8,128)(2,1)} fusion(bf16[1344,256]{1,0:T(8,128)(2,1)S(1)} %fusion.2, f32[256,768]{0,1:T(8,128)S(1)} %convolution_bitcast_fusion), kind=kOutput, calls=%fused_computation.3 | convolution fusion | flops 265347072 | bytes 2506752 | tf_op jit(solution)/shard_map/dot_general | solution.py:116
  93.8 0.0 copy-done.4
  93.8 3.8 %all-to-all-start.1 = ((bf16[24,56,384]{2,1,0:T(8,128)(2,1)}), bf16[24,56,384]{2,1,0:T(8,128)(2,1)S(1)}, u32[]{:S(2)}, u32[]{:S(2)}) async-start(bf16[24,56,384]{2,1,0:T(8,128)(2,1)} %bitcast.125), calls=%async_computation.1 | async-start | bytes 2064384 | tf_op jit(solution)/shard_map/all_to_all | solution.py:27
  97.6 0.0 copy-start.2
  97.6 1.8 %multiply_convert_fusion.2 = (bf16[256,384]{0,1:T(8,128)(2,1)S(1)}, bf16[256,384]{0,1:T(8,128)(2,1)S(1)}) fusion(f32[256,768]{0,1:T(8,128)} %copy-done.4, bf16[1344,384]{1,0:T(8,128)(2,1)S(1)} %bitcast.124, bf16[256,1344]{0,1:T(8,128)(2,1)S(1)} %copy-done), kind=kOutput, calls=%fused_computation.17 | convolution fusion | flops 265519104 | bytes 2899968 | tf_op jit(solution)/shard_map/dot_general | solution.py:122
  99.4 0.0 copy-done.2
  99.4 0.7 convolution_convert_fusion.1
  100.2 1.9 %collective-permute-start.12 = (bf16[672,256]{1,0:T(8,128)(2,1)S(1)}, bf16[672,256]{1,0:T(8,128)(2,1)S(1)}, u32[]{:S(2)}, u32[]{:S(2)}) collective-permute-start(bf16[672,256]{1,0:T(8,128)(2,1)S(1)} %constant_dynamic-slice_fusion), channel_id=1, source_target_pairs={{0,1},{1,0},{2,3},{3,2},{4,5},{5,4},{6,7},{7,6},{8,9},{9,8},{10,11... | collective-permute-start | bytes 1032200 | tf_op jit(solution)/shard_map/ppermute | solution.py:16
  102.1 1.6 %collective-permute-done.12 = bf16[672,256]{1,0:T(8,128)(2,1)S(1)} collective-permute-done((bf16[672,256]{1,0:T(8,128)(2,1)S(1)}, bf16[672,256]{1,0:T(8,128)(2,1)S(1)}, u32[]{:S(2)}, u32[]{:S(2)}) %collective-permute-start.12) | collective-permute-done | bytes 344096 | tf_op jit(solution)/shard_map/ppermute | solution.py:16
  103.7 0.1 add_convert_fusion.2
  103.8 2.7 %collective-permute-start.13 = (bf16[672,256]{1,0:T(8,128)(2,1)S(1)}, bf16[672,256]{1,0:T(8,128)(2,1)S(1)}, u32[]{:S(2)}, u32[]{:S(2)}) collective-permute-start(bf16[672,256]{1,0:T(8,128)(2,1)S(1)} %add_convert_fusion.2), channel_id=1, source_target_pairs={{0,2},{1,7},{2,0},{3,5},{4,6},{5,3},{6,4},{7,1},{8,10},{9,15},{10,... | collective-permute-start | bytes 1032200 | tf_op jit(solution)/shard_map/ppermute | solution.py:75
  106.5 6.4 %collective-permute-done.13 = bf16[672,256]{1,0:T(8,128)(2,1)S(1)} collective-permute-done((bf16[672,256]{1,0:T(8,128)(2,1)S(1)}, bf16[672,256]{1,0:T(8,128)(2,1)S(1)}, u32[]{:S(2)}, u32[]{:S(2)}) %collective-permute-start.13) | collective-permute-done | bytes 344096 | tf_op jit(solution)/shard_map/ppermute | solution.py:75
  112.9 0.1 add_convert_fusion.1
  113.0 2.4 %collective-permute-start.14 = (bf16[672,256]{1,0:T(8,128)(2,1)S(1)}, bf16[672,256]{1,0:T(8,128)(2,1)S(1)}, u32[]{:S(2)}, u32[]{:S(2)}) collective-permute-start(bf16[672,256]{1,0:T(8,128)(2,1)S(1)} %add_convert_fusion.1), channel_id=1, source_target_pairs={{0,6},{1,3},{2,4},{3,1},{4,2},{5,7},{6,0},{7,5},{8,14},{9,11},{10,... | collective-permute-start | bytes 1032200 | tf_op jit(solution)/shard_map/ppermute | solution.py:75
  115.4 8.0 %collective-permute-done.14 = bf16[672,256]{1,0:T(8,128)(2,1)S(1)} collective-permute-done((bf16[672,256]{1,0:T(8,128)(2,1)S(1)}, bf16[672,256]{1,0:T(8,128)(2,1)S(1)}, u32[]{:S(2)}, u32[]{:S(2)}) %collective-permute-start.14) | collective-permute-done | bytes 344096 | tf_op jit(solution)/shard_map/ppermute | solution.py:75
  123.4 0.1 add_convert_fusion
  123.5 1.9 %collective-permute-start.15 = (bf16[672,256]{1,0:T(8,128)(2,1)S(1)}, bf16[672,256]{1,0:T(8,128)(2,1)S(1)}, u32[]{:S(2)}, u32[]{:S(2)}) collective-permute-start(bf16[672,256]{1,0:T(8,128)(2,1)S(1)} %add_convert_fusion), channel_id=1, source_target_pairs={{0,1},{1,0},{2,3},{3,2},{4,5},{5,4},{6,7},{7,6},{8,9},{9,8},{10,11... | collective-permute-start | bytes 1032200 | tf_op jit(solution)/shard_map/ppermute | solution.py:16
  125.4 1.6 %collective-permute-done.15 = bf16[672,256]{1,0:T(8,128)(2,1)S(1)} collective-permute-done((bf16[672,256]{1,0:T(8,128)(2,1)S(1)}, bf16[672,256]{1,0:T(8,128)(2,1)S(1)}, u32[]{:S(2)}, u32[]{:S(2)}) %collective-permute-start.15) | collective-permute-done | bytes 344096 | tf_op jit(solution)/shard_map/ppermute | solution.py:16
  127.1 0.0 all-to-all-done.1
  127.1 0.1 reduce_sum.21
  127.2 0.6 reshape.25
  127.9 8.3 %all-to-all-start.2 = ((bf16[4,14,384]{2,1,0:T(8,128)(2,1)}), bf16[4,14,384]{2,1,0:T(8,128)(2,1)S(1)}, u32[]{:S(2)}, u32[]{:S(2)}) async-start(bf16[4,14,384]{2,1,0:T(8,128)(2,1)} %reshape.25), calls=%async_computation.2 | async-start | bytes 98304 | tf_op jit(solution)/shard_map/all_to_all | solution.py:27
  136.2 0.9 maximum_bitcast_fusion
  137.1 9.6 %all-to-all-done.2 = bf16[4,14,384]{2,1,0:T(8,128)(2,1)S(1)} async-done(((bf16[4,14,384]{2,1,0:T(8,128)(2,1)}), bf16[4,14,384]{2,1,0:T(8,128)(2,1)S(1)}, u32[]{:S(2)}, u32[]{:S(2)}) %all-to-all-start.2) | async-done | bytes 43040 | tf_op jit(solution)/shard_map/all_to_all | solution.py:27
  146.7 0.6 convert_reduce_fusion
  (31 shorter events, 0.6 us)
Async XLA Ops:
  0.6 9.1 %copy-start = (bf16[256,1344]{0,1:T(8,128)(2,1)S(1)}, bf16[256,1344]{0,1:T(8,128)(2,1)}, u32[]{:S(2)}) copy-start(bf16[256,1344]{0,1:T(8,128)(2,1)} %param.7) | copy-start | bytes 2064388
  2.2 18.7 %all-to-all-start = ((bf16[8,14,1152]{2,1,0:T(8,128)(2,1)}), bf16[8,14,1152]{2,1,0:T(8,128)(2,1)S(1)}, u32[]{:S(2)}, u32[]{:S(2)}) async-start(bf16[8,14,1152]{2,1,0:T(8,128)(2,1)} %broadcast_in_dim.92), calls=%async_computation | async-start | bytes 589824 | tf_op jit(solution)/shard_map/all_to_all | solution.py:21
  20.9 18.9 %collective-permute-start = (bf16[112,1152]{1,0:T(8,128)(2,1)S(1)}, bf16[112,1152]{1,0:T(8,128)(2,1)S(1)}, u32[]{:S(2)}, u32[]{:S(2)}) collective-permute-start(bf16[112,1152]{1,0:T(8,128)(2,1)S(1)} %reshape.21), channel_id=1, source_target_pairs={{0,64},{64,128},{128,192},{192,256},{256,320},{320,384},{384,448},... | collective-permute-start | bytes 774152 | tf_op jit(solution)/shard_map/ppermute | solution.py:16
  25.2 16.5 %collective-permute-start.1 = (bf16[112,1152]{1,0:T(8,128)(2,1)S(1)}, bf16[112,1152]{1,0:T(8,128)(2,1)S(1)}, u32[]{:S(2)}, u32[]{:S(2)}) collective-permute-start(bf16[112,1152]{1,0:T(8,128)(2,1)S(1)} %reshape.21), channel_id=1, source_target_pairs={{0,704},{64,0},{128,64},{192,128},{256,192},{320,256},{384,320},{4... | collective-permute-start | bytes 774152 | tf_op jit(solution)/shard_map/ppermute | solution.py:16
  39.8 9.4 %collective-permute-start.2 = (bf16[112,1152]{1,0:T(8,128)(2,1)S(1)}, bf16[112,1152]{1,0:T(8,128)(2,1)S(1)}, u32[]{:S(2)}, u32[]{:S(2)}) collective-permute-start(bf16[112,1152]{1,0:T(8,128)(2,1)S(1)} %collective-permute-done), channel_id=1, source_target_pairs={{0,64},{64,128},{128,192},{192,256},{256,320},{320,384},{384,448},... | collective-permute-start | bytes 774152 | tf_op jit(solution)/shard_map/ppermute | solution.py:16
  41.8 9.4 %collective-permute-start.3 = (bf16[112,1152]{1,0:T(8,128)(2,1)S(1)}, bf16[112,1152]{1,0:T(8,128)(2,1)S(1)}, u32[]{:S(2)}, u32[]{:S(2)}) collective-permute-start(bf16[112,1152]{1,0:T(8,128)(2,1)S(1)} %collective-permute-done.1), channel_id=1, source_target_pairs={{0,704},{64,0},{128,64},{192,128},{256,192},{320,256},{384,320},{4... | collective-permute-start | bytes 774152 | tf_op jit(solution)/shard_map/ppermute | solution.py:16
  49.3 9.8 %collective-permute-start.4 = (bf16[112,1152]{1,0:T(8,128)(2,1)S(1)}, bf16[112,1152]{1,0:T(8,128)(2,1)S(1)}, u32[]{:S(2)}, u32[]{:S(2)}) collective-permute-start(bf16[112,1152]{1,0:T(8,128)(2,1)S(1)} %collective-permute-done.2), channel_id=1, source_target_pairs={{0,64},{64,128},{128,192},{192,256},{256,320},{320,384},{384,448},... | collective-permute-start | bytes 774152 | tf_op jit(solution)/shard_map/ppermute | solution.py:16
  51.2 9.8 %collective-permute-start.5 = (bf16[112,1152]{1,0:T(8,128)(2,1)S(1)}, bf16[112,1152]{1,0:T(8,128)(2,1)S(1)}, u32[]{:S(2)}, u32[]{:S(2)}) collective-permute-start(bf16[112,1152]{1,0:T(8,128)(2,1)S(1)} %collective-permute-done.3), channel_id=1, source_target_pairs={{0,704},{64,0},{128,64},{192,128},{256,192},{320,256},{384,320},{4... | collective-permute-start | bytes 774152 | tf_op jit(solution)/shard_map/ppermute | solution.py:16
  56.4 34.4 %copy-start.3 = (bf16[256,1344]{0,1:T(8,128)(2,1)S(1)}, bf16[256,1344]{0,1:T(8,128)(2,1)}, u32[]{:S(2)}) copy-start(bf16[256,1344]{0,1:T(8,128)(2,1)} %param.6) | copy-start | bytes 2064388
  59.1 11.0 %collective-permute-start.6 = (bf16[112,1152]{1,0:T(8,128)(2,1)S(1)}, bf16[112,1152]{1,0:T(8,128)(2,1)S(1)}, u32[]{:S(2)}, u32[]{:S(2)}) collective-permute-start(bf16[112,1152]{1,0:T(8,128)(2,1)S(1)} %collective-permute-done.4), channel_id=1, source_target_pairs={{0,64},{64,128},{128,192},{192,256},{256,320},{320,384},{384,448},... | collective-permute-start | bytes 774152 | tf_op jit(solution)/shard_map/ppermute | solution.py:16
  61.0 11.1 %collective-permute-start.7 = (bf16[112,1152]{1,0:T(8,128)(2,1)S(1)}, bf16[112,1152]{1,0:T(8,128)(2,1)S(1)}, u32[]{:S(2)}, u32[]{:S(2)}) collective-permute-start(bf16[112,1152]{1,0:T(8,128)(2,1)S(1)} %collective-permute-done.5), channel_id=1, source_target_pairs={{0,704},{64,0},{128,64},{192,128},{256,192},{320,256},{384,320},{4... | collective-permute-start | bytes 774152 | tf_op jit(solution)/shard_map/ppermute | solution.py:16
  70.1 10.8 %collective-permute-start.8 = (bf16[112,1152]{1,0:T(8,128)(2,1)S(1)}, bf16[112,1152]{1,0:T(8,128)(2,1)S(1)}, u32[]{:S(2)}, u32[]{:S(2)}) collective-permute-start(bf16[112,1152]{1,0:T(8,128)(2,1)S(1)} %collective-permute-done.6), channel_id=1, source_target_pairs={{0,64},{64,128},{128,192},{192,256},{256,320},{320,384},{384,448},... | collective-permute-start | bytes 774152 | tf_op jit(solution)/shard_map/ppermute | solution.py:16
  72.1 10.7 %collective-permute-start.9 = (bf16[112,1152]{1,0:T(8,128)(2,1)S(1)}, bf16[112,1152]{1,0:T(8,128)(2,1)S(1)}, u32[]{:S(2)}, u32[]{:S(2)}) collective-permute-start(bf16[112,1152]{1,0:T(8,128)(2,1)S(1)} %collective-permute-done.7), channel_id=1, source_target_pairs={{0,704},{64,0},{128,64},{192,128},{256,192},{320,256},{384,320},{4... | collective-permute-start | bytes 774152 | tf_op jit(solution)/shard_map/ppermute | solution.py:16
  80.9 8.1 %collective-permute-start.10 = (bf16[56,1152]{1,0:T(8,128)(2,1)S(1)}, bf16[56,1152]{1,0:T(8,128)(2,1)S(1)}, u32[]{:S(2)}, u32[]{:S(2)}) collective-permute-start(bf16[56,1152]{1,0:T(8,128)(2,1)S(1)} %slice.131), channel_id=1, source_target_pairs={{0,64},{64,128},{128,192},{192,256},{256,320},{320,384},{384,448},... | collective-permute-start | bytes 387080 | tf_op jit(solution)/shard_map/ppermute | solution.py:16
  82.9 7.9 %collective-permute-start.11 = (bf16[56,1152]{1,0:T(8,128)(2,1)S(1)}, bf16[56,1152]{1,0:T(8,128)(2,1)S(1)}, u32[]{:S(2)}, u32[]{:S(2)}) collective-permute-start(bf16[56,1152]{1,0:T(8,128)(2,1)S(1)} %slice.133), channel_id=1, source_target_pairs={{0,704},{64,0},{128,64},{192,128},{256,192},{320,256},{384,320},{4... | collective-permute-start | bytes 387080 | tf_op jit(solution)/shard_map/ppermute | solution.py:16
  90.8 1.3 copy-start.1
  92.2 1.6 %copy-start.4 = (f32[256,768]{0,1:T(8,128)}, f32[256,768]{0,1:T(8,128)S(1)}, u32[]{:S(2)}) copy-start(f32[256,768]{0,1:T(8,128)S(1)} %convolution_bitcast_fusion) | copy-start | bytes 2359300
  93.8 33.3 %all-to-all-start.1 = ((bf16[24,56,384]{2,1,0:T(8,128)(2,1)}), bf16[24,56,384]{2,1,0:T(8,128)(2,1)S(1)}, u32[]{:S(2)}, u32[]{:S(2)}) async-start(bf16[24,56,384]{2,1,0:T(8,128)(2,1)} %bitcast.125), calls=%async_computation.1 | async-start | bytes 2064384 | tf_op jit(solution)/shard_map/all_to_all | solution.py:27
  97.6 1.8 %copy-start.2 = (bf16[12,112,768]{2,1,0:T(8,128)(2,1)S(1)}, bf16[12,112,768]{2,1,0:T(8,128)(2,1)}, u32[]{:S(2)}) copy-start(bf16[12,112,768]{2,1,0:T(8,128)(2,1)} %copy-done.1) | copy-start | bytes 6193156
  100.2 3.5 %collective-permute-start.12 = (bf16[672,256]{1,0:T(8,128)(2,1)S(1)}, bf16[672,256]{1,0:T(8,128)(2,1)S(1)}, u32[]{:S(2)}, u32[]{:S(2)}) collective-permute-start(bf16[672,256]{1,0:T(8,128)(2,1)S(1)} %constant_dynamic-slice_fusion), channel_id=1, source_target_pairs={{0,1},{1,0},{2,3},{3,2},{4,5},{5,4},{6,7},{7,6},{8,9},{9,8},{10,11... | collective-permute-start | bytes 1032200 | tf_op jit(solution)/shard_map/ppermute | solution.py:16
  103.8 9.1 %collective-permute-start.13 = (bf16[672,256]{1,0:T(8,128)(2,1)S(1)}, bf16[672,256]{1,0:T(8,128)(2,1)S(1)}, u32[]{:S(2)}, u32[]{:S(2)}) collective-permute-start(bf16[672,256]{1,0:T(8,128)(2,1)S(1)} %add_convert_fusion.2), channel_id=1, source_target_pairs={{0,2},{1,7},{2,0},{3,5},{4,6},{5,3},{6,4},{7,1},{8,10},{9,15},{10,... | collective-permute-start | bytes 1032200 | tf_op jit(solution)/shard_map/ppermute | solution.py:75
  113.0 10.4 %collective-permute-start.14 = (bf16[672,256]{1,0:T(8,128)(2,1)S(1)}, bf16[672,256]{1,0:T(8,128)(2,1)S(1)}, u32[]{:S(2)}, u32[]{:S(2)}) collective-permute-start(bf16[672,256]{1,0:T(8,128)(2,1)S(1)} %add_convert_fusion.1), channel_id=1, source_target_pairs={{0,6},{1,3},{2,4},{3,1},{4,2},{5,7},{6,0},{7,5},{8,14},{9,11},{10,... | collective-permute-start | bytes 1032200 | tf_op jit(solution)/shard_map/ppermute | solution.py:75
  123.5 3.5 %collective-permute-start.15 = (bf16[672,256]{1,0:T(8,128)(2,1)S(1)}, bf16[672,256]{1,0:T(8,128)(2,1)S(1)}, u32[]{:S(2)}, u32[]{:S(2)}) collective-permute-start(bf16[672,256]{1,0:T(8,128)(2,1)S(1)} %add_convert_fusion), channel_id=1, source_target_pairs={{0,1},{1,0},{2,3},{3,2},{4,5},{5,4},{6,7},{7,6},{8,9},{9,8},{10,11... | collective-permute-start | bytes 1032200 | tf_op jit(solution)/shard_map/ppermute | solution.py:16
  127.9 18.9 %all-to-all-start.2 = ((bf16[4,14,384]{2,1,0:T(8,128)(2,1)}), bf16[4,14,384]{2,1,0:T(8,128)(2,1)S(1)}, u32[]{:S(2)}, u32[]{:S(2)}) async-start(bf16[4,14,384]{2,1,0:T(8,128)(2,1)} %reshape.25), calls=%async_computation.2 | async-start | bytes 98304 | tf_op jit(solution)/shard_map/all_to_all | solution.py:27

commit v7 on v6

--- a/solution.py
+++ b/solution.py
@@ -28,6 +28,12 @@
     return got.astype(jnp.float32).sum(axis=0)
 
 
+def contract_rows(left, right):
+    return lax.dot_general(
+        left, right, (((0,), (0,)), ((), ())), preferred_element_type=jnp.float32
+    )
+
+
 def contract_cols(left, right):
     return lax.dot_general(
         left, right, (((1,), (1,)), ((), ())), preferred_element_type=jnp.float32
@@ -43,7 +49,7 @@
 def around(block, axis, widths):
     peers = lax.axis_size(axis)
     rows = block.shape[0]
-    half = rows // 2
+    half = rows // 16 * 8
     place = lax.axis_index(axis)
     ends = np.cumsum(widths)
     wholes = [jnp.zeros((peers, rows, w), block.dtype) for w in widths]
@@ -79,19 +85,21 @@
     return (left.astype(jnp.float32) + right.astype(jnp.float32)).astype(jnp.bfloat16)
 
 
-def summed_over_tp(partial):
+def summed_over_tp(partial, back, blocks):
     half = partial.shape[0] // 2
     core = lax.axis_index("core")
     kept = lax.dynamic_slice_in_dim(partial, core * half, half)
     given = lax.dynamic_slice_in_dim(partial, (1 - core) * half, half)
     total = added(kept, shifted(given, "core", 1))
+    total = jnp.dot(back, total, preferred_element_type=jnp.float32).astype(jnp.bfloat16)
     total = added(total, paired(total, 0))
     other = paired(total, 1)
     total = added(total, other)
     other = shifted(total, "core", 1)
     first = jnp.where(core == 0, total, other)
     second = jnp.where(core == 0, other, total)
-    return jnp.concatenate([first, second])
+    halves = [h.reshape(blocks, -1, h.shape[1]) for h in (first, second)]
+    return jnp.stack(halves, axis=1).reshape(partial.shape)
 
 
 def gradients(tokens, cotangent, gate_weight, up_weight, down_weight):
@@ -100,14 +108,19 @@
     width = tokens.shape[1]
 
     weights = jnp.concatenate([gate_weight, up_weight, down_weight.T], axis=1)
-    weights = sent_to_all(weights, "fs_1").reshape(inner * rows, 3 * units)
-    gate_up, down = around(weights, FS_0, (2 * units, units))
+    weights = sent_to_all(weights, FS_0[::-1]).reshape(-1, 3 * units)
+    gate_up, down = around(weights, ("fs_1",), (2 * units, units))
 
     spot = np.arange(width).reshape(FAR, near, inner, rows).transpose(2, 1, 0, 3).reshape(-1)
-    turned_cotangent = contract_cols(picked(spot), cotangent).astype(jnp.bfloat16)
-    turned_cotangent = lax.optimization_barrier(turned_cotangent)
+    turn = lax.optimization_barrier(picked(spot))
+    turned_tokens = contract_cols(turn, tokens).astype(jnp.bfloat16)
+    turned_cotangent = contract_cols(turn, cotangent).astype(jnp.bfloat16)
+    back = np.arange(width // 2).reshape(-1, near, FAR, rows).transpose(2, 1, 0, 3).reshape(-1)
+    turned_tokens, turned_cotangent, back = lax.optimization_barrier(
+        (turned_tokens, turned_cotangent, picked(back))
+    )
 
-    both = jnp.dot(tokens, gate_up, preferred_element_type=jnp.float32)
+    both = contract_rows(turned_tokens, gate_up)
     gate_pre, up_pre = both[:, :units], both[:, units:]
     sigmoid_gate = jax.nn.sigmoid(gate_pre)
     activated = gate_pre * sigmoid_gate
@@ -119,13 +132,13 @@
     terms = terms.astype(jnp.bfloat16).reshape(FAR, rows, units)
     down_grad = exchanged(terms, "fs_0h").T
 
-    hidden_grad = jnp.dot(cotangent, down, preferred_element_type=jnp.float32)
+    hidden_grad = contract_rows(turned_cotangent, down)
     gate_pre_grad = (
         hidden_grad * up_pre * sigmoid_gate * (1.0 + gate_pre * (1.0 - sigmoid_gate))
     ).astype(jnp.bfloat16)
     up_pre_grad = (hidden_grad * activated).astype(jnp.bfloat16)
     partial = contract_cols(gate_up, jnp.concatenate([gate_pre_grad, up_pre_grad], axis=1))
-    total = summed_over_tp(partial.astype(jnp.bfloat16))
+    total = summed_over_tp(partial.astype(jnp.bfloat16), back, near * FAR)
     return (total.T, down_grad)
 
 

time: 148 us -> 150 us (1.014)
  starting transfers between devices: 81.4 us -> 65.5 us
  waiting for transfers between devices: 52.1 us -> 58.6 us
  matrix products: 7.1 us -> 12.2 us
  other arithmetic: 2.79 us -> 6.42 us
  local copies, waits for them, and re-layouts: 2.74 us -> 4.95 us
    ppermute x14 -> x10, starting transfers between devices: 56.6 us -> 28.8 us  [shifted(): lax.ppermute(array, axis, [(k, (k + step) % peers) for k in range(peers)])]
    all_to_all x1, starting transfers between devices: 7.55 us -> 15.2 us  [sent_to_all(): lax.all_to_all(jnp.broadcast_to(array[None], (peers, *array.shape)), axis...]
    convert_element_type x0 -> x2, other arithmetic: none -> 4.53 us  [picked(): return (source[:, None] == spot).astype(jnp.bfloat16)]
    all_to_all x2, starting transfers between devices: 12.1 us -> 16.4 us  [exchanged(): got = lax.all_to_all(parts, axis, 0, 0, tiled=True)]
    all_to_all x1, waiting for transfers between devices: 8.86 us -> 12.4 us  [sent_to_all(): lax.all_to_all(jnp.broadcast_to(array[None], (peers, *array.shape)), axis...]
    dot_general x2 -> x3, matrix products: 2.89 us -> 6.26 us  [contract_cols(): lax.dot_general(left, right, (((1,), (1,)), ((), ())), preferred_element_...]
    ppermute x14 -> x10, waiting for transfers between devices: 19.3 us -> 22 us  [shifted(): lax.ppermute(array, axis, [(k, (k + step) % peers) for k in range(peers)])]
    dot_general x2 -> x3, matrix products: 2.63 us -> 4.4 us  [the longest x2 2.94 us: contract_rows(): lax.dot_general(left, right, (((0,), (0,)), ((), ())), preferred_element_...]
  transfers between devices with their start and end apart: 19 -> 15, of which waited for: 14 -> 13; matrix products, arithmetic and copies ran while one was open for 5% -> 11% of each run, Pallas kernels for 0% -> 0%
where the time goes in v7:
time: 150 us; the launch traced here: 149 us
  starting transfers between devices  65.5 us (44%)
  waiting for transfers between devices  58.6 us (39%)
  matrix products  12.2 us (8%)
  other arithmetic  6.42 us (4%)
  local copies, waits for them, and re-layouts  4.95 us (3%)
    ppermute x10, starting transfers between devices, shifted(): lax.ppermute(array, axis, [(k, (k + step) % peers) for k in range(peers)])  28.8 us
    ppermute x10, waiting for transfers between devices, shifted(): lax.ppermute(array, axis, [(k, (k + step) % peers) for k in range(peers)])  22 us
    all_to_all x2, starting transfers between devices, exchanged(): got = lax.all_to_all(parts, axis, 0, 0, tiled=True)  16.4 us
    all_to_all x1, starting transfers between devices, sent_to_all(): lax.all_to_all(jnp.broadcast_to(array[None], (peers, *array.shape)), axis...  15.2 us
    ppermute x2, waiting for transfers between devices, paired(): return lax.ppermute(array, ('chip', 'core'), pairs)  14.4 us
    all_to_all x1, waiting for transfers between devices, sent_to_all(): lax.all_to_all(jnp.broadcast_to(array[None], (peers, *array.shape)), axis...  12.4 us
    all_to_all x2, waiting for transfers between devices, exchanged(): got = lax.all_to_all(parts, axis, 0, 0, tiled=True)  9.74 us
    dot_general x3, matrix products, contract_cols(): lax.dot_general(left, right, (((1,), (1,)), ((), ())), preferred_element_...  6.26 us
  transfers between devices with their start and end apart: 15, of which 13 were waited for; matrix products, arithmetic and copies ran while one was open for 11% of the time, Pallas kernels for 0%

profile of v7, /device:TPU:14, one launch (start us, length us, event | category | flops | bytes accessed | tf_op | source)
XLA Modules:
  0.0 148.7 jit_solution(12285485755598809294)
XLA Ops:
  0.6 0.0 copy-start
  0.6 0.8 pad_maximum_fusion.1
  1.5 0.8 broadcast_in_dim.69
  2.3 15.2 %all-to-all-start = ((bf16[12,14,1152]{2,1,0:T(8,128)(2,1)}), bf16[12,14,1152]{2,1,0:T(8,128)(2,1)S(1)}, u32[]{:S(2)}, u32[]{:S(2)}) async-start(bf16[12,14,1152]{2,1,0:T(8,128)(2,1)} %broadcast_in_dim.69), calls=%async_computation | async-start | bytes 884736 | tf_op jit(solution)/shard_map/all_to_all | solution.py:21
  17.4 0.0 copy-start.6
  17.5 3.3 %fusion = bf16[1344,1344]{1,0:T(8,128)(2,1)} fusion(s32[1344]{0:T(1024)} %constant.92.clone), kind=kLoop, calls=%fused_computation.1 | loop fusion | flops 3612672 | bytes 3618048 | tf_op jit(solution)/shard_map/convert_element_type | solution.py:46
  20.8 0.0 copy-done.6
  20.8 1.2 fusion.1
  22.0 0.0 copy-done
  22.0 4.3 %convolution_convert_fusion.2 = bf16[1344,256]{1,0:T(8,128)(2,1)} fusion(bf16[1344,1344]{1,0:T(8,128)(2,1)} %fusion, bf16[256,1344]{0,1:T(8,128)(2,1)S(1)} %copy-done), kind=kOutput, calls=%fused_computation.4 | convolution fusion | flops 925188096 | bytes 4988928 | tf_op jit(solution)/shard_map/dot_general | solution.py:38
  26.3 0.0 copy-done.1
  26.3 0.0 copy-done.7
  26.3 1.2 convolution_convert_fusion.3
  27.6 12.4 %all-to-all-done = bf16[12,14,1152]{2,1,0:T(8,128)(2,1)S(1)} async-done(((bf16[12,14,1152]{2,1,0:T(8,128)(2,1)}), bf16[12,14,1152]{2,1,0:T(8,128)(2,1)S(1)}, u32[]{:S(2)}, u32[]{:S(2)}) %all-to-all-start) | async-done | bytes 387104 | tf_op jit(solution)/shard_map/all_to_all | solution.py:21
  40.0 0.1 reshape.25
  40.1 2.4 %collective-permute-start.1 = (bf16[168,1152]{1,0:T(8,128)(2,1)S(1)}, bf16[168,1152]{1,0:T(8,128)(2,1)S(1)}, u32[]{:S(2)}, u32[]{:S(2)}) collective-permute-start(bf16[168,1152]{1,0:T(8,128)(2,1)S(1)} %reshape.25), channel_id=1, source_target_pairs={{0,56},{8,0},{16,8},{24,16},{32,24},{40,32},{48,40},{56,48},{1,57}... | collective-permute-start | bytes 1161224 | tf_op jit(solution)/shard_map/ppermute | solution.py:16
  42.5 3.5 %collective-permute-start = (bf16[168,1152]{1,0:T(8,128)(2,1)S(1)}, bf16[168,1152]{1,0:T(8,128)(2,1)S(1)}, u32[]{:S(2)}, u32[]{:S(2)}) collective-permute-start(bf16[168,1152]{1,0:T(8,128)(2,1)S(1)} %reshape.25), channel_id=1, source_target_pairs={{0,8},{8,16},{16,24},{24,32},{32,40},{40,48},{48,56},{56,0},{1,9},... | collective-permute-start | bytes 1161224 | tf_op jit(solution)/shard_map/ppermute | solution.py:16
  46.0 0.1 broadcast_in_dim.79
  46.1 0.1 broadcast_in_dim.68
  46.3 4.1 %collective-permute-done.1 = bf16[168,1152]{1,0:T(8,128)(2,1)S(1)} collective-permute-done((bf16[168,1152]{1,0:T(8,128)(2,1)S(1)}, bf16[168,1152]{1,0:T(8,128)(2,1)S(1)}, u32[]{:S(2)}, u32[]{:S(2)}) %collective-permute-start.1) | collective-permute-done | bytes 387104 | tf_op jit(solution)/shard_map/ppermute | solution.py:16
  50.4 3.3 %collective-permute-start.3 = (bf16[168,1152]{1,0:T(8,128)(2,1)S(1)}, bf16[168,1152]{1,0:T(8,128)(2,1)S(1)}, u32[]{:S(2)}, u32[]{:S(2)}) collective-permute-start(bf16[168,1152]{1,0:T(8,128)(2,1)S(1)} %collective-permute-done.1), channel_id=1, source_target_pairs={{0,56},{8,0},{16,8},{24,16},{32,24},{40,32},{48,40},{56,48},{1,57}... | collective-permute-start | bytes 1161224 | tf_op jit(solution)/shard_map/ppermute | solution.py:16
  53.7 0.5 collective-permute-done
  54.2 2.0 %collective-permute-start.2 = (bf16[168,1152]{1,0:T(8,128)(2,1)S(1)}, bf16[168,1152]{1,0:T(8,128)(2,1)S(1)}, u32[]{:S(2)}, u32[]{:S(2)}) collective-permute-start(bf16[168,1152]{1,0:T(8,128)(2,1)S(1)} %collective-permute-done), channel_id=1, source_target_pairs={{0,8},{8,16},{16,24},{24,32},{32,40},{40,48},{48,56},{56,0},{1,9},... | collective-permute-start | bytes 1161224 | tf_op jit(solution)/shard_map/ppermute | solution.py:16
  56.3 3.6 %collective-permute-done.3 = bf16[168,1152]{1,0:T(8,128)(2,1)S(1)} collective-permute-done((bf16[168,1152]{1,0:T(8,128)(2,1)S(1)}, bf16[168,1152]{1,0:T(8,128)(2,1)S(1)}, u32[]{:S(2)}, u32[]{:S(2)}) %collective-permute-start.3) | collective-permute-done | bytes 387104 | tf_op jit(solution)/shard_map/ppermute | solution.py:16
  59.9 4.5 %collective-permute-start.5 = (bf16[168,1152]{1,0:T(8,128)(2,1)S(1)}, bf16[168,1152]{1,0:T(8,128)(2,1)S(1)}, u32[]{:S(2)}, u32[]{:S(2)}) collective-permute-start(bf16[168,1152]{1,0:T(8,128)(2,1)S(1)} %collective-permute-done.3), channel_id=1, source_target_pairs={{0,56},{8,0},{16,8},{24,16},{32,24},{40,32},{48,40},{56,48},{1,57}... | collective-permute-start | bytes 1161224 | tf_op jit(solution)/shard_map/ppermute | solution.py:16
  64.5 0.5 collective-permute-done.2
  65.0 1.9 %collective-permute-start.4 = (bf16[168,1152]{1,0:T(8,128)(2,1)S(1)}, bf16[168,1152]{1,0:T(8,128)(2,1)S(1)}, u32[]{:S(2)}, u32[]{:S(2)}) collective-permute-start(bf16[168,1152]{1,0:T(8,128)(2,1)S(1)} %collective-permute-done.2), channel_id=1, source_target_pairs={{0,8},{8,16},{16,24},{24,32},{32,40},{40,48},{48,56},{56,0},{1,9},... | collective-permute-start | bytes 1161224 | tf_op jit(solution)/shard_map/ppermute | solution.py:16
  67.0 2.9 %collective-permute-done.5 = bf16[168,1152]{1,0:T(8,128)(2,1)S(1)} collective-permute-done((bf16[168,1152]{1,0:T(8,128)(2,1)S(1)}, bf16[168,1152]{1,0:T(8,128)(2,1)S(1)}, u32[]{:S(2)}, u32[]{:S(2)}) %collective-permute-start.5) | collective-permute-done | bytes 387104 | tf_op jit(solution)/shard_map/ppermute | solution.py:16
  69.9 5.4 %collective-permute-start.7 = (bf16[88,1152]{1,0:T(8,128)(2,1)S(1)}, bf16[88,1152]{1,0:T(8,128)(2,1)S(1)}, u32[]{:S(2)}, u32[]{:S(2)}) collective-permute-start(bf16[88,1152]{1,0:T(8,128)(2,1)S(1)} %slice.97), channel_id=1, source_target_pairs={{0,56},{8,0},{16,8},{24,16},{32,24},{40,32},{48,40},{56,48},{1,57}... | collective-permute-start | bytes 608264 | tf_op jit(solution)/shard_map/ppermute | solution.py:16
  75.3 0.5 collective-permute-done.4
  75.8 1.9 %collective-permute-start.6 = (bf16[80,1152]{1,0:T(8,128)(2,1)S(1)}, bf16[80,1152]{1,0:T(8,128)(2,1)S(1)}, u32[]{:S(2)}, u32[]{:S(2)}) collective-permute-start(bf16[80,1152]{1,0:T(8,128)(2,1)S(1)} %slice.95), channel_id=1, source_target_pairs={{0,8},{8,16},{16,24},{24,32},{32,40},{40,48},{48,56},{56,0},{1,9},... | collective-permute-start | bytes 552968 | tf_op jit(solution)/shard_map/ppermute | solution.py:16
  77.9 6.8 %collective-permute-done.6 = bf16[80,1152]{1,0:T(8,128)(2,1)S(1)} collective-permute-done((bf16[80,1152]{1,0:T(8,128)(2,1)S(1)}, bf16[80,1152]{1,0:T(8,128)(2,1)S(1)}, u32[]{:S(2)}, u32[]{:S(2)}) %collective-permute-start.6) | collective-permute-done | bytes 184352 | tf_op jit(solution)/shard_map/ppermute | solution.py:16
  84.7 0.0 copy-start.9
  84.7 0.0 collective-permute-done.7
  84.8 0.0 copy-start.2
  84.8 0.8 fusion.29
  85.6 0.0 copy-start.8
  85.6 0.9 copy-done.8
  86.5 1.6 %convolution_convert_fusion = bf16[1344,384]{1,0:T(8,128)(2,1)} fusion(bf16[1344,256]{1,0:T(8,128)(2,1)S(1)} %copy-done.9, f32[256,768]{1,0:T(8,128)S(1)} %fusion.29), kind=kOutput, calls=%fused_computation.2 | convolution fusion | flops 265347072 | bytes 2506752 | tf_op jit(solution)/shard_map/dot_general | solution.py:129
  88.1 8.6 %all-to-all-start.1 = ((bf16[24,56,384]{2,1,0:T(8,128)(2,1)}), bf16[24,56,384]{2,1,0:T(8,128)(2,1)S(1)}, u32[]{:S(2)}, u32[]{:S(2)}) async-start(bf16[24,56,384]{2,1,0:T(8,128)(2,1)} %bitcast.98), calls=%async_computation.1 | async-start | bytes 2064384 | tf_op jit(solution)/shard_map/all_to_all | solution.py:27
  96.7 2.1 %multiply_convert_fusion.2 = (bf16[256,384]{1,0:T(8,128)(2,1)S(1)}, bf16[256,384]{1,0:T(8,128)(2,1)S(1)}) fusion(f32[256,768]{1,0:T(8,128)} %copy-done.8, bf16[1344,256]{1,0:T(8,128)(2,1)} %convolution_convert_fusion.2, bf16[1344,384]{1,0:T(8,128)(2,1)S(1)} %bitcast.97), kind=kOutput, calls=%fused_computation.18 | convolution fusion | flops 265519104 | bytes 2899968 | tf_op jit(solution)/shard_map/dot_general | solution.py:32
  98.9 0.7 convolution_convert_fusion.1
  99.6 0.0 copy-start.5
  99.6 0.8 copy-done.5
  100.5 1.9 %collective-permute-start.8 = (bf16[672,256]{1,0:T(8,128)(2,1)S(1)}, bf16[672,256]{1,0:T(8,128)(2,1)S(1)}, u32[]{:S(2)}, u32[]{:S(2)}) collective-permute-start(bf16[672,256]{1,0:T(8,128)(2,1)S(1)} %constant_dynamic-slice_fusion), channel_id=1, source_target_pairs={{0,1},{1,0},{2,3},{3,2},{4,5},{5,4},{6,7},{7,6},{8,9},{9,8},{10,11... | collective-permute-start | bytes 1032200 | tf_op jit(solution)/shard_map/ppermute | solution.py:16
  102.4 1.6 %collective-permute-done.8 = bf16[672,256]{1,0:T(8,128)(2,1)S(1)} collective-permute-done((bf16[672,256]{1,0:T(8,128)(2,1)S(1)}, bf16[672,256]{1,0:T(8,128)(2,1)S(1)}, u32[]{:S(2)}, u32[]{:S(2)}) %collective-permute-start.8) | collective-permute-done | bytes 344096 | tf_op jit(solution)/shard_map/ppermute | solution.py:16
  104.1 0.0 copy-done.4
  104.1 1.5 convolution_convert_fusion.4
  105.5 2.7 %collective-permute-start.9 = (bf16[672,256]{1,0:T(8,128)(2,1)S(1)}, bf16[672,256]{1,0:T(8,128)(2,1)S(1)}, u32[]{:S(2)}, u32[]{:S(2)}) collective-permute-start(bf16[672,256]{1,0:T(8,128)(2,1)S(1)} %convolution_convert_fusion.4), channel_id=1, source_target_pairs={{0,2},{1,7},{2,0},{3,5},{4,6},{5,3},{6,4},{7,1},{8,10},{9,15},{10,... | collective-permute-start | bytes 1032200 | tf_op jit(solution)/shard_map/ppermute | solution.py:81
  108.3 6.4 %collective-permute-done.9 = bf16[672,256]{1,0:T(8,128)(2,1)S(1)} collective-permute-done((bf16[672,256]{1,0:T(8,128)(2,1)S(1)}, bf16[672,256]{1,0:T(8,128)(2,1)S(1)}, u32[]{:S(2)}, u32[]{:S(2)}) %collective-permute-start.9) | collective-permute-done | bytes 344096 | tf_op jit(solution)/shard_map/ppermute | solution.py:81
  114.7 0.1 add_convert_fusion.1
  114.8 2.4 %collective-permute-start.10 = (bf16[672,256]{1,0:T(8,128)(2,1)S(1)}, bf16[672,256]{1,0:T(8,128)(2,1)S(1)}, u32[]{:S(2)}, u32[]{:S(2)}) collective-permute-start(bf16[672,256]{1,0:T(8,128)(2,1)S(1)} %add_convert_fusion.1), channel_id=1, source_target_pairs={{0,6},{1,3},{2,4},{3,1},{4,2},{5,7},{6,0},{7,5},{8,14},{9,11},{10,... | collective-permute-start | bytes 1032200 | tf_op jit(solution)/shard_map/ppermute | solution.py:81
  117.2 8.0 %collective-permute-done.10 = bf16[672,256]{1,0:T(8,128)(2,1)S(1)} collective-permute-done((bf16[672,256]{1,0:T(8,128)(2,1)S(1)}, bf16[672,256]{1,0:T(8,128)(2,1)S(1)}, u32[]{:S(2)}, u32[]{:S(2)}) %collective-permute-start.10) | collective-permute-done | bytes 344096 | tf_op jit(solution)/shard_map/ppermute | solution.py:81
  125.1 0.1 add_convert_fusion
  125.2 1.9 %collective-permute-start.11 = (bf16[672,256]{1,0:T(8,128)(2,1)S(1)}, bf16[672,256]{1,0:T(8,128)(2,1)S(1)}, u32[]{:S(2)}, u32[]{:S(2)}) collective-permute-start(bf16[672,256]{1,0:T(8,128)(2,1)S(1)} %add_convert_fusion), channel_id=1, source_target_pairs={{0,1},{1,0},{2,3},{3,2},{4,5},{5,4},{6,7},{7,6},{8,9},{9,8},{10,11... | collective-permute-start | bytes 1032200 | tf_op jit(solution)/shard_map/ppermute | solution.py:16
  127.2 1.6 %collective-permute-done.11 = bf16[672,256]{1,0:T(8,128)(2,1)S(1)} collective-permute-done((bf16[672,256]{1,0:T(8,128)(2,1)S(1)}, bf16[672,256]{1,0:T(8,128)(2,1)S(1)}, u32[]{:S(2)}, u32[]{:S(2)}) %collective-permute-start.11) | collective-permute-done | bytes 344096 | tf_op jit(solution)/shard_map/ppermute | solution.py:16
  128.8 0.0 all-to-all-done.1
  128.8 0.1 reduce_sum.21
  129.0 0.6 reshape.30
  129.6 7.8 %all-to-all-start.2 = ((bf16[4,14,384]{2,1,0:T(8,128)(2,1)}), bf16[4,14,384]{2,1,0:T(8,128)(2,1)S(1)}, u32[]{:S(2)}, u32[]{:S(2)}) async-start(bf16[4,14,384]{2,1,0:T(8,128)(2,1)} %reshape.30), calls=%async_computation.2 | async-start | bytes 98304 | tf_op jit(solution)/shard_map/all_to_all | solution.py:27
  137.4 0.1 pad_maximum_fusion
  137.5 0.9 copy.10
  138.4 9.7 %all-to-all-done.2 = bf16[4,14,384]{2,1,0:T(8,128)(2,1)S(1)} async-done(((bf16[4,14,384]{2,1,0:T(8,128)(2,1)}), bf16[4,14,384]{2,1,0:T(8,128)(2,1)S(1)}, u32[]{:S(2)}, u32[]{:S(2)}) %all-to-all-start.2) | async-done | bytes 43040 | tf_op jit(solution)/shard_map/all_to_all | solution.py:27
  148.1 0.6 convert_reduce_fusion
  (29 shorter events, 0.5 us)
Async XLA Ops:
  0.6 21.4 %copy-start = (bf16[256,1344]{0,1:T(8,128)(2,1)S(1)}, bf16[256,1344]{0,1:T(8,128)(2,1)}, u32[]{:S(2)}) copy-start(bf16[256,1344]{0,1:T(8,128)(2,1)} %param.8) | copy-start | bytes 2064388
  2.3 37.7 %all-to-all-start = ((bf16[12,14,1152]{2,1,0:T(8,128)(2,1)}), bf16[12,14,1152]{2,1,0:T(8,128)(2,1)S(1)}, u32[]{:S(2)}, u32[]{:S(2)}) async-start(bf16[12,14,1152]{2,1,0:T(8,128)(2,1)} %broadcast_in_dim.69), calls=%async_computation | async-start | bytes 884736 | tf_op jit(solution)/shard_map/all_to_all | solution.py:21
  17.4 3.3 %copy-start.6 = (s32[672]{0:T(1024)S(1)}, s32[672]{0:T(1024)}, u32[]{:S(2)}) copy-start(s32[672]{0:T(1024)} %constant.93.clone) | copy-start | bytes 8068
  22.0 4.3 %copy-start.1 = (bf16[1344,1344]{1,0:T(8,128)(2,1)S(1)}, bf16[1344,1344]{1,0:T(8,128)(2,1)}, u32[]{:S(2)}) copy-start(bf16[1344,1344]{1,0:T(8,128)(2,1)} %fusion) | copy-start | bytes 10838020
  22.0 4.3 %copy-start.7 = (bf16[256,1344]{0,1:T(8,128)(2,1)S(1)}, bf16[256,1344]{0,1:T(8,128)(2,1)}, u32[]{:S(2)}) copy-start(bf16[256,1344]{0,1:T(8,128)(2,1)} %param.7) | copy-start | bytes 2064388
  40.1 10.2 %collective-permute-start.1 = (bf16[168,1152]{1,0:T(8,128)(2,1)S(1)}, bf16[168,1152]{1,0:T(8,128)(2,1)S(1)}, u32[]{:S(2)}, u32[]{:S(2)}) collective-permute-start(bf16[168,1152]{1,0:T(8,128)(2,1)S(1)} %reshape.25), channel_id=1, source_target_pairs={{0,56},{8,0},{16,8},{24,16},{32,24},{40,32},{48,40},{56,48},{1,57}... | collective-permute-start | bytes 1161224 | tf_op jit(solution)/shard_map/ppermute | solution.py:16
  42.5 11.7 %collective-permute-start = (bf16[168,1152]{1,0:T(8,128)(2,1)S(1)}, bf16[168,1152]{1,0:T(8,128)(2,1)S(1)}, u32[]{:S(2)}, u32[]{:S(2)}) collective-permute-start(bf16[168,1152]{1,0:T(8,128)(2,1)S(1)} %reshape.25), channel_id=1, source_target_pairs={{0,8},{8,16},{16,24},{24,32},{32,40},{40,48},{48,56},{56,0},{1,9},... | collective-permute-start | bytes 1161224 | tf_op jit(solution)/shard_map/ppermute | solution.py:16
  50.4 9.6 %collective-permute-start.3 = (bf16[168,1152]{1,0:T(8,128)(2,1)S(1)}, bf16[168,1152]{1,0:T(8,128)(2,1)S(1)}, u32[]{:S(2)}, u32[]{:S(2)}) collective-permute-start(bf16[168,1152]{1,0:T(8,128)(2,1)S(1)} %collective-permute-done.1), channel_id=1, source_target_pairs={{0,56},{8,0},{16,8},{24,16},{32,24},{40,32},{48,40},{56,48},{1,57}... | collective-permute-start | bytes 1161224 | tf_op jit(solution)/shard_map/ppermute | solution.py:16
  54.2 10.8 %collective-permute-start.2 = (bf16[168,1152]{1,0:T(8,128)(2,1)S(1)}, bf16[168,1152]{1,0:T(8,128)(2,1)S(1)}, u32[]{:S(2)}, u32[]{:S(2)}) collective-permute-start(bf16[168,1152]{1,0:T(8,128)(2,1)S(1)} %collective-permute-done), channel_id=1, source_target_pairs={{0,8},{8,16},{16,24},{24,32},{32,40},{40,48},{48,56},{56,0},{1,9},... | collective-permute-start | bytes 1161224 | tf_op jit(solution)/shard_map/ppermute | solution.py:16
  59.9 10.0 %collective-permute-start.5 = (bf16[168,1152]{1,0:T(8,128)(2,1)S(1)}, bf16[168,1152]{1,0:T(8,128)(2,1)S(1)}, u32[]{:S(2)}, u32[]{:S(2)}) collective-permute-start(bf16[168,1152]{1,0:T(8,128)(2,1)S(1)} %collective-permute-done.3), channel_id=1, source_target_pairs={{0,56},{8,0},{16,8},{24,16},{32,24},{40,32},{48,40},{56,48},{1,57}... | collective-permute-start | bytes 1161224 | tf_op jit(solution)/shard_map/ppermute | solution.py:16
  65.0 10.8 %collective-permute-start.4 = (bf16[168,1152]{1,0:T(8,128)(2,1)S(1)}, bf16[168,1152]{1,0:T(8,128)(2,1)S(1)}, u32[]{:S(2)}, u32[]{:S(2)}) collective-permute-start(bf16[168,1152]{1,0:T(8,128)(2,1)S(1)} %collective-permute-done.2), channel_id=1, source_target_pairs={{0,8},{8,16},{16,24},{24,32},{32,40},{40,48},{48,56},{56,0},{1,9},... | collective-permute-start | bytes 1161224 | tf_op jit(solution)/shard_map/ppermute | solution.py:16
  69.9 14.8 %collective-permute-start.7 = (bf16[88,1152]{1,0:T(8,128)(2,1)S(1)}, bf16[88,1152]{1,0:T(8,128)(2,1)S(1)}, u32[]{:S(2)}, u32[]{:S(2)}) collective-permute-start(bf16[88,1152]{1,0:T(8,128)(2,1)S(1)} %slice.97), channel_id=1, source_target_pairs={{0,56},{8,0},{16,8},{24,16},{32,24},{40,32},{48,40},{56,48},{1,57}... | collective-permute-start | bytes 608264 | tf_op jit(solution)/shard_map/ppermute | solution.py:16
  75.8 8.9 %collective-permute-start.6 = (bf16[80,1152]{1,0:T(8,128)(2,1)S(1)}, bf16[80,1152]{1,0:T(8,128)(2,1)S(1)}, u32[]{:S(2)}, u32[]{:S(2)}) collective-permute-start(bf16[80,1152]{1,0:T(8,128)(2,1)S(1)} %slice.95), channel_id=1, source_target_pairs={{0,8},{8,16},{16,24},{24,32},{32,40},{40,48},{48,56},{56,0},{1,9},... | collective-permute-start | bytes 552968 | tf_op jit(solution)/shard_map/ppermute | solution.py:16
  84.7 1.8 %copy-start.9 = (bf16[1344,256]{1,0:T(8,128)(2,1)S(1)}, bf16[1344,256]{1,0:T(8,128)(2,1)}, u32[]{:S(2)}) copy-start(bf16[1344,256]{1,0:T(8,128)(2,1)} %convolution_convert_fusion.2) | copy-start | bytes 2064388
  84.8 3.3 %copy-start.2 = (bf16[8,168,768]{2,1,0:T(8,128)(2,1)}, bf16[8,168,768]{2,1,0:T(8,128)(2,1)S(1)}, u32[]{:S(2)}) copy-start(bf16[8,168,768]{2,1,0:T(8,128)(2,1)S(1)} %fusion.14) | copy-start | bytes 6193156
  85.6 0.9 copy-start.8
  88.1 40.7 %all-to-all-start.1 = ((bf16[24,56,384]{2,1,0:T(8,128)(2,1)}), bf16[24,56,384]{2,1,0:T(8,128)(2,1)S(1)}, u32[]{:S(2)}, u32[]{:S(2)}) async-start(bf16[24,56,384]{2,1,0:T(8,128)(2,1)} %bitcast.98), calls=%async_computation.1 | async-start | bytes 2064384 | tf_op jit(solution)/shard_map/all_to_all | solution.py:27
  96.7 2.2 %copy-start.3 = (bf16[8,168,768]{2,1,0:T(8,128)(2,1)S(1)}, bf16[8,168,768]{2,1,0:T(8,128)(2,1)}, u32[]{:S(2)}) copy-start(bf16[8,168,768]{2,1,0:T(8,128)(2,1)} %copy-done.2) | copy-start | bytes 6193156
  98.9 5.2 %copy-start.4 = (bf16[672,672]{1,0:T(8,128)(2,1)S(1)}, bf16[672,672]{1,0:T(8,128)(2,1)}, u32[]{:S(2)}) copy-start(bf16[672,672]{1,0:T(8,128)(2,1)} %fusion.1) | copy-start | bytes 2709508
  99.6 0.8 copy-start.5
  100.5 3.5 %collective-permute-start.8 = (bf16[672,256]{1,0:T(8,128)(2,1)S(1)}, bf16[672,256]{1,0:T(8,128)(2,1)S(1)}, u32[]{:S(2)}, u32[]{:S(2)}) collective-permute-start(bf16[672,256]{1,0:T(8,128)(2,1)S(1)} %constant_dynamic-slice_fusion), channel_id=1, source_target_pairs={{0,1},{1,0},{2,3},{3,2},{4,5},{5,4},{6,7},{7,6},{8,9},{9,8},{10,11... | collective-permute-start | bytes 1032200 | tf_op jit(solution)/shard_map/ppermute | solution.py:16
  105.5 9.1 %collective-permute-start.9 = (bf16[672,256]{1,0:T(8,128)(2,1)S(1)}, bf16[672,256]{1,0:T(8,128)(2,1)S(1)}, u32[]{:S(2)}, u32[]{:S(2)}) collective-permute-start(bf16[672,256]{1,0:T(8,128)(2,1)S(1)} %convolution_convert_fusion.4), channel_id=1, source_target_pairs={{0,2},{1,7},{2,0},{3,5},{4,6},{5,3},{6,4},{7,1},{8,10},{9,15},{10,... | collective-permute-start | bytes 1032200 | tf_op jit(solution)/shard_map/ppermute | solution.py:81
  114.8 10.4 %collective-permute-start.10 = (bf16[672,256]{1,0:T(8,128)(2,1)S(1)}, bf16[672,256]{1,0:T(8,128)(2,1)S(1)}, u32[]{:S(2)}, u32[]{:S(2)}) collective-permute-start(bf16[672,256]{1,0:T(8,128)(2,1)S(1)} %add_convert_fusion.1), channel_id=1, source_target_pairs={{0,6},{1,3},{2,4},{3,1},{4,2},{5,7},{6,0},{7,5},{8,14},{9,11},{10,... | collective-permute-start | bytes 1032200 | tf_op jit(solution)/shard_map/ppermute | solution.py:81
  125.2 3.5 %collective-permute-start.11 = (bf16[672,256]{1,0:T(8,128)(2,1)S(1)}, bf16[672,256]{1,0:T(8,128)(2,1)S(1)}, u32[]{:S(2)}, u32[]{:S(2)}) collective-permute-start(bf16[672,256]{1,0:T(8,128)(2,1)S(1)} %add_convert_fusion), channel_id=1, source_target_pairs={{0,1},{1,0},{2,3},{3,2},{4,5},{5,4},{6,7},{7,6},{8,9},{9,8},{10,11... | collective-permute-start | bytes 1032200 | tf_op jit(solution)/shard_map/ppermute | solution.py:16
  129.6 18.5 %all-to-all-start.2 = ((bf16[4,14,384]{2,1,0:T(8,128)(2,1)}), bf16[4,14,384]{2,1,0:T(8,128)(2,1)S(1)}, u32[]{:S(2)}, u32[]{:S(2)}) async-start(bf16[4,14,384]{2,1,0:T(8,128)(2,1)} %reshape.30), calls=%async_computation.2 | async-start | bytes 98304 | tf_op jit(solution)/shard_map/all_to_all | solution.py:27

commit v8 on v7

--- a/solution.py
+++ b/solution.py
@@ -49,7 +49,6 @@
 def around(block, axis, widths):
     peers = lax.axis_size(axis)
     rows = block.shape[0]
-    half = rows // 16 * 8
     place = lax.axis_index(axis)
     ends = np.cumsum(widths)
     wholes = [jnp.zeros((peers, rows, w), block.dtype) for w in widths]
@@ -66,8 +65,13 @@
         up, down = shifted(up, axis, 1), shifted(down, axis, -1)
         put(up, place - step, 0)
         put(down, place + step, 0)
-    put(shifted(up[:half], axis, 1), place + peers // 2, 0)
-    put(shifted(down[half:], axis, -1), place + peers // 2, half)
+    last = jnp.where(lax.axis_index("core") == 0, up, down)
+    pairs = [
+        (2 * k + core, 2 * ((k + 1 - 2 * core) % peers) + core)
+        for k in range(peers)
+        for core in range(2)
+    ]
+    put(lax.ppermute(last, (*axis, "core"), pairs), place + peers // 2, 0)
     return [w.reshape(peers * rows, -1) for w in wholes]
 
 

time: 150 us -> 153 us (1.020)
  the two profiles are of different devices: /device:TPU:14 before, /device:TPU:8 now
where the time goes in v8:
time: 153 us; the launch traced here: 152 us
  starting transfers between devices  63 us (41%)
  waiting for transfers between devices  62.9 us (41%)
  matrix products  12.2 us (8%)
  local copies, waits for them, and re-layouts  6.55 us (4%)
  other arithmetic  6.48 us (4%)
    ppermute x8, starting transfers between devices, shifted(): lax.ppermute(array, axis, [(k, (k + step) % peers) for k in range(peers)])  21.5 us
    ppermute x8, waiting for transfers between devices, shifted(): lax.ppermute(array, axis, [(k, (k + step) % peers) for k in range(peers)])  20.6 us
    all_to_all x2, starting transfers between devices, exchanged(): got = lax.all_to_all(parts, axis, 0, 0, tiled=True)  16.3 us
    all_to_all x1, starting transfers between devices, sent_to_all(): lax.all_to_all(jnp.broadcast_to(array[None], (peers, *array.shape)), axis...  15.2 us
    all_to_all x1, waiting for transfers between devices, sent_to_all(): lax.all_to_all(jnp.broadcast_to(array[None], (peers, *array.shape)), axis...  12.4 us
    ppermute x2, waiting for transfers between devices, paired(): return lax.ppermute(array, ('chip', 'core'), pairs)  11.4 us
    all_to_all x2, waiting for transfers between devices, exchanged(): got = lax.all_to_all(parts, axis, 0, 0, tiled=True)  9.74 us
    ppermute x1, waiting for transfers between devices, around(): put(lax.ppermute(last, (*axis, 'core'), pairs), place + peers // 2, 0)  8.74 us
  transfers between devices with their start and end apart: 14, of which 13 were waited for; matrix products, arithmetic and copies ran while one was open for 11% of the time, Pallas kernels for 0%

profile of v8, /device:TPU:8, one launch (start us, length us, event | category | flops | bytes accessed | tf_op | source)
XLA Modules:
  0.0 152.2 jit_solution(1588279070471654618)
XLA Ops:
  0.6 0.0 copy-start
  0.6 0.8 pad_maximum_fusion.1
  1.5 0.8 broadcast_in_dim.63
  2.3 15.2 %all-to-all-start = ((bf16[12,14,1152]{2,1,0:T(8,128)(2,1)}), bf16[12,14,1152]{2,1,0:T(8,128)(2,1)S(1)}, u32[]{:S(2)}, u32[]{:S(2)}) async-start(bf16[12,14,1152]{2,1,0:T(8,128)(2,1)} %broadcast_in_dim.63), calls=%async_computation | async-start | bytes 884736 | tf_op jit(solution)/shard_map/all_to_all | solution.py:21
  17.4 0.0 copy-start.7
  17.5 3.3 %fusion = bf16[1344,1344]{1,0:T(8,128)(2,1)} fusion(s32[1344]{0:T(1024)} %constant.88.clone), kind=kLoop, calls=%fused_computation.1 | loop fusion | flops 3612672 | bytes 3618048 | tf_op jit(solution)/shard_map/convert_element_type | solution.py:46
  20.8 0.0 copy-done.7
  20.8 1.2 fusion.1
  22.0 0.0 copy-done
  22.0 4.3 %convolution_convert_fusion.2 = bf16[1344,256]{1,0:T(8,128)(2,1)} fusion(bf16[1344,1344]{1,0:T(8,128)(2,1)} %fusion, bf16[256,1344]{0,1:T(8,128)(2,1)S(1)} %copy-done), kind=kOutput, calls=%fused_computation.4 | convolution fusion | flops 925188096 | bytes 4988928 | tf_op jit(solution)/shard_map/dot_general | solution.py:38
  26.3 0.0 copy-done.1
  26.3 0.0 copy-done.8
  26.3 1.2 convolution_convert_fusion.3
  27.6 12.4 %all-to-all-done = bf16[12,14,1152]{2,1,0:T(8,128)(2,1)S(1)} async-done(((bf16[12,14,1152]{2,1,0:T(8,128)(2,1)}), bf16[12,14,1152]{2,1,0:T(8,128)(2,1)S(1)}, u32[]{:S(2)}, u32[]{:S(2)}) %all-to-all-start) | async-done | bytes 387104 | tf_op jit(solution)/shard_map/all_to_all | solution.py:21
  40.0 0.1 reshape.25
  40.1 2.4 %collective-permute-start.1 = (bf16[168,1152]{1,0:T(8,128)(2,1)S(1)}, bf16[168,1152]{1,0:T(8,128)(2,1)S(1)}, u32[]{:S(2)}, u32[]{:S(2)}) collective-permute-start(bf16[168,1152]{1,0:T(8,128)(2,1)S(1)} %reshape.25), channel_id=1, source_target_pairs={{0,56},{8,0},{16,8},{24,16},{32,24},{40,32},{48,40},{56,48},{1,57}... | collective-permute-start | bytes 1161224 | tf_op jit(solution)/shard_map/ppermute | solution.py:16
  42.5 3.5 %collective-permute-start = (bf16[168,1152]{1,0:T(8,128)(2,1)S(1)}, bf16[168,1152]{1,0:T(8,128)(2,1)S(1)}, u32[]{:S(2)}, u32[]{:S(2)}) collective-permute-start(bf16[168,1152]{1,0:T(8,128)(2,1)S(1)} %reshape.25), channel_id=1, source_target_pairs={{0,8},{8,16},{16,24},{24,32},{32,40},{40,48},{48,56},{56,0},{1,9},... | collective-permute-start | bytes 1161224 | tf_op jit(solution)/shard_map/ppermute | solution.py:16
  46.0 0.1 broadcast_in_dim.72
  46.1 0.1 broadcast_in_dim.62
  46.3 4.1 %collective-permute-done.1 = bf16[168,1152]{1,0:T(8,128)(2,1)S(1)} collective-permute-done((bf16[168,1152]{1,0:T(8,128)(2,1)S(1)}, bf16[168,1152]{1,0:T(8,128)(2,1)S(1)}, u32[]{:S(2)}, u32[]{:S(2)}) %collective-permute-start.1) | collective-permute-done | bytes 387104 | tf_op jit(solution)/shard_map/ppermute | solution.py:16
  50.4 3.3 %collective-permute-start.3 = (bf16[168,1152]{1,0:T(8,128)(2,1)S(1)}, bf16[168,1152]{1,0:T(8,128)(2,1)S(1)}, u32[]{:S(2)}, u32[]{:S(2)}) collective-permute-start(bf16[168,1152]{1,0:T(8,128)(2,1)S(1)} %collective-permute-done.1), channel_id=1, source_target_pairs={{0,56},{8,0},{16,8},{24,16},{32,24},{40,32},{48,40},{56,48},{1,57}... | collective-permute-start | bytes 1161224 | tf_op jit(solution)/shard_map/ppermute | solution.py:16
  53.7 0.5 collective-permute-done
  54.2 2.0 %collective-permute-start.2 = (bf16[168,1152]{1,0:T(8,128)(2,1)S(1)}, bf16[168,1152]{1,0:T(8,128)(2,1)S(1)}, u32[]{:S(2)}, u32[]{:S(2)}) collective-permute-start(bf16[168,1152]{1,0:T(8,128)(2,1)S(1)} %collective-permute-done), channel_id=1, source_target_pairs={{0,8},{8,16},{16,24},{24,32},{32,40},{40,48},{48,56},{56,0},{1,9},... | collective-permute-start | bytes 1161224 | tf_op jit(solution)/shard_map/ppermute | solution.py:16
  56.3 3.6 %collective-permute-done.3 = bf16[168,1152]{1,0:T(8,128)(2,1)S(1)} collective-permute-done((bf16[168,1152]{1,0:T(8,128)(2,1)S(1)}, bf16[168,1152]{1,0:T(8,128)(2,1)S(1)}, u32[]{:S(2)}, u32[]{:S(2)}) %collective-permute-start.3) | collective-permute-done | bytes 387104 | tf_op jit(solution)/shard_map/ppermute | solution.py:16
  59.9 4.5 %collective-permute-start.5 = (bf16[168,1152]{1,0:T(8,128)(2,1)S(1)}, bf16[168,1152]{1,0:T(8,128)(2,1)S(1)}, u32[]{:S(2)}, u32[]{:S(2)}) collective-permute-start(bf16[168,1152]{1,0:T(8,128)(2,1)S(1)} %collective-permute-done.3), channel_id=1, source_target_pairs={{0,56},{8,0},{16,8},{24,16},{32,24},{40,32},{48,40},{56,48},{1,57}... | collective-permute-start | bytes 1161224 | tf_op jit(solution)/shard_map/ppermute | solution.py:16
  64.5 0.5 collective-permute-done.2
  65.0 1.9 %collective-permute-start.4 = (bf16[168,1152]{1,0:T(8,128)(2,1)S(1)}, bf16[168,1152]{1,0:T(8,128)(2,1)S(1)}, u32[]{:S(2)}, u32[]{:S(2)}) collective-permute-start(bf16[168,1152]{1,0:T(8,128)(2,1)S(1)} %collective-permute-done.2), channel_id=1, source_target_pairs={{0,8},{8,16},{16,24},{24,32},{32,40},{40,48},{48,56},{56,0},{1,9},... | collective-permute-start | bytes 1161224 | tf_op jit(solution)/shard_map/ppermute | solution.py:16
  67.0 2.9 %collective-permute-done.5 = bf16[168,1152]{1,0:T(8,128)(2,1)S(1)} collective-permute-done((bf16[168,1152]{1,0:T(8,128)(2,1)S(1)}, bf16[168,1152]{1,0:T(8,128)(2,1)S(1)}, u32[]{:S(2)}, u32[]{:S(2)}) %collective-permute-start.5) | collective-permute-done | bytes 387104 | tf_op jit(solution)/shard_map/ppermute | solution.py:16
  69.9 5.9 %collective-permute-done.4 = bf16[168,1152]{1,0:T(8,128)(2,1)S(1)} collective-permute-done((bf16[168,1152]{1,0:T(8,128)(2,1)S(1)}, bf16[168,1152]{1,0:T(8,128)(2,1)S(1)}, u32[]{:S(2)}, u32[]{:S(2)}) %collective-permute-start.4) | collective-permute-done | bytes 387104 | tf_op jit(solution)/shard_map/ppermute | solution.py:16
  75.8 0.1 broadcast_select_fusion
  75.9 1.9 %collective-permute-start.6 = (bf16[168,1152]{1,0:T(8,128)(2,1)S(1)}, bf16[168,1152]{1,0:T(8,128)(2,1)S(1)}, u32[]{:S(2)}, u32[]{:S(2)}) collective-permute-start(bf16[168,1152]{1,0:T(8,128)(2,1)S(1)} %broadcast_select_fusion), channel_id=1, source_target_pairs={{0,8},{1,57},{8,16},{9,1},{16,24},{17,9},{24,32},{25,17},{32,40},{... | collective-permute-start | bytes 1161224 | tf_op jit(solution)/shard_map/ppermute | solution.py:74
  77.9 0.0 copy-start.10
  77.9 8.7 %collective-permute-done.6 = bf16[168,1152]{1,0:T(8,128)(2,1)S(1)} collective-permute-done((bf16[168,1152]{1,0:T(8,128)(2,1)S(1)}, bf16[168,1152]{1,0:T(8,128)(2,1)S(1)}, u32[]{:S(2)}, u32[]{:S(2)}) %collective-permute-start.6) | collective-permute-done | bytes 387104 | tf_op jit(solution)/shard_map/ppermute | solution.py:74
  86.7 0.7 copy-done.5
  87.4 0.8 fusion.27
  88.2 0.0 copy-start.9
  88.2 0.9 copy-done.9
  89.2 1.6 %convolution_convert_fusion = bf16[1344,384]{1,0:T(8,128)(2,1)} fusion(bf16[1344,256]{1,0:T(8,128)(2,1)S(1)} %copy-done.10, f32[256,768]{1,0:T(8,128)S(1)} %fusion.27), kind=kOutput, calls=%fused_computation.2 | convolution fusion | flops 265347072 | bytes 2506752 | tf_op jit(solution)/shard_map/dot_general | solution.py:133
  90.7 7.4 %all-to-all-start.1 = ((bf16[24,56,384]{2,1,0:T(8,128)(2,1)}), bf16[24,56,384]{2,1,0:T(8,128)(2,1)S(1)}, u32[]{:S(2)}, u32[]{:S(2)}) async-start(bf16[24,56,384]{2,1,0:T(8,128)(2,1)} %bitcast.90), calls=%async_computation.1 | async-start | bytes 2064384 | tf_op jit(solution)/shard_map/all_to_all | solution.py:27
  98.1 0.9 fusion.15
  99.1 0.0 copy-start.3
  99.1 2.1 %multiply_convert_fusion.2 = (bf16[256,384]{1,0:T(8,128)(2,1)S(1)}, bf16[256,384]{1,0:T(8,128)(2,1)S(1)}) fusion(f32[256,768]{1,0:T(8,128)} %copy-done.9, bf16[1344,256]{1,0:T(8,128)(2,1)} %convolution_convert_fusion.2, bf16[1344,384]{1,0:T(8,128)(2,1)S(1)} %bitcast.89), kind=kOutput, calls=%fused_computation.18 | convolution fusion | flops 265519104 | bytes 2899968 | tf_op jit(solution)/shard_map/dot_general | solution.py:32
  101.2 0.7 convolution_convert_fusion.1
  102.0 0.0 copy-start.6
  102.0 0.8 copy-done.6
  102.8 1.9 %collective-permute-start.7 = (bf16[672,256]{1,0:T(8,128)(2,1)S(1)}, bf16[672,256]{1,0:T(8,128)(2,1)S(1)}, u32[]{:S(2)}, u32[]{:S(2)}) collective-permute-start(bf16[672,256]{1,0:T(8,128)(2,1)S(1)} %constant_dynamic-slice_fusion), channel_id=1, source_target_pairs={{0,1},{1,0},{2,3},{3,2},{4,5},{5,4},{6,7},{7,6},{8,9},{9,8},{10,11... | collective-permute-start | bytes 1032200 | tf_op jit(solution)/shard_map/ppermute | solution.py:16
  104.8 1.6 %collective-permute-done.7 = bf16[672,256]{1,0:T(8,128)(2,1)S(1)} collective-permute-done((bf16[672,256]{1,0:T(8,128)(2,1)S(1)}, bf16[672,256]{1,0:T(8,128)(2,1)S(1)}, u32[]{:S(2)}, u32[]{:S(2)}) %collective-permute-start.7) | collective-permute-done | bytes 344096 | tf_op jit(solution)/shard_map/ppermute | solution.py:16
  106.4 1.4 convolution_convert_fusion.4
  107.9 3.4 %collective-permute-start.8 = (bf16[672,256]{1,0:T(8,128)(2,1)S(1)}, bf16[672,256]{1,0:T(8,128)(2,1)S(1)}, u32[]{:S(2)}, u32[]{:S(2)}) collective-permute-start(bf16[672,256]{1,0:T(8,128)(2,1)S(1)} %convolution_convert_fusion.4), channel_id=1, source_target_pairs={{0,2},{1,7},{2,0},{3,5},{4,6},{5,3},{6,4},{7,1},{8,10},{9,15},{10,... | collective-permute-start | bytes 1032200 | tf_op jit(solution)/shard_map/ppermute | solution.py:85
  111.3 5.7 %collective-permute-done.8 = bf16[672,256]{1,0:T(8,128)(2,1)S(1)} collective-permute-done((bf16[672,256]{1,0:T(8,128)(2,1)S(1)}, bf16[672,256]{1,0:T(8,128)(2,1)S(1)}, u32[]{:S(2)}, u32[]{:S(2)}) %collective-permute-start.8) | collective-permute-done | bytes 344096 | tf_op jit(solution)/shard_map/ppermute | solution.py:85
  117.0 0.1 add_convert_fusion.1
  117.1 4.7 %collective-permute-start.9 = (bf16[672,256]{1,0:T(8,128)(2,1)S(1)}, bf16[672,256]{1,0:T(8,128)(2,1)S(1)}, u32[]{:S(2)}, u32[]{:S(2)}) collective-permute-start(bf16[672,256]{1,0:T(8,128)(2,1)S(1)} %add_convert_fusion.1), channel_id=1, source_target_pairs={{0,6},{1,3},{2,4},{3,1},{4,2},{5,7},{6,0},{7,5},{8,14},{9,11},{10,... | collective-permute-start | bytes 1032200 | tf_op jit(solution)/shard_map/ppermute | solution.py:85
  121.8 5.7 %collective-permute-done.9 = bf16[672,256]{1,0:T(8,128)(2,1)S(1)} collective-permute-done((bf16[672,256]{1,0:T(8,128)(2,1)S(1)}, bf16[672,256]{1,0:T(8,128)(2,1)S(1)}, u32[]{:S(2)}, u32[]{:S(2)}) %collective-permute-start.9) | collective-permute-done | bytes 344096 | tf_op jit(solution)/shard_map/ppermute | solution.py:85
  127.5 0.1 add_convert_fusion
  127.6 1.9 %collective-permute-start.10 = (bf16[672,256]{1,0:T(8,128)(2,1)S(1)}, bf16[672,256]{1,0:T(8,128)(2,1)S(1)}, u32[]{:S(2)}, u32[]{:S(2)}) collective-permute-start(bf16[672,256]{1,0:T(8,128)(2,1)S(1)} %add_convert_fusion), channel_id=1, source_target_pairs={{0,1},{1,0},{2,3},{3,2},{4,5},{5,4},{6,7},{7,6},{8,9},{9,8},{10,11... | collective-permute-start | bytes 1032200 | tf_op jit(solution)/shard_map/ppermute | solution.py:16
  129.5 1.6 %collective-permute-done.10 = bf16[672,256]{1,0:T(8,128)(2,1)S(1)} collective-permute-done((bf16[672,256]{1,0:T(8,128)(2,1)S(1)}, bf16[672,256]{1,0:T(8,128)(2,1)S(1)}, u32[]{:S(2)}, u32[]{:S(2)}) %collective-permute-start.10) | collective-permute-done | bytes 344096 | tf_op jit(solution)/shard_map/ppermute | solution.py:16
  131.2 0.0 all-to-all-done.1
  131.2 0.1 reduce_sum.21
  131.3 0.6 reshape.30
  132.0 9.0 %all-to-all-start.2 = ((bf16[4,14,384]{2,1,0:T(8,128)(2,1)}), bf16[4,14,384]{2,1,0:T(8,128)(2,1)S(1)}, u32[]{:S(2)}, u32[]{:S(2)}) async-start(bf16[4,14,384]{2,1,0:T(8,128)(2,1)} %reshape.30), calls=%async_computation.2 | async-start | bytes 98304 | tf_op jit(solution)/shard_map/all_to_all | solution.py:27
  140.9 0.1 pad_maximum_fusion
  141.0 0.9 copy.10
  141.9 9.7 %all-to-all-done.2 = bf16[4,14,384]{2,1,0:T(8,128)(2,1)S(1)} async-done(((bf16[4,14,384]{2,1,0:T(8,128)(2,1)}), bf16[4,14,384]{2,1,0:T(8,128)(2,1)S(1)}, u32[]{:S(2)}, u32[]{:S(2)}) %all-to-all-start.2) | async-done | bytes 43040 | tf_op jit(solution)/shard_map/all_to_all | solution.py:27
  151.6 0.6 convert_reduce_fusion
  (26 shorter events, 0.5 us)
Async XLA Ops:
  0.6 21.4 %copy-start = (bf16[256,1344]{0,1:T(8,128)(2,1)S(1)}, bf16[256,1344]{0,1:T(8,128)(2,1)}, u32[]{:S(2)}) copy-start(bf16[256,1344]{0,1:T(8,128)(2,1)} %param.8) | copy-start | bytes 2064388
  2.3 37.7 %all-to-all-start = ((bf16[12,14,1152]{2,1,0:T(8,128)(2,1)}), bf16[12,14,1152]{2,1,0:T(8,128)(2,1)S(1)}, u32[]{:S(2)}, u32[]{:S(2)}) async-start(bf16[12,14,1152]{2,1,0:T(8,128)(2,1)} %broadcast_in_dim.63), calls=%async_computation | async-start | bytes 884736 | tf_op jit(solution)/shard_map/all_to_all | solution.py:21
  17.4 3.3 %copy-start.7 = (s32[672]{0:T(1024)S(1)}, s32[672]{0:T(1024)}, u32[]{:S(2)}) copy-start(s32[672]{0:T(1024)} %constant.89.clone) | copy-start | bytes 8068
  22.0 4.3 %copy-start.1 = (bf16[1344,1344]{1,0:T(8,128)(2,1)S(1)}, bf16[1344,1344]{1,0:T(8,128)(2,1)}, u32[]{:S(2)}) copy-start(bf16[1344,1344]{1,0:T(8,128)(2,1)} %fusion) | copy-start | bytes 10838020
  22.0 4.3 %copy-start.8 = (bf16[256,1344]{0,1:T(8,128)(2,1)S(1)}, bf16[256,1344]{0,1:T(8,128)(2,1)}, u32[]{:S(2)}) copy-start(bf16[256,1344]{0,1:T(8,128)(2,1)} %param.7) | copy-start | bytes 2064388
  40.1 10.2 %collective-permute-start.1 = (bf16[168,1152]{1,0:T(8,128)(2,1)S(1)}, bf16[168,1152]{1,0:T(8,128)(2,1)S(1)}, u32[]{:S(2)}, u32[]{:S(2)}) collective-permute-start(bf16[168,1152]{1,0:T(8,128)(2,1)S(1)} %reshape.25), channel_id=1, source_target_pairs={{0,56},{8,0},{16,8},{24,16},{32,24},{40,32},{48,40},{56,48},{1,57}... | collective-permute-start | bytes 1161224 | tf_op jit(solution)/shard_map/ppermute | solution.py:16
  42.5 11.7 %collective-permute-start = (bf16[168,1152]{1,0:T(8,128)(2,1)S(1)}, bf16[168,1152]{1,0:T(8,128)(2,1)S(1)}, u32[]{:S(2)}, u32[]{:S(2)}) collective-permute-start(bf16[168,1152]{1,0:T(8,128)(2,1)S(1)} %reshape.25), channel_id=1, source_target_pairs={{0,8},{8,16},{16,24},{24,32},{32,40},{40,48},{48,56},{56,0},{1,9},... | collective-permute-start | bytes 1161224 | tf_op jit(solution)/shard_map/ppermute | solution.py:16
  50.4 9.6 %collective-permute-start.3 = (bf16[168,1152]{1,0:T(8,128)(2,1)S(1)}, bf16[168,1152]{1,0:T(8,128)(2,1)S(1)}, u32[]{:S(2)}, u32[]{:S(2)}) collective-permute-start(bf16[168,1152]{1,0:T(8,128)(2,1)S(1)} %collective-permute-done.1), channel_id=1, source_target_pairs={{0,56},{8,0},{16,8},{24,16},{32,24},{40,32},{48,40},{56,48},{1,57}... | collective-permute-start | bytes 1161224 | tf_op jit(solution)/shard_map/ppermute | solution.py:16
  54.2 10.8 %collective-permute-start.2 = (bf16[168,1152]{1,0:T(8,128)(2,1)S(1)}, bf16[168,1152]{1,0:T(8,128)(2,1)S(1)}, u32[]{:S(2)}, u32[]{:S(2)}) collective-permute-start(bf16[168,1152]{1,0:T(8,128)(2,1)S(1)} %collective-permute-done), channel_id=1, source_target_pairs={{0,8},{8,16},{16,24},{24,32},{32,40},{40,48},{48,56},{56,0},{1,9},... | collective-permute-start | bytes 1161224 | tf_op jit(solution)/shard_map/ppermute | solution.py:16
  59.9 10.0 %collective-permute-start.5 = (bf16[168,1152]{1,0:T(8,128)(2,1)S(1)}, bf16[168,1152]{1,0:T(8,128)(2,1)S(1)}, u32[]{:S(2)}, u32[]{:S(2)}) collective-permute-start(bf16[168,1152]{1,0:T(8,128)(2,1)S(1)} %collective-permute-done.3), channel_id=1, source_target_pairs={{0,56},{8,0},{16,8},{24,16},{32,24},{40,32},{48,40},{56,48},{1,57}... | collective-permute-start | bytes 1161224 | tf_op jit(solution)/shard_map/ppermute | solution.py:16
  65.0 10.8 %collective-permute-start.4 = (bf16[168,1152]{1,0:T(8,128)(2,1)S(1)}, bf16[168,1152]{1,0:T(8,128)(2,1)S(1)}, u32[]{:S(2)}, u32[]{:S(2)}) collective-permute-start(bf16[168,1152]{1,0:T(8,128)(2,1)S(1)} %collective-permute-done.2), channel_id=1, source_target_pairs={{0,8},{8,16},{16,24},{24,32},{32,40},{40,48},{48,56},{56,0},{1,9},... | collective-permute-start | bytes 1161224 | tf_op jit(solution)/shard_map/ppermute | solution.py:16
  75.9 10.8 %collective-permute-start.6 = (bf16[168,1152]{1,0:T(8,128)(2,1)S(1)}, bf16[168,1152]{1,0:T(8,128)(2,1)S(1)}, u32[]{:S(2)}, u32[]{:S(2)}) collective-permute-start(bf16[168,1152]{1,0:T(8,128)(2,1)S(1)} %broadcast_select_fusion), channel_id=1, source_target_pairs={{0,8},{1,57},{8,16},{9,1},{16,24},{17,9},{24,32},{25,17},{32,40},{... | collective-permute-start | bytes 1161224 | tf_op jit(solution)/shard_map/ppermute | solution.py:74
  77.9 11.2 %copy-start.10 = (bf16[1344,256]{1,0:T(8,128)(2,1)S(1)}, bf16[1344,256]{1,0:T(8,128)(2,1)}, u32[]{:S(2)}) copy-start(bf16[1344,256]{1,0:T(8,128)(2,1)} %convolution_convert_fusion.2) | copy-start | bytes 2064388
  86.7 0.7 copy-start.5
  87.4 3.3 %copy-start.2 = (bf16[8,168,768]{2,1,0:T(8,128)(2,1)}, bf16[8,168,768]{2,1,0:T(8,128)(2,1)S(1)}, u32[]{:S(2)}) copy-start(bf16[8,168,768]{2,1,0:T(8,128)(2,1)S(1)} %fusion.7) | copy-start | bytes 6193156
  88.2 0.9 copy-start.9
  90.7 40.4 %all-to-all-start.1 = ((bf16[24,56,384]{2,1,0:T(8,128)(2,1)}), bf16[24,56,384]{2,1,0:T(8,128)(2,1)S(1)}, u32[]{:S(2)}, u32[]{:S(2)}) async-start(bf16[24,56,384]{2,1,0:T(8,128)(2,1)} %bitcast.90), calls=%async_computation.1 | async-start | bytes 2064384 | tf_op jit(solution)/shard_map/all_to_all | solution.py:27
  99.1 2.2 %copy-start.3 = (bf16[8,168,768]{2,1,0:T(8,128)(2,1)S(1)}, bf16[8,168,768]{2,1,0:T(8,128)(2,1)}, u32[]{:S(2)}) copy-start(bf16[8,168,768]{2,1,0:T(8,128)(2,1)} %copy-done.2) | copy-start | bytes 6193156
  101.2 5.2 %copy-start.4 = (bf16[672,672]{1,0:T(8,128)(2,1)S(1)}, bf16[672,672]{1,0:T(8,128)(2,1)}, u32[]{:S(2)}) copy-start(bf16[672,672]{1,0:T(8,128)(2,1)} %fusion.1) | copy-start | bytes 2709508
  102.0 0.8 copy-start.6
  102.8 3.5 %collective-permute-start.7 = (bf16[672,256]{1,0:T(8,128)(2,1)S(1)}, bf16[672,256]{1,0:T(8,128)(2,1)S(1)}, u32[]{:S(2)}, u32[]{:S(2)}) collective-permute-start(bf16[672,256]{1,0:T(8,128)(2,1)S(1)} %constant_dynamic-slice_fusion), channel_id=1, source_target_pairs={{0,1},{1,0},{2,3},{3,2},{4,5},{5,4},{6,7},{7,6},{8,9},{9,8},{10,11... | collective-permute-start | bytes 1032200 | tf_op jit(solution)/shard_map/ppermute | solution.py:16
  107.9 9.1 %collective-permute-start.8 = (bf16[672,256]{1,0:T(8,128)(2,1)S(1)}, bf16[672,256]{1,0:T(8,128)(2,1)S(1)}, u32[]{:S(2)}, u32[]{:S(2)}) collective-permute-start(bf16[672,256]{1,0:T(8,128)(2,1)S(1)} %convolution_convert_fusion.4), channel_id=1, source_target_pairs={{0,2},{1,7},{2,0},{3,5},{4,6},{5,3},{6,4},{7,1},{8,10},{9,15},{10,... | collective-permute-start | bytes 1032200 | tf_op jit(solution)/shard_map/ppermute | solution.py:85
  117.1 10.4 %collective-permute-start.9 = (bf16[672,256]{1,0:T(8,128)(2,1)S(1)}, bf16[672,256]{1,0:T(8,128)(2,1)S(1)}, u32[]{:S(2)}, u32[]{:S(2)}) collective-permute-start(bf16[672,256]{1,0:T(8,128)(2,1)S(1)} %add_convert_fusion.1), channel_id=1, source_target_pairs={{0,6},{1,3},{2,4},{3,1},{4,2},{5,7},{6,0},{7,5},{8,14},{9,11},{10,... | collective-permute-start | bytes 1032200 | tf_op jit(solution)/shard_map/ppermute | solution.py:85
  127.6 3.5 %collective-permute-start.10 = (bf16[672,256]{1,0:T(8,128)(2,1)S(1)}, bf16[672,256]{1,0:T(8,128)(2,1)S(1)}, u32[]{:S(2)}, u32[]{:S(2)}) collective-permute-start(bf16[672,256]{1,0:T(8,128)(2,1)S(1)} %add_convert_fusion), channel_id=1, source_target_pairs={{0,1},{1,0},{2,3},{3,2},{4,5},{5,4},{6,7},{7,6},{8,9},{9,8},{10,11... | collective-permute-start | bytes 1032200 | tf_op jit(solution)/shard_map/ppermute | solution.py:16
  132.0 19.7 %all-to-all-start.2 = ((bf16[4,14,384]{2,1,0:T(8,128)(2,1)}), bf16[4,14,384]{2,1,0:T(8,128)(2,1)S(1)}, u32[]{:S(2)}, u32[]{:S(2)}) async-start(bf16[4,14,384]{2,1,0:T(8,128)(2,1)} %reshape.30), calls=%async_computation.2 | async-start | bytes 98304 | tf_op jit(solution)/shard_map/all_to_all | solution.py:27
